TPU v7x, 256 devices: a whole 4x4x8 slice. The times are simulated.
256 devices in a mesh: fs: 32 (over z, x), rep: 4 (over y), tp: 2 (over core).
Axes of the slice: x: 4, y: 4, z: 8, core: 2. Of those that a mesh axis runs over, the one named last changes fastest.
Arguments:
- inputs: bfloat16 [16384, 2048], P(('fs', 'rep')), may hold values from -24 to 24
- query_cot: bfloat16 [16384, 1024], P(('fs', 'rep'), 'tp'), may hold values from -0.046875 to 0.046875
- attended: bfloat16 [16384, 1024], P(('fs', 'rep')), may hold values from -24 to 24
- output_cot: bfloat16 [16384, 2048], P(('fs', 'rep'), 'tp'), may hold values from -0.046875 to 0.046875
- proj_query: bfloat16 [2048, 256], P('fs'), may hold values from -0.125 to 0.125
- proj_output: bfloat16 [1024, 256], P('fs'), may hold values from -0.1875 to 0.1875
- weight_query: float32 [2048, 1024], P('fs', 'tp'), may hold values from -0.125 to 0.125
- weight_output: float32 [1024, 2048], P('fs', 'tp'), may hold values from -0.1875 to 0.1875
- first_query: float32 [256, 1024], P('fs', 'tp'), may hold values from -6 to 6
- second_query: float32 [256, 1024], P('fs', 'tp'), may hold values from 0.0002 to 2
- first_output: float32 [256, 2048], P('fs', 'tp'), may hold values from -6 to 6
- second_output: float32 [256, 2048], P('fs', 'tp'), may hold values from 0.0002 to 2
Outputs:
- new_weight_query: float32 [2048, 1024], P('fs', 'tp')
- new_weight_output: float32 [1024, 2048], P('fs', 'tp')
- step_query: float32 [2048, 1024], P('fs', 'tp')
- step_output: float32 [1024, 2048], P('fs', 'tp')
- new_first_query: float32 [256, 1024], P('fs', 'tp')
- new_second_query: float32 [256, 1024], P('fs', 'tp')
- new_first_output: float32 [256, 2048], P('fs', 'tp')
- new_second_output: float32 [256, 2048], P('fs', 'tp')
- copy_query: bfloat16 [2048, 1024], P(None, 'tp')
- copy_output: bfloat16 [1024, 2048], P(None, 'tp')
All inputs are finite; a program needn't handle non-finite values.
Results may differ from a plain program's by a relative error of at most 0.0031.
Values may be sent and summed in bfloat16 or wider, within the bound.
No kernel may reach another device: no remote copies, remote signals or barrier semaphores. Data moves between devices by JAX's collectives and lax.ppermute only.
A program may use at most 64 MiB of HBM per device.

v0:
```python
import jax
import jax.numpy as jnp
from jax import lax
from jax.sharding import PartitionSpec as P

D = 2048
DA = 1024
RANK = 256


beta_first = 0.9
beta_second = 0.95
adam_eps = 1e-08
mean_eps = 1e-06
learn_rate = 0.02


def joined_along(pieces, dim):
    shape = list(pieces.shape[1:])
    shape[dim] *= pieces.shape[0]
    return jnp.moveaxis(pieces, 0, dim).reshape(shape)


def one_gather(arrays, axis, dims):
    vector = jnp.concatenate([a.reshape(-1) for a in arrays])
    lines, at, gathered = (lax.all_gather(vector, axis), 0, [])
    for a, dim in zip(arrays, dims):
        pieces = lines[:, at : at + a.size].reshape(-1, *a.shape)
        gathered.append(joined_along(pieces, dim))
        at += a.size
    return tuple(gathered)


def cut_along(shard, dim, devices):
    before, after = (shard.shape[:dim], shard.shape[dim + 1 :])
    return jnp.moveaxis(shard.reshape(*before, devices, -1, *after), dim, 0)


def sent_and_summed(shard, axis, dim):
    pieces = cut_along(shard, dim, lax.axis_size(axis))
    arrived = lax.all_to_all(pieces, axis, split_axis=0, concat_axis=0, tiled=True)
    return arrived.sum(axis=0)


def side_by_side(arrays, axis, dim, along):
    both = jnp.concatenate(arrays, axis=along)
    result, at, gathered = (sent_and_summed(both, axis, dim), 0, [])
    for a in arrays:
        gathered.append(lax.slice_in_dim(result, at, at + a.shape[along], axis=along))
        at += a.shape[along]
    return tuple(gathered)


def from_everyone(shard, axis):
    copies = jnp.broadcast_to(shard, (lax.axis_size(axis), *shard.shape))
    return lax.all_to_all(copies, axis, split_axis=0, concat_axis=0, tiled=True)


def of_everyone(shard, axis):
    everything = from_everyone(shard, axis)
    return jnp.sum(everything, axis=0)


def in_one(arrays, axis):
    ends = [0]
    for a in arrays:
        ends.append(ends[-1] + a.size)
    so_far = of_everyone(jnp.concatenate([a.ravel() for a in arrays]), axis)
    return tuple((so_far[b:e].reshape(a.shape) for a, b, e in zip(arrays, ends, ends[1:])))


def in_one_piece(arrays, axis, dim, along):
    widths = [a.shape[along] for a in arrays]
    both = jnp.concatenate(arrays, axis=along)
    result = lax.all_gather(both, axis, axis=dim, tiled=True)
    return tuple(jnp.split(result, [sum(widths[:k]) for k in range(1, len(widths))], axis=along))


def contract_rows(left, right):
    return lax.dot_general(
        left,
        right,
        (((0,), (0,)), ((), ())),
        precision=lax.Precision.HIGHEST,
        preferred_element_type=jnp.float32,
    )


def moment_update(low_sum, first, second):
    first_new = beta_first * first + (1.0 - beta_first) * low_sum
    second_new = beta_second * second + (1.0 - beta_second) * low_sum * low_sum
    normed = first_new / (jnp.sqrt(second_new) + adam_eps)
    return (first_new, second_new, normed)


def local(
    inputs,
    query_cot,
    attended,
    output_cot,
    proj_query,
    proj_output,
    weight_query,
    weight_output,
    first_query,
    second_query,
    first_output,
    second_output,
):
    whole_query, whole_output = one_gather((proj_query, proj_output), "fs", (0, 0))
    reduced_query = jnp.dot(inputs, whole_query, preferred_element_type=jnp.float32)
    reduced_output = jnp.dot(attended, whole_output, preferred_element_type=jnp.float32)
    part_query = contract_rows(reduced_query, query_cot.astype(jnp.float32))
    part_output = contract_rows(reduced_output, output_cot.astype(jnp.float32))
    low_query, low_output = side_by_side((part_query, part_output), "fs", 0, 1)
    low_query, low_output = in_one((low_query, low_output), "rep")
    first_q, second_q, normed_q = moment_update(low_query, first_query, second_query)
    first_o, second_o, normed_o = moment_update(low_output, first_output, second_output)
    local_total = jnp.sum(normed_q * normed_q) + jnp.sum(normed_o * normed_o)
    total = of_everyone(local_total, ("fs", "tp"))
    scale = lax.rsqrt(total / (RANK * (DA + D)) + mean_eps)
    half_q = normed_q.astype(jnp.bfloat16)
    half_o = normed_o.astype(jnp.bfloat16)
    pieces = in_one_piece((half_q, half_o), "fs", 0, 1)
    update_query = jnp.dot(proj_query, pieces[0], preferred_element_type=jnp.float32)
    update_output = jnp.dot(proj_output, pieces[1], preferred_element_type=jnp.float32)
    step_q = scale * update_query
    step_o = scale * update_output
    new_q = weight_query - learn_rate * step_q
    new_o = weight_output - learn_rate * step_o
    copy_q, copy_o = one_gather(
        (new_q.astype(jnp.bfloat16), new_o.astype(jnp.bfloat16)), "fs", (0, 0)
    )
    return (new_q, new_o, step_q, step_o, first_q, second_q, first_o, second_o, copy_q, copy_o)


def solution(mesh):
    return jax.shard_map(
        local,
        mesh=mesh,
        in_specs=(
            P(("fs", "rep"), None),
            P(("fs", "rep"), "tp"),
            P(("fs", "rep"), None),
            P(("fs", "rep"), "tp"),
            P("fs", None),
            P("fs", None),
            P("fs", "tp"),
            P("fs", "tp"),
            P("fs", "tp"),
            P("fs", "tp"),
            P("fs", "tp"),
            P("fs", "tp"),
        ),
        out_specs=(
            P("fs", "tp"),
            P("fs", "tp"),
            P("fs", "tp"),
            P("fs", "tp"),
            P("fs", "tp"),
            P("fs", "tp"),
            P("fs", "tp"),
            P("fs", "tp"),
            P(None, "tp"),
            P(None, "tp"),
        ),
        check_vma=False,
    )
```

profile of v0, /device:TPU:1, one launch (start us, length us, event | category | flops | bytes accessed | tf_op | source)
XLA Modules:
  0.0 311.5 jit_solution(3104404758752084554)
XLA Ops:
  7.2 0.8 copy.29
  8.0 0.8 copy.28
  8.8 0.6 pad_maximum_fusion.1
  9.5 77.9 %all-gather.5.cloned.1.call-done = bf16[786432]{0:T(1024)(128)(2,1)} async-done(((bf16[24576]{0:T(1024)(128)(2,1)}), bf16[786432]{0:T(1024)(128)(2,1)}) %all-gather.5.cloned.1.call-update) | async-done | bytes 1572880 | tf_op jit(solution)/shard_map/all_gather | solution.py:26
  87.4 1.8 reshape.72
  89.2 0.8 slice.55
  90.1 0.5 reshape_reshape.12
  90.7 1.3 reshape_reshape.13
  92.0 0.5 fusion.11
  92.5 0.3 fusion.13
  92.8 0.4 fusion.12
  93.2 0.6 fusion.14
  93.8 0.1 maximum_bitcast_fusion
  93.9 39.3 %all_to_all.17 = f32[32,8,1536]{2,1,0:T(8,128)S(1)} all-to-all(f32[32,8,1536]{2,1,0:T(8,128)S(1)} %maximum_bitcast_fusion), channel_id=1, replica_groups=mesh['fs'=32,'rep'=4,'tp'=2] {'fs'}, dimensions={0} | all-to-all | bytes 3145728 | tf_op jit(solution)/shard_map/all_to_all | solution.py:41
  133.5 9.0 %all_to_all.18 = f32[4,1,12288]{2,1,0:T(1,128)S(1)} all-to-all(f32[4,1,12288]{2,1,0:T(1,128)S(1)} %broadcast_in_dim.6), channel_id=1, replica_groups=mesh['fs'=32,'rep'=4,'tp'=2] {'rep'}, dimensions={0} | all-to-all | bytes 393216 | tf_op jit(solution)/shard_map/all_to_all | solution.py:56
  142.5 0.2 reduce_sum.46
  142.8 0.6 multiply_reduce_fusion.1
  143.4 0.6 multiply_reduce_fusion
  145.3 0.6 broadcast_in_dim.7
  146.0 13.5 %all-to-all-start.2 = ((f32[64,1,1]{2,1,0:T(1,128)}), f32[64,1,1]{2,1,0:T(1,128)S(1)}, u32[]{:S(2)}, u32[]{:S(2)}) async-start(f32[64,1,1]{2,1,0:T(1,128)} %broadcast_in_dim.7), calls=%async_computation.2 | async-start | bytes 65536 | tf_op jit(solution)/shard_map/all_to_all | solution.py:56
  159.6 39.1 %all_gather.17 = bf16[256,1536]{1,0:T(8,128)(2,1)S(1)} all-gather(bf16[8,1536]{1,0:T(8,128)(2,1)S(1)} %pad_maximum_fusion.3), channel_id=1, replica_groups=mesh['fs'=32,'rep'=4,'tp'=2] {'fs'}, dimensions={0}, use_global_device_ids=true | all-gather | bytes 811008 | tf_op jit(solution)/shard_map/all_gather | solution.py:75
  198.7 0.7 reduce_sum.49
  200.1 0.2 fusion
  200.3 0.2 fusion.1
  200.5 0.7 convert_bitcast_fusion.1
  201.2 0.7 convert_bitcast_fusion
  201.9 0.7 pad_maximum_fusion
  202.6 86.1 %all-gather.7.cloned.1.call-done = bf16[2097152]{0:T(1024)(128)(2,1)} async-done(((bf16[65536]{0:T(1024)(128)(2,1)}), bf16[2097152]{0:T(1024)(128)(2,1)}) %all-gather.7.cloned.1.call-update) | async-done | bytes 4194320 | tf_op jit(solution)/shard_map/all_gather | solution.py:26
  288.7 5.6 %reshape.73 = bf16[32,65536]{1,0:T(8,128)(2,1)} reshape(bf16[2097152]{0:T(1024)(128)(2,1)} %all-gather.7.cloned.1.call-done) | data formatting | bytes 8388608 | tf_op jit(solution)/shard_map/all_gather | solution.py:26
  294.3 3.8 %fusion.10 = (bf16[32,32768]{1,0:T(8,128)(2,1)}, bf16[32,32768]{1,0:T(8,128)(2,1)S(1)}) fusion(bf16[32,65536]{1,0:T(8,128)(2,1)} %reshape.73), kind=kLoop, calls=%fused_computation.30 | loop fusion | bytes 8388608 | tf_op jit(solution)/shard_map/slice | solution.py:28
  298.1 4.2 %reshape_reshape.15 = bf16[1024,1024]{1,0:T(8,128)(2,1)} reshape(bf16[32,32768]{1,0:T(8,128)(2,1)} %get-tuple-element.20) | data formatting | bytes 4194304 | tf_op jit(solution)/shard_map/reshape;reshape | solution.py:21
  302.3 2.3 reshape_reshape.14
  (58 shorter events, 0.6 us)
Async XLA Ops:
  7.2 84.8 %copy-start = (bf16[128,2048]{1,0:T(8,128)(2,1)S(1)}, bf16[128,2048]{1,0:T(8,128)(2,1)}, u32[]{:S(2)}) copy-start(bf16[128,2048]{1,0:T(8,128)(2,1)} %param.12) | copy-start | bytes 1572868
  7.2 80.2 %all-gather.5.cloned.1.call-start = ((), (), s32[]{:S(2)}) async-start(), calls=%async_computation.3 | async-start | bytes 1622016 | tf_op jit(solution)/shard_map/all_gather | solution.py:26
  90.1 2.4 copy-start.3
  90.6 2.2 copy-start.9
  90.7 2.6 copy-start.4
  133.2 9.5 %copy-start.16 = (f32[8,512]{1,0:T(8,128)S(1)}, f32[8,512]{1,0:T(8,128)}, u32[]{:S(2)}) copy-start(f32[8,512]{1,0:T(8,128)} %param.21) | copy-start | bytes 49156
  133.2 9.6 %copy-start.17 = (f32[8,512]{1,0:T(8,128)S(1)}, f32[8,512]{1,0:T(8,128)}, u32[]{:S(2)}) copy-start(f32[8,512]{1,0:T(8,128)} %param.20) | copy-start | bytes 49156
  133.2 10.2 %copy-start.14 = (f32[8,1024]{1,0:T(8,128)S(1)}, f32[8,1024]{1,0:T(8,128)}, u32[]{:S(2)}) copy-start(f32[8,1024]{1,0:T(8,128)} %param.23) | copy-start | bytes 98308
  133.2 10.2 %copy-start.15 = (f32[8,1024]{1,0:T(8,128)S(1)}, f32[8,1024]{1,0:T(8,128)}, u32[]{:S(2)}) copy-start(f32[8,1024]{1,0:T(8,128)} %param.22) | copy-start | bytes 98308
  133.2 66.9 %copy-start.11 = (bf16[32,256]{1,0:T(8,128)(2,1)S(1)}, bf16[32,256]{1,0:T(8,128)(2,1)}, u32[]{:S(2)}) copy-start(bf16[32,256]{1,0:T(8,128)(2,1)} %param.17) | copy-start | bytes 49156
  133.3 67.0 %copy-start.10 = (bf16[64,256]{1,0:T(8,128)(2,1)S(1)}, bf16[64,256]{1,0:T(8,128)(2,1)}, u32[]{:S(2)}) copy-start(bf16[64,256]{1,0:T(8,128)(2,1)} %param.16) | copy-start | bytes 98308
  133.3 67.1 %copy-start.5 = (f32[64,512]{1,0:T(8,128)S(1)}, f32[64,512]{1,0:T(8,128)}, u32[]{:S(2)}) copy-start(f32[64,512]{1,0:T(8,128)} %param.18) | copy-start | bytes 393220
  133.4 67.8 %copy-start.6 = (f32[32,1024]{1,0:T(8,128)S(1)}, f32[32,1024]{1,0:T(8,128)}, u32[]{:S(2)}) copy-start(f32[32,1024]{1,0:T(8,128)} %param.19) | copy-start | bytes 393220
  143.4 150.9 %copy-start.12 = (f32[8,512]{1,0:T(8,128)}, f32[8,512]{1,0:T(8,128)S(1)}, u32[]{:S(2)}) copy-start(f32[8,512]{1,0:T(8,128)S(1)} %get-tuple-element.18) | copy-start | bytes 49156
  143.4 150.9 %copy-start.13 = (f32[8,512]{1,0:T(8,128)}, f32[8,512]{1,0:T(8,128)S(1)}, u32[]{:S(2)}) copy-start(f32[8,512]{1,0:T(8,128)S(1)} %get-tuple-element.19) | copy-start | bytes 49156
  144.0 150.2 %copy-start.7 = (f32[8,1024]{1,0:T(8,128)}, f32[8,1024]{1,0:T(8,128)S(1)}, u32[]{:S(2)}) copy-start(f32[8,1024]{1,0:T(8,128)S(1)} %get-tuple-element.15) | copy-start | bytes 98308
  144.0 150.3 %copy-start.8 = (f32[8,1024]{1,0:T(8,128)}, f32[8,1024]{1,0:T(8,128)S(1)}, u32[]{:S(2)}) copy-start(f32[8,1024]{1,0:T(8,128)S(1)} %get-tuple-element.16) | copy-start | bytes 98308
  146.0 52.7 %all-to-all-start.2 = ((f32[64,1,1]{2,1,0:T(1,128)}), f32[64,1,1]{2,1,0:T(1,128)S(1)}, u32[]{:S(2)}, u32[]{:S(2)}) async-start(f32[64,1,1]{2,1,0:T(1,128)} %broadcast_in_dim.7), calls=%async_computation.2 | async-start | bytes 65536 | tf_op jit(solution)/shard_map/all_to_all | solution.py:56
  159.5 129.2 %all-gather.7.cloned.1.call-start = ((), (), s32[]{:S(2)}) async-start(), calls=%async_computation.4 | async-start | bytes 4325376 | tf_op jit(solution)/shard_map/all_gather | solution.py:26
  200.3 94.0 %copy-start.1 = (f32[32,1024]{1,0:T(8,128)}, f32[32,1024]{1,0:T(8,128)S(1)}, u32[]{:S(2)}) copy-start(f32[32,1024]{1,0:T(8,128)S(1)} %fusion) | copy-start | bytes 393220
  200.5 93.8 %copy-start.2 = (f32[64,512]{1,0:T(8,128)}, f32[64,512]{1,0:T(8,128)S(1)}, u32[]{:S(2)}) copy-start(f32[64,512]{1,0:T(8,128)S(1)} %fusion.1) | copy-start | bytes 393220
Sparse Core Ops, SparseCore 0:
  11.2 76.1 all-gather.4
  202.7 85.9 all-gather.6
where the time goes:
time: 315 us; the launch traced here: 311 us
  waiting for transfers between devices  164 us (52%)
  blocking collectives  87.3 us (28%)
  local copies, waits for them, and re-layouts  23 us (7%)
  between operations  16.4 us (5%)
  starting transfers between devices  13.6 us (4%)
  other arithmetic  5.03 us (2%)
    all_gather x2, waiting for transfers between devices, one_gather(): lines, at, gathered = (lax.all_gather(vector, axis), 0, [])  164 us
    all_to_all x1, blocking collectives, sent_and_summed(): lax.all_to_all(pieces, axis, split_axis=0, concat_axis=0, tiled=True)  39.3 us
    all_gather x1, blocking collectives, in_one_piece(): result = lax.all_gather(both, axis, axis=dim, tiled=True)  39.1 us
    all_to_all x1, starting transfers between devices, from_everyone(): return lax.all_to_all(copies, axis, split_axis=0, concat_axis=0, tiled=True)  13.5 us
    all_to_all x1, blocking collectives, from_everyone(): return lax.all_to_all(copies, axis, split_axis=0, concat_axis=0, tiled=True)  8.98 us
    another operation x4, local copies, waits for them, and re-layouts, joined_along(): return jnp.moveaxis(pieces, 0, dim).reshape(shape)  8.37 us
    all_gather x2, local copies, waits for them, and re-layouts, one_gather(): lines, at, gathered = (lax.all_gather(vector, axis), 0, [])  7.42 us
  transfers between devices with their start and end apart: 3, of which 2 were waited for; matrix products, arithmetic and copies ran while one was open for 0% of the time, Pallas kernels for 0%

commit v1 on v0

v1 whole, which is shorter than its diff:
```python
import jax
import jax.numpy as jnp
from jax import lax
from jax.experimental import pallas as pl
from jax.experimental.pallas import tpu as pltpu
from jax.sharding import Mesh, PartitionSpec as P

D = 2048
DA = 1024
RANK = 256
NZ, NX, NREP, NTP = 8, 4, 4, 2
FS = NZ * NX

beta_first = 0.9
beta_second = 0.95
adam_eps = 1e-08
mean_eps = 1e-06
learn_rate = 0.02

bf16 = jnp.bfloat16
f32 = jnp.float32


def exchange(pieces, axes):
    return lax.all_to_all(pieces, axes, split_axis=0, concat_axis=0, tiled=True)


def from_everyone(shard, axes, devices):
    return exchange(jnp.broadcast_to(shard, (devices, *shard.shape)), axes)


def shifted(array, axis, by):
    n = lax.axis_size(axis)
    return lax.ppermute(array, axis, [(i, (i + by) % n) for i in range(n)])


def one_hot(rows_of, columns, rows):
    r = lax.broadcasted_iota(jnp.int32, (rows, columns), 0)
    return (r == rows_of).astype(bf16)


def rank_of(core):
    k = lax.broadcasted_iota(jnp.int32, (1, RANK // NTP), 1)
    x, j, z = k // 32, (k // 8) % 4, k % 8
    return 8 * (4 * z + x) + 2 * j + core


def finish_kernel(scale_ref, w_ref, p_ref, half_ref, copy_q_ref, copy_o_ref):
    rate = learn_rate
    scale = scale_ref[0, 0]
    p = p_ref[...]
    n = p.shape[0]
    pq = p[:, :64, :].reshape(n * 64, RANK)
    po = p[:, 64:, :].reshape(n * 32, RANK)
    uq = jnp.dot(pq, half_ref[:, :512], preferred_element_type=f32)
    uo = jnp.dot(po, half_ref[:, 512:], preferred_element_type=f32)
    wq = w_ref[:, :64, :].reshape(n * 64, 512)
    copy_q_ref[...] = (wq - rate * (scale * uq)).astype(bf16)
    w0 = w_ref[:, 64:96, :].reshape(n * 32, 512)
    w1 = w_ref[:, 96:, :].reshape(n * 32, 512)
    copy_o_ref[:, :512] = (w0 - rate * (scale * uo[:, :512])).astype(bf16)
    copy_o_ref[:, 512:] = (w1 - rate * (scale * uo[:, 512:])).astype(bf16)


def finish(scale, weights, factors, half):
    step = 4
    return pl.pallas_call(
        finish_kernel,
        grid=(FS // step,),
        in_specs=[
            pl.BlockSpec(memory_space=pltpu.SMEM),
            pl.BlockSpec((step, 128, 512), lambda i: (i, 0, 0)),
            pl.BlockSpec((step, 96, RANK), lambda i: (i, 0, 0)),
            pl.BlockSpec((RANK, 1536), lambda i: (0, 0)),
        ],
        out_specs=[
            pl.BlockSpec((step * 64, 512), lambda i: (i, 0)),
            pl.BlockSpec((step * 32, 1024), lambda i: (i, 0)),
        ],
        out_shape=[
            jax.ShapeDtypeStruct((D, 512), bf16),
            jax.ShapeDtypeStruct((DA, 1024), bf16),
        ],
        name="finish",
    )(scale, weights, factors, half)


def local(
    inputs,
    query_cot,
    attended,
    output_cot,
    proj_query,
    proj_output,
    weight_query,
    weight_output,
    first_query,
    second_query,
    first_output,
    second_output,
):
    z, x = lax.axis_index("z"), lax.axis_index("x")
    rep, core = lax.axis_index("rep"), lax.axis_index("tp")
    fs = z * NX + x

    weights = jnp.concatenate(
        [weight_query, weight_output[:, :512], weight_output[:, 512:]], axis=0
    )
    weights = lax.all_gather(weights, ("z", "x"), axis=0, tiled=True)

    cots = jnp.concatenate([query_cot, output_cot], axis=1)
    cots = [cots, shifted(cots, "rep", 1), shifted(cots, "rep", 2), shifted(cots, "rep", 3)]

    both = jnp.concatenate([proj_query, proj_output], axis=0)
    mine = jnp.dot(both, one_hot(rank_of(core), 128, RANK), preferred_element_type=f32)
    mine = mine.astype(bf16).reshape(NREP, 24, 128)
    piece = lax.dynamic_index_in_dim(mine, rep, 0, keepdims=False)
    piece = from_everyone(piece, "z", NZ)
    piece = from_everyone(piece.reshape(NZ * 24, 128), ("x", "rep"), 16)
    factors = piece.reshape(NX, NREP, NZ, 24, 128).transpose(2, 0, 1, 3, 4)
    factors = factors.reshape(FS, 96, 128)
    factors_q = factors[:, :64].reshape(D, 128)
    factors_o = factors[:, 64:].reshape(DA, 128)

    turned = (((0,), (1,)), ((), ()))
    red_q = lax.dot_general(factors_q, inputs, turned, preferred_element_type=f32)
    red_o = lax.dot_general(factors_o, attended, turned, preferred_element_type=f32)
    red = jnp.stack([red_q, red_o]).reshape(2, NX, NREP, NZ, 128)
    red = red.transpose(2, 0, 1, 3, 4).reshape(NREP, 1, 2, 32, 128)
    red = jnp.broadcast_to(red, (NREP, NTP, 2, 32, 128)).reshape(8, 2, 32, 128)
    red = exchange(red, ("rep", "tp")).reshape(NREP, NTP, 2, 32, 128)

    parts = [
        lax.dynamic_index_in_dim(red, (rep - k) % NREP, 0, keepdims=False)
        for k in range(NREP)
    ]
    left_q = jnp.concatenate([p[:, 0].reshape(64, 128) for p in parts], axis=1)
    left_o = jnp.concatenate([p[:, 1].reshape(64, 128) for p in parts], axis=1)
    right = jnp.concatenate(cots, axis=0).astype(f32)
    part_q = jnp.dot(left_q, right[:, :512], precision=lax.Precision.HIGHEST, preferred_element_type=f32)
    part_o = jnp.dot(left_o, right[:, 512:], precision=lax.Precision.HIGHEST, preferred_element_type=f32)
    part = jnp.concatenate([part_q, part_o], axis=1).reshape(NTP, FS, 1536)
    part = exchange(part.transpose(1, 0, 2), ("x", "z"))
    low = part.sum(axis=0)

    low_rows = [low, shifted(low, "rep", 1), shifted(low, "rep", 2), shifted(low, "rep", 3)]

    def own(a):
        return lax.dynamic_slice_in_dim(a, 2 * rep, 2, 0)

    def moments(low_sum, first, second):
        first_new = beta_first * first + (1.0 - beta_first) * low_sum
        second_new = beta_second * second + (1.0 - beta_second) * low_sum * low_sum
        return first_new, second_new

    def normed_of(low_sum, first, second):
        first_new, second_new = moments(low_sum, first, second)
        return first_new / (jnp.sqrt(second_new) + adam_eps)

    normed_q = normed_of(low[:, :512], own(first_query), own(second_query))
    normed_o = normed_of(low[:, 512:], own(first_output), own(second_output))
    local_total = jnp.sum(normed_q * normed_q) + jnp.sum(normed_o * normed_o)

    def thirds(total):
        high = lax.reduce_precision(total, 8, 7)
        middle = lax.reduce_precision(total - high, 8, 7)
        last = total - high - middle
        lane = lax.broadcasted_iota(jnp.int32, (1, 128), 1)
        row = jnp.where(lane == 0, high, jnp.where(lane == 1, middle, jnp.where(lane == 2, last, 0.0)))
        return row.astype(bf16)

    half = jnp.concatenate([normed_q, normed_o], axis=1).astype(bf16)
    sums = jnp.concatenate([thirds(local_total), jnp.zeros((1, 128), bf16)], axis=0)
    half = from_everyone(jnp.concatenate([half, sums], axis=1), "z", NZ)
    half = from_everyone(half.reshape(16, 1664), ("x", "rep"), 16).reshape(RANK, 1664)
    total = jnp.sum(half[:, 1536:].astype(f32))
    total = total + shifted(total.reshape(1, 1), "tp", 1)[0, 0]
    scale = lax.rsqrt(total / (RANK * (DA + D)) + mean_eps)

    others = shifted(factors, "tp", 1)
    k = lax.broadcasted_iota(jnp.int32, (128, RANK), 0)
    c = lax.broadcasted_iota(jnp.int32, (128, RANK), 1)
    spread = (c == 2 * k + core).astype(bf16)
    spread_other = (c == 2 * k + 1 - core).astype(bf16)
    whole = jnp.dot(factors.reshape(FS * 96, 128), spread, preferred_element_type=f32)
    whole = whole + jnp.dot(others.reshape(FS * 96, 128), spread_other, preferred_element_type=f32)
    whole = whole.astype(bf16).reshape(FS, 96, RANK)
    half = half[:, :1536]

    rows = lax.dynamic_index_in_dim(whole, fs, 0, keepdims=False)
    step_q = scale * jnp.dot(rows[:64], half[:, :512], preferred_element_type=f32)
    step_o = scale * jnp.dot(rows[64:], half[:, 512:], preferred_element_type=f32)
    new_q = weight_query - learn_rate * step_q
    new_o = weight_output - learn_rate * step_o
    copy_q, copy_o = finish(
        scale.reshape(1, 1), weights.reshape(FS, 128, 512), whole, half
    )

    rolled = jnp.stack(low_rows)
    order = (rep - jnp.arange(NREP)) % NREP
    low_all = jnp.take(rolled, order, axis=0).reshape(8, 1536)
    first_q, second_q = moments(low_all[:, :512], first_query, second_query)
    first_o, second_o = moments(low_all[:, 512:], first_output, second_output)
    return (new_q, new_o, step_q, step_o, first_q, second_q, first_o, second_o, copy_q, copy_o)


def solution(mesh):
    devices = mesh.devices.reshape(NZ, NX, NREP, NTP)
    grid = Mesh(devices, ("z", "x", "rep", "tp"))
    fs = ("z", "x")
    tokens = ("z", "x", "rep")
    return jax.shard_map(
        local,
        mesh=grid,
        in_specs=(
            P(tokens, None),
            P(tokens, "tp"),
            P(tokens, None),
            P(tokens, "tp"),
            P(fs, None),
            P(fs, None),
            P(fs, "tp"),
            P(fs, "tp"),
            P(fs, "tp"),
            P(fs, "tp"),
            P(fs, "tp"),
            P(fs, "tp"),
        ),
        out_specs=(
            P(fs, "tp"),
            P(fs, "tp"),
            P(fs, "tp"),
            P(fs, "tp"),
            P(fs, "tp"),
            P(fs, "tp"),
            P(fs, "tp"),
            P(fs, "tp"),
            P(None, "tp"),
            P(None, "tp"),
        ),
        check_vma=False,
    )
```

time: 315 us -> 161 us (0.51)
  waiting for transfers between devices: 164 us -> 44 us
  blocking collectives: 87.3 us -> 15.9 us
  starting transfers between devices: 13.6 us -> 48.1 us
  local copies, waits for them, and re-layouts: 23 us -> 8.2 us
  Pallas kernels: 0 us -> 8.69 us
  matrix products: 2.06 us -> 8.89 us
    all_gather x2 -> x1, waiting for transfers between devices: 164 us -> 0.01 us  [local(): weights = lax.all_gather(weights, ('z', 'x'), axis=0, tiled=True)]
    all_to_all x1 -> x5, waiting for transfers between devices: 0.01 us -> 43 us  [exchange(): return lax.all_to_all(pieces, axes, split_axis=0, concat_axis=0, tiled=True)]
    all_gather x1 -> x0, blocking collectives: 39.1 us -> none  [in_one_piece(): result = lax.all_gather(both, axis, axis=dim, tiled=True)]
    all_to_all x2 -> x1, blocking collectives: 48.3 us -> 15.9 us  [exchange(): return lax.all_to_all(pieces, axes, split_axis=0, concat_axis=0, tiled=True)]
    all_to_all x1 -> x5, starting transfers between devices: 13.5 us -> 36.1 us  [exchange(): return lax.all_to_all(pieces, axes, split_axis=0, concat_axis=0, tiled=True)]
    ppermute x0 -> x8, starting transfers between devices: none -> 12 us  [shifted(): return lax.ppermute(array, axis, [(i, (i + by) % n) for i in range(n)])]
    pallas_call x0 -> x1, Pallas kernels: none -> 8.69 us  [finish(): pl.pallas_call(finish_kernel, grid=(FS // step,), in_specs=[pl.BlockSpec(...]
    another operation x4 -> x0, local copies, waits for them, and re-layouts: 8.37 us -> none  [joined_along(): return jnp.moveaxis(pieces, 0, dim).reshape(shape)]
  transfers between devices with their start and end apart: 3 -> 14, of which waited for: 2 -> 6; matrix products, arithmetic and copies ran while one was open for 0% -> 13% of each run, Pallas kernels for 0% -> 0%
where the time goes in v1:
time: 161 us; the launch traced here: 160 us
  starting transfers between devices  48.1 us (30%)
  waiting for transfers between devices  44 us (27%)
  between operations  19.5 us (12%)
  blocking collectives  15.9 us (10%)
  matrix products  8.89 us (6%)
  Pallas kernels  8.69 us (5%)
  local copies, waits for them, and re-layouts  8.2 us (5%)
  other arithmetic  6.43 us (4%)
    all_to_all x5, waiting for transfers between devices, exchange(): return lax.all_to_all(pieces, axes, split_axis=0, concat_axis=0, tiled=True)  43 us
    all_to_all x5, starting transfers between devices, exchange(): return lax.all_to_all(pieces, axes, split_axis=0, concat_axis=0, tiled=True)  36.1 us
    all_to_all x1, blocking collectives, exchange(): return lax.all_to_all(pieces, axes, split_axis=0, concat_axis=0, tiled=True)  15.9 us
    ppermute x8, starting transfers between devices, shifted(): return lax.ppermute(array, axis, [(i, (i + by) % n) for i in range(n)])  12 us
    pallas_call x1, Pallas kernels, finish(): pl.pallas_call(finish_kernel, grid=(FS // step,), in_specs=[pl.BlockSpec(...  8.69 us
  transfers between devices with their start and end apart: 14, of which 6 were waited for; matrix products, arithmetic and copies ran while one was open for 13% of the time, Pallas kernels for 0%

profile of v1, /device:TPU:1, one launch (start us, length us, event | category | flops | bytes accessed | tf_op | source)
XLA Modules:
  0.0 159.7 jit_solution(1189224900390377407)
XLA Ops:
  7.3 1.0 fusion.70
  8.2 1.6 %pad_maximum_fusion.7 = f32[128,512]{1,0:T(8,128)} fusion(f32[32,512]{1,0:T(8,128)S(1)} %get-tuple-element.23, f32[32,512]{1,0:T(8,128)S(1)} %get-tuple-element.22, f32[64,512]{1,0:T(8,128)} %param.18), kind=kLoop, calls=%fused_computation.26 | loop fusion | flops 131072 | bytes 524288 | tf_op jit(solution)/shard_map/concatenate | solution.py:106
  9.9 0.9 convolution_convert_fusion
  10.9 15.9 %all_to_all.30 = bf16[8,24,128]{2,1,0:T(8,128)(2,1)S(1)} all-to-all(bf16[8,24,128]{2,1,0:T(8,128)(2,1)S(1)} %broadcast_in_dim.49), channel_id=1, replica_groups=mesh['z'=8,'x'=4,'rep'=4,'tp'=2] {'z'}, dimensions={0} | all-to-all | bytes 98304 | tf_op jit(solution)/shard_map/all_to_all | solution.py:25
  26.7 1.0 broadcast_in_dim.50
  27.7 6.8 %all-to-all-start.1 = ((bf16[16,192,128]{2,1,0:T(8,128)(2,1)}), bf16[16,192,128]{2,1,0:T(8,128)(2,1)S(1)}, u32[]{:S(2)}, u32[]{:S(2)}) async-start(bf16[16,192,128]{2,1,0:T(8,128)(2,1)} %broadcast_in_dim.50), calls=%async_computation.1 | async-start | bytes 1572864 | tf_op jit(solution)/shard_map/all_to_all | solution.py:25
  34.6 2.6 %collective-permute-start.2 = (bf16[128,1536]{1,0:T(8,128)(2,1)S(1)}, bf16[128,1536]{1,0:T(8,128)(2,1)}, u32[]{:S(2)}, u32[]{:S(2)}) collective-permute-start(bf16[128,1536]{1,0:T(8,128)(2,1)S(1)} %constant_dynamic-update-slice_fusion), channel_id=1, source_target_pairs={{0,6},{2,0},{4,2},{6,4},{1,7},{3,1},{5,3},{7,5},{8,14},{10,8},{12,... | collective-permute-start | bytes 1179656 | tf_op jit(solution)/shard_map/ppermute | solution.py:34
  38.4 7.8 %all-to-all-done.1 = bf16[16,192,128]{2,1,0:T(8,128)(2,1)S(1)} async-done(((bf16[16,192,128]{2,1,0:T(8,128)(2,1)}), bf16[16,192,128]{2,1,0:T(8,128)(2,1)S(1)}, u32[]{:S(2)}, u32[]{:S(2)}) %all-to-all-start.1) | async-done | bytes 786464 | tf_op jit(solution)/shard_map/all_to_all | solution.py:25
  47.7 0.7 broadcast_in_dim.52
  48.4 13.4 %all-to-all-start.2 = ((f32[8,2,32,128]{3,2,1,0:T(8,128)}), f32[8,2,32,128]{3,2,1,0:T(8,128)S(1)}, u32[]{:S(2)}, u32[]{:S(2)}) async-start(f32[8,2,32,128]{3,2,1,0:T(8,128)} %bitcast.20), calls=%async_computation.2 | async-start | bytes 524288 | tf_op jit(solution)/shard_map/all_to_all | solution.py:25
  62.3 6.0 %all-to-all-done.2 = f32[8,2,32,128]{3,2,1,0:T(8,128)S(1)} async-done(((f32[8,2,32,128]{3,2,1,0:T(8,128)}), f32[8,2,32,128]{3,2,1,0:T(8,128)S(1)}, u32[]{:S(2)}, u32[]{:S(2)}) %all-to-all-start.2) | async-done | bytes 262176 | tf_op jit(solution)/shard_map/all_to_all | solution.py:25
  68.4 1.8 %fusion.1 = f32[64,1024]{1,0:T(8,128)S(1)} fusion(bf16[128,1536]{1,0:T(8,128)(2,1)} %collective-permute-done.2, bf16[128,1536]{1,0:T(8,128)(2,1)} %collective-permute-done.1, bf16[128,1536]{1,0:T(8,128)(2,1)} %collective-permute-done, bf16[128,1536]{1,0:T(8,128)(2,1)S(1)} %constant_dynamic-update-slice_fusion, f32[64,128]{1,0:T(8,128)S(1)} %bitcast.111, ...), kind=kOutput, calls=%fused_computation.9 | convolution fusion | flops 406945792 | bytes 1966080 | tf_op jit(solution)/shard_map/dot_general | solution.py:141
  70.2 1.4 fusion.4
  71.7 1.1 copy.37
  72.7 4.2 %all-to-all-start.3 = ((f32[32,2,1536]{2,1,0:T(2,128)}), f32[32,2,1536]{2,1,0:T(2,128)S(1)}, u32[]{:S(2)}, u32[]{:S(2)}) async-start(f32[32,2,1536]{2,1,0:T(2,128)} %bitcast.84), calls=%async_computation.3 | async-start | bytes 786432 | tf_op jit(solution)/shard_map/all_to_all | solution.py:25
  77.6 1.8 %fusion = bf16[3072,256]{1,0:T(8,128)(2,1)S(1)} fusion(f32[3072,256]{1,0:T(8,128)S(1)} %fusion.29, bf16[3072,128]{1,0:T(8,128)(2,1)} %bitcast.41, s32[128]{0:T(128)S(1)} %get-tuple-element.40), kind=kOutput, calls=%fused_computation.2 | convolution fusion | flops 202932224 | bytes 5505536 | tf_op jit(solution)/shard_map/dot_general | solution.py:186
  79.5 12.7 %all-to-all-done.3 = f32[32,2,1536]{2,1,0:T(2,128)S(1)} async-done(((f32[32,2,1536]{2,1,0:T(2,128)}), f32[32,2,1536]{2,1,0:T(2,128)S(1)}, u32[]{:S(2)}, u32[]{:S(2)}) %all-to-all-start.3) | async-done | bytes 393248 | tf_op jit(solution)/shard_map/all_to_all | solution.py:25
  92.6 2.0 %collective-permute-start.6 = (f32[2,1536]{1,0:T(2,128)S(1)}, f32[2,1536]{1,0:T(2,128)S(1)}, u32[]{:S(2)}, u32[]{:S(2)}) collective-permute-start(f32[2,1536]{1,0:T(2,128)S(1)} %reduce_sum.36), channel_id=1, source_target_pairs={{0,4},{2,6},{4,0},{6,2},{1,5},{3,7},{5,1},{7,3},{8,12},{10,14},{12... | collective-permute-start | bytes 36872 | tf_op jit(solution)/shard_map/ppermute | solution.py:34
  99.5 1.3 fusion.55
  100.8 0.7 broadcast_in_dim.57
  101.5 6.1 %all-to-all-start.4 = ((bf16[8,2,1664]{2,1,0:T(2,128)(2,1)}), bf16[8,2,1664]{2,1,0:T(2,128)(2,1)S(1)}, u32[]{:S(2)}, u32[]{:S(2)}) async-start(bf16[8,2,1664]{2,1,0:T(2,128)(2,1)} %broadcast_in_dim.57), calls=%async_computation.4 | async-start | bytes 106496 | tf_op jit(solution)/shard_map/all_to_all | solution.py:25
  108.3 7.1 %all-to-all-done.4 = bf16[8,2,1664]{2,1,0:T(2,128)(2,1)S(1)} async-done(((bf16[8,2,1664]{2,1,0:T(2,128)(2,1)}), bf16[8,2,1664]{2,1,0:T(2,128)(2,1)S(1)}, u32[]{:S(2)}, u32[]{:S(2)}) %all-to-all-start.4) | async-done | bytes 53280 | tf_op jit(solution)/shard_map/all_to_all | solution.py:25
  115.4 1.0 broadcast_in_dim.58
  116.4 5.5 %all-to-all-start.5 = ((bf16[16,16,1664]{2,1,0:T(8,128)(2,1)}), bf16[16,16,1664]{2,1,0:T(8,128)(2,1)S(1)}, u32[]{:S(2)}, u32[]{:S(2)}) async-start(bf16[16,16,1664]{2,1,0:T(8,128)(2,1)} %broadcast_in_dim.58), calls=%async_computation.5 | async-start | bytes 1703936 | tf_op jit(solution)/shard_map/all_to_all | solution.py:25
  122.6 0.6 fusion.36
  123.2 9.5 %all-to-all-done.5 = bf16[16,16,1664]{2,1,0:T(8,128)(2,1)S(1)} async-done(((bf16[16,16,1664]{2,1,0:T(8,128)(2,1)}), bf16[16,16,1664]{2,1,0:T(8,128)(2,1)S(1)}, u32[]{:S(2)}, u32[]{:S(2)}) %all-to-all-start.5) | async-done | bytes 852000 | tf_op jit(solution)/shard_map/all_to_all | solution.py:25
  132.7 0.9 slice.125.half_ref
  134.3 5.8 %collective-permute-start.3 = (f32[1,1]{1,0:T(1,128)}, f32[1,1]{1,0:T(1,128)}, u32[]{:S(2)}, u32[]{:S(2)}) collective-permute-start(f32[1,1]{1,0:T(1,128)} %bitcast.37), channel_id=1, source_target_pairs={{0,1},{1,0},{2,3},{3,2},{4,5},{5,4},{6,7},{7,6},{8,9},{9,8},{10,11... | collective-permute-start | bytes 20 | tf_op jit(solution)/shard_map/ppermute | solution.py:34
  140.0 1.0 collective-permute-done.3
  142.4 0.9 multiply_subtract_fusion.1
  143.3 0.9 multiply_subtract_fusion
  144.2 8.7 %finish.1 = (bf16[2048,512]{1,0:T(8,128)(2,1)}, bf16[1024,1024]{1,0:T(8,128)(2,1)}) custom-call(f32[1,1]{1,0:T(1,128)} %bitcast.50.scale_ref, f32[32,128,512]{2,1,0:T(8,128)} %bitcast.85, bf16[32,96,256]{2,1,0:T(8,128)(2,1)} %bitcast.96, bf16[256,1536]{1,0:T(8,128)(2,1)} %slice.125.half_ref), custom_call_target="tpu_custom_call" | custom-call | tf_op jit(solution)/shard_map/finish/pallas_call | solution.py:67
  (74 shorter events, 7.6 us)
Async XLA Ops:
  7.2 40.2 %copy-start = (bf16[128,2048]{1,0:T(8,128)(2,1)S(1)}, bf16[128,2048]{1,0:T(8,128)(2,1)}, u32[]{:S(2)}) copy-start(bf16[128,2048]{1,0:T(8,128)(2,1)} %param.12) | copy-start | bytes 1572868
  7.2 27.3 %copy-start.6 = (bf16[128,512]{1,0:T(8,128)(2,1)S(1)}, bf16[128,512]{1,0:T(8,128)(2,1)}, u32[]{:S(2)}) copy-start(bf16[128,512]{1,0:T(8,128)(2,1)} %param.13) | copy-start | bytes 393220
  7.2 27.3 %copy-start.4 = (bf16[128,1024]{1,0:T(8,128)(2,1)S(1)}, bf16[128,1024]{1,0:T(8,128)(2,1)}, u32[]{:S(2)}) copy-start(bf16[128,1024]{1,0:T(8,128)(2,1)} %param.15) | copy-start | bytes 786436
  7.2 136.9 %all-gather.2.cloned.1.call-start = ((), (), s32[]{:S(2)}) async-start(), calls=%async_computation.6 | async-start | bytes 8650752 | tf_op jit(solution)/shard_map/all_gather | solution.py:109
  27.7 18.4 %all-to-all-start.1 = ((bf16[16,192,128]{2,1,0:T(8,128)(2,1)}), bf16[16,192,128]{2,1,0:T(8,128)(2,1)S(1)}, u32[]{:S(2)}, u32[]{:S(2)}) async-start(bf16[16,192,128]{2,1,0:T(8,128)(2,1)} %broadcast_in_dim.50), calls=%async_computation.1 | async-start | bytes 1572864 | tf_op jit(solution)/shard_map/all_to_all | solution.py:25
  34.6 33.9 %collective-permute-start.2 = (bf16[128,1536]{1,0:T(8,128)(2,1)S(1)}, bf16[128,1536]{1,0:T(8,128)(2,1)}, u32[]{:S(2)}, u32[]{:S(2)}) collective-permute-start(bf16[128,1536]{1,0:T(8,128)(2,1)S(1)} %constant_dynamic-update-slice_fusion), channel_id=1, source_target_pairs={{0,6},{2,0},{4,2},{6,4},{1,7},{3,1},{5,3},{7,5},{8,14},{10,8},{12,... | collective-permute-start | bytes 1179656 | tf_op jit(solution)/shard_map/ppermute | solution.py:34
  37.2 31.2 %collective-permute-start.1 = (bf16[128,1536]{1,0:T(8,128)(2,1)S(1)}, bf16[128,1536]{1,0:T(8,128)(2,1)}, u32[]{:S(2)}, u32[]{:S(2)}) collective-permute-start(bf16[128,1536]{1,0:T(8,128)(2,1)S(1)} %constant_dynamic-update-slice_fusion), channel_id=1, source_target_pairs={{0,4},{2,6},{4,0},{6,2},{1,5},{3,7},{5,1},{7,3},{8,12},{10,14},{12... | collective-permute-start | bytes 1179656 | tf_op jit(solution)/shard_map/ppermute | solution.py:34
  37.8 30.6 %collective-permute-start = (bf16[128,1536]{1,0:T(8,128)(2,1)S(1)}, bf16[128,1536]{1,0:T(8,128)(2,1)}, u32[]{:S(2)}, u32[]{:S(2)}) collective-permute-start(bf16[128,1536]{1,0:T(8,128)(2,1)S(1)} %constant_dynamic-update-slice_fusion), channel_id=1, source_target_pairs={{0,2},{2,4},{4,6},{6,0},{1,3},{3,5},{5,7},{7,1},{8,10},{10,12},{12... | collective-permute-start | bytes 1179656 | tf_op jit(solution)/shard_map/ppermute | solution.py:34
  46.2 1.0 copy-start.5
  48.4 19.9 %all-to-all-start.2 = ((f32[8,2,32,128]{3,2,1,0:T(8,128)}), f32[8,2,32,128]{3,2,1,0:T(8,128)S(1)}, u32[]{:S(2)}, u32[]{:S(2)}) async-start(f32[8,2,32,128]{3,2,1,0:T(8,128)} %bitcast.20), calls=%async_computation.2 | async-start | bytes 524288 | tf_op jit(solution)/shard_map/all_to_all | solution.py:25
  62.1 15.4 %collective-permute-start.4 = (bf16[32,96,128]{2,1,0:T(8,128)(2,1)S(1)}, bf16[32,96,128]{2,1,0:T(8,128)(2,1)}, u32[]{:S(2)}, u32[]{:S(2)}) collective-permute-start(bf16[32,96,128]{2,1,0:T(8,128)(2,1)S(1)} %bitcast.92), channel_id=1, source_target_pairs={{0,1},{1,0},{2,3},{3,2},{4,5},{5,4},{6,7},{7,6},{8,9},{9,8},{10,11... | collective-permute-start | bytes 2359304 | tf_op jit(solution)/shard_map/ppermute | solution.py:34
  72.7 19.4 %all-to-all-start.3 = ((f32[32,2,1536]{2,1,0:T(2,128)}), f32[32,2,1536]{2,1,0:T(2,128)S(1)}, u32[]{:S(2)}, u32[]{:S(2)}) async-start(f32[32,2,1536]{2,1,0:T(2,128)} %bitcast.84), calls=%async_computation.3 | async-start | bytes 786432 | tf_op jit(solution)/shard_map/all_to_all | solution.py:25
  77.6 17.0 %copy-start.9 = (f32[8,512]{1,0:T(8,128)S(1)}, f32[8,512]{1,0:T(8,128)}, u32[]{:S(2)}) copy-start(f32[8,512]{1,0:T(8,128)} %param.21) | copy-start | bytes 49156
  77.6 16.9 %copy-start.10 = (f32[8,512]{1,0:T(8,128)S(1)}, f32[8,512]{1,0:T(8,128)}, u32[]{:S(2)}) copy-start(f32[8,512]{1,0:T(8,128)} %param.20) | copy-start | bytes 49156
  77.6 17.6 %copy-start.7 = (f32[8,1024]{1,0:T(8,128)S(1)}, f32[8,1024]{1,0:T(8,128)}, u32[]{:S(2)}) copy-start(f32[8,1024]{1,0:T(8,128)} %param.23) | copy-start | bytes 98308
  77.6 17.6 %copy-start.8 = (f32[8,1024]{1,0:T(8,128)S(1)}, f32[8,1024]{1,0:T(8,128)}, u32[]{:S(2)}) copy-start(f32[8,1024]{1,0:T(8,128)} %param.22) | copy-start | bytes 98308
  79.5 63.8 %copy-start.1 = (bf16[3072,256]{1,0:T(8,128)(2,1)}, bf16[3072,256]{1,0:T(8,128)(2,1)S(1)}, u32[]{:S(2)}) copy-start(bf16[3072,256]{1,0:T(8,128)(2,1)S(1)} %fusion) | copy-start | bytes 4718596
  92.3 15.3 %collective-permute-start.7 = (f32[2,1536]{1,0:T(2,128)S(1)}, f32[2,1536]{1,0:T(2,128)S(1)}, u32[]{:S(2)}, u32[]{:S(2)}) collective-permute-start(f32[2,1536]{1,0:T(2,128)S(1)} %reduce_sum.36), channel_id=1, source_target_pairs={{0,6},{2,0},{4,2},{6,4},{1,7},{3,1},{5,3},{7,5},{8,14},{10,8},{12,... | collective-permute-start | bytes 36872 | tf_op jit(solution)/shard_map/ppermute | solution.py:34
  92.6 15.0 %collective-permute-start.6 = (f32[2,1536]{1,0:T(2,128)S(1)}, f32[2,1536]{1,0:T(2,128)S(1)}, u32[]{:S(2)}, u32[]{:S(2)}) collective-permute-start(f32[2,1536]{1,0:T(2,128)S(1)} %reduce_sum.36), channel_id=1, source_target_pairs={{0,4},{2,6},{4,0},{6,2},{1,5},{3,7},{5,1},{7,3},{8,12},{10,14},{12... | collective-permute-start | bytes 36872 | tf_op jit(solution)/shard_map/ppermute | solution.py:34
  94.5 13.1 %collective-permute-start.5 = (f32[2,1536]{1,0:T(2,128)S(1)}, f32[2,1536]{1,0:T(2,128)S(1)}, u32[]{:S(2)}, u32[]{:S(2)}) collective-permute-start(f32[2,1536]{1,0:T(2,128)S(1)} %reduce_sum.36), channel_id=1, source_target_pairs={{0,2},{2,4},{4,6},{6,0},{1,3},{3,5},{5,7},{7,1},{8,10},{10,12},{12... | collective-permute-start | bytes 36872 | tf_op jit(solution)/shard_map/ppermute | solution.py:34
  101.5 13.9 %all-to-all-start.4 = ((bf16[8,2,1664]{2,1,0:T(2,128)(2,1)}), bf16[8,2,1664]{2,1,0:T(2,128)(2,1)S(1)}, u32[]{:S(2)}, u32[]{:S(2)}) async-start(bf16[8,2,1664]{2,1,0:T(2,128)(2,1)} %broadcast_in_dim.57), calls=%async_computation.4 | async-start | bytes 106496 | tf_op jit(solution)/shard_map/all_to_all | solution.py:25
  115.4 27.0 %copy-start.3 = (f32[64,512]{1,0:T(8,128)S(1)}, f32[64,512]{1,0:T(8,128)}, u32[]{:S(2)}) copy-start(f32[64,512]{1,0:T(8,128)} %param.18) | copy-start | bytes 393220
  116.4 26.9 %copy-start.2 = (f32[32,1024]{1,0:T(8,128)S(1)}, f32[32,1024]{1,0:T(8,128)}, u32[]{:S(2)}) copy-start(f32[32,1024]{1,0:T(8,128)} %param.19) | copy-start | bytes 393220
  116.4 16.3 %all-to-all-start.5 = ((bf16[16,16,1664]{2,1,0:T(8,128)(2,1)}), bf16[16,16,1664]{2,1,0:T(8,128)(2,1)S(1)}, u32[]{:S(2)}, u32[]{:S(2)}) async-start(bf16[16,16,1664]{2,1,0:T(8,128)(2,1)} %broadcast_in_dim.58), calls=%async_computation.5 | async-start | bytes 1703936 | tf_op jit(solution)/shard_map/all_to_all | solution.py:25
  134.3 6.7 %collective-permute-start.3 = (f32[1,1]{1,0:T(1,128)}, f32[1,1]{1,0:T(1,128)}, u32[]{:S(2)}, u32[]{:S(2)}) collective-permute-start(f32[1,1]{1,0:T(1,128)} %bitcast.37), channel_id=1, source_target_pairs={{0,1},{1,0},{2,3},{3,2},{4,5},{5,4},{6,7},{7,6},{8,9},{9,8},{10,11... | collective-permute-start | bytes 20 | tf_op jit(solution)/shard_map/ppermute | solution.py:34
Sparse Core Ops, SparseCore 0:
  11.2 108.9 all-gather.1

commit v2 on v1

v2 whole, which is shorter than its diff:
```python
import jax
import jax.numpy as jnp
from jax import lax
from jax.experimental import pallas as pl
from jax.experimental.pallas import tpu as pltpu
from jax.sharding import Mesh, PartitionSpec as P

D = 2048
DA = 1024
RANK = 256
NZ, NX, NREP, NTP = 8, 4, 4, 2
FS = NZ * NX

beta_first = 0.9
beta_second = 0.95
adam_eps = 1e-08
mean_eps = 1e-06
learn_rate = 0.02

bf16 = jnp.bfloat16
f32 = jnp.float32


def exchange(pieces, axes):
    return lax.all_to_all(pieces, axes, split_axis=0, concat_axis=0, tiled=True)


def from_everyone(shard, axes, devices):
    return exchange(jnp.broadcast_to(shard, (devices, *shard.shape)), axes)


def shifted(array, axis, by):
    n = lax.axis_size(axis)
    return lax.ppermute(array, axis, [(i, (i + by) % n) for i in range(n)])


def one_hot(rows_of, columns, rows):
    r = lax.broadcasted_iota(jnp.int32, (rows, columns), 0)
    return (r == rows_of).astype(bf16)


def rank_of(core):
    k = lax.broadcasted_iota(jnp.int32, (1, RANK // NTP), 1)
    x, j, z = k // 32, (k // 8) % 4, k % 8
    return 8 * (4 * z + x) + 2 * j + core


VMEM = pl.BlockSpec(memory_space=pltpu.VMEM)
SMEM = pl.BlockSpec(memory_space=pltpu.SMEM)


def join_kernel(query_ref, output_ref, both_ref):
    both_ref[:64] = query_ref[...]
    both_ref[64:96] = output_ref[:, :512]
    both_ref[96:] = output_ref[:, 512:]


def join(query, output):
    return pl.pallas_call(
        join_kernel,
        in_specs=[VMEM, VMEM],
        out_specs=VMEM,
        out_shape=jax.ShapeDtypeStruct((128, 512), f32),
        name="join",
    )(query, output)


def project_kernel(factor_ref, inputs_ref, attended_ref, out_ref):
    factors_q = factor_ref[:, :64, :].reshape(D, 128)
    factors_o = factor_ref[:, 64:, :].reshape(DA, 128)
    for n, (left, right) in enumerate(((inputs_ref, factors_q), (attended_ref, factors_o))):
        red = jnp.dot(left[...], right, preferred_element_type=f32).T
        red = red.reshape(NX, NREP, NZ, 128)
        for j in range(NREP):
            mine = red[:, j].reshape(FS, 128)
            out_ref[j, 0, n] = mine
            out_ref[j, 1, n] = mine


def project(factors, inputs, attended):
    return pl.pallas_call(
        project_kernel,
        in_specs=[VMEM, VMEM, VMEM],
        out_specs=VMEM,
        out_shape=jax.ShapeDtypeStruct((NREP, NTP, 2, FS, 128), f32),
        name="project",
    )(factors, inputs, attended)


def partial_kernel(rep_ref, red_ref, c0_ref, c1_ref, c2_ref, c3_ref, out_ref):
    rep = rep_ref[0]
    totals = [None, None]
    for k, cot_ref in enumerate((c0_ref, c1_ref, c2_ref, c3_ref)):
        red = red_ref[lax.rem(rep + (NREP - k), NREP)]
        for n, (low, high) in enumerate(((0, 512), (512, 1536))):
            left = red[:, n].reshape(64, 128)
            first = left.astype(bf16)
            rest = left - first.astype(f32)
            second = rest.astype(bf16)
            third = (rest - second.astype(f32)).astype(bf16)
            terms = jnp.concatenate([first, second, third], axis=0)
            part = jnp.dot(terms, cot_ref[:, low:high], preferred_element_type=f32)
            totals[n] = part if totals[n] is None else totals[n] + part
    for n, (low, high) in enumerate(((0, 512), (512, 1536))):
        part = totals[n]
        part = part[:64] + (part[64:128] + part[128:])
        out_ref[:, 0, low:high] = part[:32]
        out_ref[:, 1, low:high] = part[32:]


def partial_sums(rep, red, cots):
    return pl.pallas_call(
        partial_kernel,
        in_specs=[SMEM] + [VMEM] * 5,
        out_specs=VMEM,
        out_shape=jax.ShapeDtypeStruct((FS, NTP, 1536), f32),
        name="partial_sums",
    )(rep, red, *cots)


def moments(low_sum, first, second):
    first_new = beta_first * first + (1.0 - beta_first) * low_sum
    second_new = beta_second * second + (1.0 - beta_second) * low_sum * low_sum
    return first_new, second_new


def own_rows(ref, rep):
    value = ref[...]
    rows = value[:2]
    for k in range(1, NREP):
        rows = jnp.where(rep == k, value[2 * k : 2 * k + 2], rows)
    return rows


def normed_kernel(rep_ref, part_ref, fq_ref, sq_ref, fo_ref, so_ref, low_ref, half_ref):
    rep = rep_ref[0]
    low = part_ref[0]
    for k in range(1, FS):
        low = low + part_ref[k]
    low_ref[...] = low
    pieces = []
    total = jnp.zeros((2, 1), f32)
    for low_sum, first_ref, second_ref in (
        (low[:, :512], fq_ref, sq_ref),
        (low[:, 512:], fo_ref, so_ref),
    ):
        first_new, second_new = moments(low_sum, own_rows(first_ref, rep), own_rows(second_ref, rep))
        normed = first_new / (jnp.sqrt(second_new) + adam_eps)
        total = total + jnp.sum(normed * normed, axis=1, keepdims=True)
        pieces.append(normed.astype(bf16))
    high = total.astype(bf16).astype(f32)
    middle = (total - high).astype(bf16).astype(f32)
    last = total - high - middle
    lane = lax.broadcasted_iota(jnp.int32, (2, 128), 1)
    sums = jnp.where(lane == 0, high, jnp.where(lane == 1, middle, jnp.where(lane == 2, last, 0.0)))
    payload = jnp.concatenate(pieces + [sums.astype(bf16)], axis=1)
    for k in range(NZ):
        half_ref[k] = payload


def normed_payload(rep, part, first_query, second_query, first_output, second_output):
    return pl.pallas_call(
        normed_kernel,
        in_specs=[SMEM] + [VMEM] * 5,
        out_specs=[VMEM, VMEM],
        out_shape=[
            jax.ShapeDtypeStruct((2, 1536), f32),
            jax.ShapeDtypeStruct((NZ, 2, 1664), bf16),
        ],
        name="normed_payload",
    )(rep, part, first_query, second_query, first_output, second_output)


def finish_kernel(
    mine_ref, other_ref, half_ref, rows_ref, wq_ref, wo_ref, w_ref, p_ref,
    copy_q_ref, copy_o_ref, step_q_ref, step_o_ref, new_q_ref, new_o_ref,
):
    total = jnp.full((1, 128), mine_ref[0, 0] + other_ref[0, 0], f32)
    scale = lax.rsqrt(total / (RANK * (DA + D)) + mean_eps)[:, :1]

    @pl.when(pl.program_id(0) == 0)
    def _():
        rows = rows_ref[...]
        uq = jnp.dot(rows[:64], half_ref[:, :512], preferred_element_type=f32)
        uo = jnp.dot(rows[64:], half_ref[:, 512:1536], preferred_element_type=f32)
        step_q = scale * uq
        step_o = scale * uo
        step_q_ref[...] = step_q
        step_o_ref[...] = step_o
        new_q_ref[...] = wq_ref[...] - learn_rate * step_q
        new_o_ref[...] = wo_ref[...] - learn_rate * step_o

    p = p_ref[...]
    n = p.shape[0]
    pq = p[:, :64, :].reshape(n * 64, RANK)
    po = p[:, 64:, :].reshape(n * 32, RANK)
    uq = jnp.dot(pq, half_ref[:, :512], preferred_element_type=f32)
    uo = jnp.dot(po, half_ref[:, 512:1536], preferred_element_type=f32)
    wq = w_ref[:, :64, :].reshape(n * 64, 512)
    copy_q_ref[...] = (wq - learn_rate * (scale * uq)).astype(bf16)
    w0 = w_ref[:, 64:96, :].reshape(n * 32, 512)
    w1 = w_ref[:, 96:, :].reshape(n * 32, 512)
    copy_o_ref[:, :512] = (w0 - learn_rate * (scale * uo[:, :512])).astype(bf16)
    copy_o_ref[:, 512:] = (w1 - learn_rate * (scale * uo[:, 512:])).astype(bf16)


def finish(mine, other, half, rows, weight_query, weight_output, weights, factors):
    step = 4
    def whole(shape):
        return pl.BlockSpec(shape, lambda i: (0,) * len(shape))

    return pl.pallas_call(
        finish_kernel,
        grid=(FS // step,),
        in_specs=[
            SMEM,
            SMEM,
            whole((RANK, 1664)),
            whole((96, RANK)),
            whole((64, 512)),
            whole((32, 1024)),
            pl.BlockSpec((step, 128, 512), lambda i: (i, 0, 0)),
            pl.BlockSpec((step, 96, RANK), lambda i: (i, 0, 0)),
        ],
        out_specs=[
            pl.BlockSpec((step * 64, 512), lambda i: (i, 0)),
            pl.BlockSpec((step * 32, 1024), lambda i: (i, 0)),
            whole((64, 512)),
            whole((32, 1024)),
            whole((64, 512)),
            whole((32, 1024)),
        ],
        out_shape=[
            jax.ShapeDtypeStruct((D, 512), bf16),
            jax.ShapeDtypeStruct((DA, 1024), bf16),
            jax.ShapeDtypeStruct((64, 512), f32),
            jax.ShapeDtypeStruct((32, 1024), f32),
            jax.ShapeDtypeStruct((64, 512), f32),
            jax.ShapeDtypeStruct((32, 1024), f32),
        ],
        name="finish",
    )(mine, other, half, rows, weight_query, weight_output, weights, factors)


def local(
    inputs,
    query_cot,
    attended,
    output_cot,
    proj_query,
    proj_output,
    weight_query,
    weight_output,
    first_query,
    second_query,
    first_output,
    second_output,
):
    z, x = lax.axis_index("z"), lax.axis_index("x")
    rep, core = lax.axis_index("rep"), lax.axis_index("tp")
    fs = z * NX + x

    here = rep.reshape(1)

    weights = join(weight_query, weight_output)
    weights = lax.all_gather(weights, ("z", "x"), axis=0, tiled=True)

    cots = jnp.concatenate([query_cot, output_cot], axis=1)
    cots = [cots, shifted(cots, "rep", 1), shifted(cots, "rep", 2), shifted(cots, "rep", 3)]

    both = jnp.concatenate([proj_query, proj_output], axis=0)
    mine = jnp.dot(both, one_hot(rank_of(core), 128, RANK), preferred_element_type=f32)
    factors = from_everyone(mine.astype(bf16).reshape(96, 128), ("z", "x"), FS)

    red = project(factors, inputs, attended).reshape(8, 2, FS, 128)
    red = exchange(red, ("rep", "tp")).reshape(NREP, NTP, 2, FS, 128)
    part = exchange(partial_sums(here, red, cots), ("x", "z"))
    low, half = normed_payload(
        here, part, first_query, second_query, first_output, second_output
    )
    half = exchange(half, "z")
    low, half = lax.optimization_barrier((low, half))
    low_rows = [low, shifted(low, "rep", 1), shifted(low, "rep", 2), shifted(low, "rep", 3)]
    half = from_everyone(half.reshape(16, 1664), ("x", "rep"), 16).reshape(RANK, 1664)
    total = jnp.sum(half[:, 1536:].astype(f32)).reshape(1, 1)
    other = shifted(total, "tp", 1)

    others = shifted(factors, "tp", 1)
    k = lax.broadcasted_iota(jnp.int32, (128, RANK), 0)
    c = lax.broadcasted_iota(jnp.int32, (128, RANK), 1)
    spread = (c == 2 * k + core).astype(bf16)
    spread_other = (c == 2 * k + 1 - core).astype(bf16)
    whole = jnp.dot(factors.reshape(FS * 96, 128), spread, preferred_element_type=f32)
    whole = whole + jnp.dot(others.reshape(FS * 96, 128), spread_other, preferred_element_type=f32)
    whole = whole.astype(bf16).reshape(FS, 96, RANK)
    rows = lax.dynamic_index_in_dim(whole, fs, 0, keepdims=False)

    copy_q, copy_o, step_q, step_o, new_q, new_o = finish(
        total, other, half, rows, weight_query, weight_output,
        weights.reshape(FS, 128, 512), whole,
    )

    rolled = jnp.stack(low_rows)
    order = (rep - jnp.arange(NREP)) % NREP
    low_all = jnp.take(rolled, order, axis=0).reshape(8, 1536)
    first_q, second_q = moments(low_all[:, :512], first_query, second_query)
    first_o, second_o = moments(low_all[:, 512:], first_output, second_output)
    return (new_q, new_o, step_q, step_o, first_q, second_q, first_o, second_o, copy_q, copy_o)


def solution(mesh):
    devices = mesh.devices.reshape(NZ, NX, NREP, NTP)
    grid = Mesh(devices, ("z", "x", "rep", "tp"))
    fs = ("z", "x")
    tokens = ("z", "x", "rep")
    return jax.shard_map(
        local,
        mesh=grid,
        in_specs=(
            P(tokens, None),
            P(tokens, "tp"),
            P(tokens, None),
            P(tokens, "tp"),
            P(fs, None),
            P(fs, None),
            P(fs, "tp"),
            P(fs, "tp"),
            P(fs, "tp"),
            P(fs, "tp"),
            P(fs, "tp"),
            P(fs, "tp"),
        ),
        out_specs=(
            P(fs, "tp"),
            P(fs, "tp"),
            P(fs, "tp"),
            P(fs, "tp"),
            P(fs, "tp"),
            P(fs, "tp"),
            P(fs, "tp"),
            P(fs, "tp"),
            P(None, "tp"),
            P(None, "tp"),
        ),
        check_vma=False,
    )
```

time: 161 us -> 153 us (0.950)
  blocking collectives: 15.9 us -> 0 us
  Pallas kernels: 8.69 us -> 19.4 us
  waiting for transfers between devices: 44 us -> 53.1 us
  between operations: 19.5 us -> 14.3 us
  matrix products: 8.89 us -> 5.67 us
  other arithmetic: 6.43 us -> 4.68 us
    all_to_all x1 -> x0, blocking collectives: 15.9 us -> none  [exchange(): return lax.all_to_all(pieces, axes, split_axis=0, concat_axis=0, tiled=True)]
    pallas_call x1 -> x5, Pallas kernels: 8.69 us -> 19.4 us  [the longest x1 10.4 us: finish(): pl.pallas_call(finish_kernel, grid=(FS // step,), in_specs=[SMEM, SMEM, w...]
    all_to_all x5, waiting for transfers between devices: 43 us -> 52.1 us  [exchange(): return lax.all_to_all(pieces, axes, split_axis=0, concat_axis=0, tiled=True)]
    dot_general x6 -> x0, matrix products: 5.51 us -> none  [the longest x1 1.77 us: local(): jnp.dot(left_o, right[:, 512:], precision=lax.Precision.HIGHEST, preferre...]
    slice x6 -> x0, local copies, waits for them, and re-layouts: 1.99 us -> none  [the longest x1 0.95 us: local(): weight_output[:, :512]]
    unnamed x23 -> x29, local copies, waits for them, and re-layouts: 0.45 us -> 2.36 us
    concatenate x3 -> x0, other arithmetic: 1.67 us -> none  [the longest x1 1.63 us: local(): jnp.concatenate([weight_query, weight_output[:, :512], weight_output[:, 5...]
  transfers between devices with their start and end apart: 14 -> 14, of which waited for: 6 -> 6; matrix products, arithmetic and copies ran while one was open for 13% -> 10% of each run, Pallas kernels for 0% -> 5%
where the time goes in v2:
time: 153 us; the launch traced here: 152 us
  waiting for transfers between devices  53.1 us (35%)
  starting transfers between devices  47.9 us (31%)
  Pallas kernels  19.4 us (13%)
  between operations  14.3 us (9%)
  local copies, waits for them, and re-layouts  7.2 us (5%)
  matrix products  5.67 us (4%)
  other arithmetic  4.68 us (3%)
    all_to_all x5, waiting for transfers between devices, exchange(): return lax.all_to_all(pieces, axes, split_axis=0, concat_axis=0, tiled=True)  52.1 us
    all_to_all x5, starting transfers between devices, exchange(): return lax.all_to_all(pieces, axes, split_axis=0, concat_axis=0, tiled=True)  34.5 us
    ppermute x8, starting transfers between devices, shifted(): return lax.ppermute(array, axis, [(i, (i + by) % n) for i in range(n)])  13.3 us
    pallas_call x1, Pallas kernels, finish(): pl.pallas_call(finish_kernel, grid=(FS // step,), in_specs=[SMEM, SMEM, w...  10.4 us
  transfers between devices with their start and end apart: 14, of which 6 were waited for; matrix products, arithmetic and copies ran while one was open for 10% of the time, Pallas kernels for 5%

profile of v2, /device:TPU:1, one launch (start us, length us, event | category | flops | bytes accessed | tf_op | source)
XLA Modules:
  0.0 152.2 jit_solution(9537935153824126765)
XLA Ops:
  7.2 1.7 %join.1 = f32[128,512]{1,0:T(8,128)} custom-call(f32[64,512]{1,0:T(8,128)} %wq_ref.1, f32[32,1024]{1,0:T(8,128)} %wo_ref.1), custom_call_target="tpu_custom_call" | custom-call | tf_op jit(solution)/shard_map/join/pallas_call | solution.py:59
  9.0 0.9 convolution_convert_fusion
  10.0 1.0 broadcast_in_dim.20
  10.9 11.9 %all-to-all-start = ((bf16[32,96,128]{2,1,0:T(8,128)(2,1)}), bf16[32,96,128]{2,1,0:T(8,128)(2,1)S(1)}, u32[]{:S(2)}, u32[]{:S(2)}) async-start(bf16[32,96,128]{2,1,0:T(8,128)(2,1)} %broadcast_in_dim.20), calls=%async_computation | async-start | bytes 1572864 | tf_op jit(solution)/shard_map/all_to_all | solution.py:25
  22.9 1.4 collective-permute-start
  24.3 2.6 %collective-permute-start.1 = (bf16[128,1536]{1,0:T(8,128)(2,1)S(1)}, bf16[128,1536]{1,0:T(8,128)(2,1)S(1)}, u32[]{:S(2)}, u32[]{:S(2)}) collective-permute-start(bf16[128,1536]{1,0:T(8,128)(2,1)S(1)} %constant_dynamic-update-slice_fusion.c0_ref), channel_id=1, source_target_pairs={{0,4},{2,6},{4,0},{6,2},{1,5},{3,7},{5,1},{7,3},{8,12},{10,14},{12... | collective-permute-start | bytes 1179656 | tf_op jit(solution)/shard_map/ppermute | solution.py:34
  26.9 1.1 collective-permute-start.2
  27.9 20.5 %all-to-all-done.factor_ref = bf16[32,96,128]{2,1,0:T(8,128)(2,1)S(1)} async-done(((bf16[32,96,128]{2,1,0:T(8,128)(2,1)}), bf16[32,96,128]{2,1,0:T(8,128)(2,1)S(1)}, u32[]{:S(2)}, u32[]{:S(2)}) %all-to-all-start) | async-done | bytes 786464 | tf_op jit(solution)/shard_map/all_to_all | solution.py:25
  48.5 0.9 copy-done
  49.3 2.5 %project.1 = f32[4,2,2,32,128]{4,3,2,1,0:T(8,128)} custom-call(bf16[32,96,128]{2,1,0:T(8,128)(2,1)} %copy-done, bf16[128,2048]{1,0:T(8,128)(2,1)} %inputs_ref.1, bf16[128,1024]{1,0:T(8,128)(2,1)} %attended_ref.1), custom_call_target="tpu_custom_call" | custom-call | tf_op jit(solution)/shard_map/project/pallas_call | solution.py:81
  51.8 8.6 %all-to-all-start.1 = ((f32[8,2,32,128]{3,2,1,0:T(8,128)}), f32[8,2,32,128]{3,2,1,0:T(8,128)S(1)}, u32[]{:S(2)}, u32[]{:S(2)}) async-start(f32[8,2,32,128]{3,2,1,0:T(8,128)} %bitcast.26), calls=%async_computation.1 | async-start | bytes 524288 | tf_op jit(solution)/shard_map/all_to_all | solution.py:25
  60.5 6.4 %all-to-all-done.1 = f32[8,2,32,128]{3,2,1,0:T(8,128)S(1)} async-done(((f32[8,2,32,128]{3,2,1,0:T(8,128)}), f32[8,2,32,128]{3,2,1,0:T(8,128)S(1)}, u32[]{:S(2)}, u32[]{:S(2)}) %all-to-all-start.1) | async-done | bytes 262176 | tf_op jit(solution)/shard_map/all_to_all | solution.py:25
  67.6 2.9 %partial_sums.1 = f32[32,2,1536]{2,1,0:T(2,128)} custom-call(s32[1]{0:T(128)} %bitcast.rep_ref, f32[4,2,2,32,128]{4,3,2,1,0:T(8,128)} %bitcast.25, bf16[128,1536]{1,0:T(8,128)(2,1)} %copy-done.4, bf16[128,1536]{1,0:T(8,128)(2,1)} %copy-done.5, bf16[128,1536]{1,0:T(8,128)(2,1)} %copy-done.6, bf16[128,1536]{1,0:T(8,128)(2,1)} %copy-done.7), custom_call_target="tpu_custom_call" | custom-call | tf_op jit(solution)/shard_map/partial_sums/pallas_call | solution.py:112
  70.5 4.0 %all-to-all-start.2 = ((f32[32,2,1536]{2,1,0:T(2,128)}), f32[32,2,1536]{2,1,0:T(2,128)S(1)}, u32[]{:S(2)}, u32[]{:S(2)}) async-start(f32[32,2,1536]{2,1,0:T(2,128)} %partial_sums.1), calls=%async_computation.2 | async-start | bytes 786432 | tf_op jit(solution)/shard_map/all_to_all | solution.py:25
  76.4 1.8 %fusion.1 = f32[3072,256]{1,0:T(8,128)S(1)} fusion(bf16[3072,128]{1,0:T(8,128)(2,1)} %bitcast.20, s32[128]{0:T(128)S(1)} %get-tuple-element.35), kind=kOutput, calls=%fused_computation.8 | convolution fusion | flops 201359360 | bytes 3932672 | tf_op jit(solution)/shard_map/dot_general | solution.py:293
  78.2 13.1 %all-to-all-done.2.part_ref = f32[32,2,1536]{2,1,0:T(2,128)S(1)} async-done(((f32[32,2,1536]{2,1,0:T(2,128)}), f32[32,2,1536]{2,1,0:T(2,128)S(1)}, u32[]{:S(2)}, u32[]{:S(2)}) %all-to-all-start.2) | async-done | bytes 393248 | tf_op jit(solution)/shard_map/all_to_all | solution.py:25
  91.3 0.7 copy-done.2
  92.1 1.8 %normed_payload.1 = (f32[2,1536]{1,0:T(2,128)}, bf16[8,2,1664]{2,1,0:T(2,128)(2,1)}) custom-call(s32[1]{0:T(128)} %bitcast.rep_ref, f32[32,2,1536]{2,1,0:T(2,128)} %copy-done.2, f32[8,512]{1,0:T(8,128)} %fq_ref.1, f32[8,512]{1,0:T(8,128)} %sq_ref.1, f32[8,1024]{1,0:T(8,128)} %fo_ref.1, f32[8,1024]{1,0:T(8,128)} %so_ref.1), custom_call_target="tpu_custom_call" | custom-call | tf_op jit(solution)/shard_map/normed_payload/pallas_call | solution.py:162
  93.9 4.8 %all-to-all-start.3 = ((bf16[8,2,1664]{2,1,0:T(2,128)(2,1)}), bf16[8,2,1664]{2,1,0:T(2,128)(2,1)S(1)}, u32[]{:S(2)}, u32[]{:S(2)}) async-start(bf16[8,2,1664]{2,1,0:T(2,128)(2,1)} %get-tuple-element.21), calls=%async_computation.3 | async-start | bytes 106496 | tf_op jit(solution)/shard_map/all_to_all | solution.py:25
  98.7 3.0 %fusion = bf16[3072,256]{1,0:T(8,128)(2,1)} fusion(f32[3072,256]{1,0:T(8,128)S(1)} %fusion.1, bf16[3072,128]{1,0:T(8,128)(2,1)} %bitcast.6, s32[128]{0:T(128)} %get-tuple-element.34), kind=kOutput, calls=%fused_computation.2 | convolution fusion | flops 202932224 | bytes 5505536 | tf_op jit(solution)/shard_map/dot_general | solution.py:294
  101.7 4.8 %all-to-all-done.3 = bf16[8,2,1664]{2,1,0:T(2,128)(2,1)S(1)} async-done(((bf16[8,2,1664]{2,1,0:T(2,128)(2,1)}), bf16[8,2,1664]{2,1,0:T(2,128)(2,1)S(1)}, u32[]{:S(2)}, u32[]{:S(2)}) %all-to-all-start.3) | async-done | bytes 53280 | tf_op jit(solution)/shard_map/all_to_all | solution.py:25
  106.6 1.8 %collective-permute-start.6 = (f32[2,1536]{1,0:T(2,128)}, f32[2,1536]{1,0:T(2,128)S(1)}, u32[]{:S(2)}, u32[]{:S(2)}) collective-permute-start(f32[2,1536]{1,0:T(2,128)} %get-tuple-element.27), channel_id=1, source_target_pairs={{0,4},{2,6},{4,0},{6,2},{1,5},{3,7},{5,1},{7,3},{8,12},{10,14},{12... | collective-permute-start | bytes 36872 | tf_op jit(solution)/shard_map/ppermute | solution.py:34
  108.4 0.9 collective-permute-start.7
  109.3 1.4 dynamic-slice_bitcast_fusion.rows_ref
  110.8 1.0 broadcast_in_dim.21
  111.7 5.2 %all-to-all-start.4 = ((bf16[16,16,1664]{2,1,0:T(8,128)(2,1)}), bf16[16,16,1664]{2,1,0:T(8,128)(2,1)S(1)}, u32[]{:S(2)}, u32[]{:S(2)}) async-start(bf16[16,16,1664]{2,1,0:T(8,128)(2,1)} %broadcast_in_dim.21), calls=%async_computation.4 | async-start | bytes 1703936 | tf_op jit(solution)/shard_map/all_to_all | solution.py:25
  117.0 0.7 pad_maximum_fusion
  120.5 7.3 %all-to-all-done.4 = bf16[16,16,1664]{2,1,0:T(8,128)(2,1)S(1)} async-done(((bf16[16,16,1664]{2,1,0:T(8,128)(2,1)}), bf16[16,16,1664]{2,1,0:T(8,128)(2,1)S(1)}, u32[]{:S(2)}, u32[]{:S(2)}) %all-to-all-start.4) | async-done | bytes 852000 | tf_op jit(solution)/shard_map/all_to_all | solution.py:25
  127.8 0.8 convert_reduce_fusion
  128.6 5.5 %collective-permute-start.3 = (f32[1,1]{1,0:T(1,128)}, f32[1,1]{1,0:T(1,128)}, u32[]{:S(2)}, u32[]{:S(2)}) collective-permute-start(f32[1,1]{1,0:T(1,128)} %bitcast.4.mine_ref), channel_id=1, source_target_pairs={{0,1},{1,0},{2,3},{3,2},{4,5},{5,4},{6,7},{7,6},{8,9},{9,8},{10,11... | collective-permute-start | bytes 20 | tf_op jit(solution)/shard_map/ppermute | solution.py:34
  134.1 0.9 collective-permute-done.3.other_ref
  135.0 10.4 %finish.1 = (bf16[2048,512]{1,0:T(8,128)(2,1)}, bf16[1024,1024]{1,0:T(8,128)(2,1)}, f32[64,512]{1,0:T(8,128)}, f32[32,1024]{1,0:T(8,128)}, f32[64,512]{1,0:T(8,128)}, /*index=5*/f32[32,1024]{1,0:T(8,128)}) custom-call(f32[1,1]{1,0:T(1,128)} %bitcast.4.mine_ref, f32[1,1]{1,0:T(1,128)} %collective-permute-done.3.other_ref, bf16[256,1664]{1,0:T(8,128)(2,1)} %bitcast.24, ...), custom_call_target="tpu_custom_call" | custom-call | tf_op jit(solution)/shard_map/finish/pallas_call | solution.py:212
  (53 shorter events, 5.5 us)
Async XLA Ops:
  7.2 15.6 %copy-start.11 = (bf16[128,512]{1,0:T(8,128)(2,1)S(1)}, bf16[128,512]{1,0:T(8,128)(2,1)}, u32[]{:S(2)}) copy-start(bf16[128,512]{1,0:T(8,128)(2,1)} %param.13) | copy-start | bytes 393220
  7.2 15.6 %copy-start.8 = (bf16[128,1024]{1,0:T(8,128)(2,1)S(1)}, bf16[128,1024]{1,0:T(8,128)(2,1)}, u32[]{:S(2)}) copy-start(bf16[128,1024]{1,0:T(8,128)(2,1)} %param.15) | copy-start | bytes 786436
  7.2 127.8 %all-gather.2.cloned.1.call-start = ((), (), s32[]{:S(2)}) async-start(), calls=%async_computation.5 | async-start | bytes 8650752 | tf_op jit(solution)/shard_map/all_gather | solution.py:266
  10.9 37.5 %all-to-all-start = ((bf16[32,96,128]{2,1,0:T(8,128)(2,1)}), bf16[32,96,128]{2,1,0:T(8,128)(2,1)S(1)}, u32[]{:S(2)}, u32[]{:S(2)}) async-start(bf16[32,96,128]{2,1,0:T(8,128)(2,1)} %broadcast_in_dim.20), calls=%async_computation | async-start | bytes 1572864 | tf_op jit(solution)/shard_map/all_to_all | solution.py:25
  22.9 44.0 %copy-start.4 = (bf16[128,1536]{1,0:T(8,128)(2,1)}, bf16[128,1536]{1,0:T(8,128)(2,1)S(1)}, u32[]{:S(2)}) copy-start(bf16[128,1536]{1,0:T(8,128)(2,1)S(1)} %constant_dynamic-update-slice_fusion.c0_ref) | copy-start | bytes 1179652
  22.9 37.6 %collective-permute-start = (bf16[128,1536]{1,0:T(8,128)(2,1)S(1)}, bf16[128,1536]{1,0:T(8,128)(2,1)S(1)}, u32[]{:S(2)}, u32[]{:S(2)}) collective-permute-start(bf16[128,1536]{1,0:T(8,128)(2,1)S(1)} %constant_dynamic-update-slice_fusion.c0_ref), channel_id=1, source_target_pairs={{0,2},{2,4},{4,6},{6,0},{1,3},{3,5},{5,7},{7,1},{8,10},{10,12},{12... | collective-permute-start | bytes 1179656 | tf_op jit(solution)/shard_map/ppermute | solution.py:34
  24.3 36.2 %collective-permute-start.1 = (bf16[128,1536]{1,0:T(8,128)(2,1)S(1)}, bf16[128,1536]{1,0:T(8,128)(2,1)S(1)}, u32[]{:S(2)}, u32[]{:S(2)}) collective-permute-start(bf16[128,1536]{1,0:T(8,128)(2,1)S(1)} %constant_dynamic-update-slice_fusion.c0_ref), channel_id=1, source_target_pairs={{0,4},{2,6},{4,0},{6,2},{1,5},{3,7},{5,1},{7,3},{8,12},{10,14},{12... | collective-permute-start | bytes 1179656 | tf_op jit(solution)/shard_map/ppermute | solution.py:34
  26.9 33.6 %collective-permute-start.2 = (bf16[128,1536]{1,0:T(8,128)(2,1)S(1)}, bf16[128,1536]{1,0:T(8,128)(2,1)S(1)}, u32[]{:S(2)}, u32[]{:S(2)}) collective-permute-start(bf16[128,1536]{1,0:T(8,128)(2,1)S(1)} %constant_dynamic-update-slice_fusion.c0_ref), channel_id=1, source_target_pairs={{0,6},{2,0},{4,2},{6,4},{1,7},{3,1},{5,3},{7,5},{8,14},{10,8},{12,... | collective-permute-start | bytes 1179656 | tf_op jit(solution)/shard_map/ppermute | solution.py:34
  48.5 0.9 copy-start
  51.8 15.1 %all-to-all-start.1 = ((f32[8,2,32,128]{3,2,1,0:T(8,128)}), f32[8,2,32,128]{3,2,1,0:T(8,128)S(1)}, u32[]{:S(2)}, u32[]{:S(2)}) async-start(f32[8,2,32,128]{3,2,1,0:T(8,128)} %bitcast.26), calls=%async_computation.1 | async-start | bytes 524288 | tf_op jit(solution)/shard_map/all_to_all | solution.py:25
  60.4 38.3 %collective-permute-start.4 = (bf16[32,96,128]{2,1,0:T(8,128)(2,1)}, bf16[32,96,128]{2,1,0:T(8,128)(2,1)}, u32[]{:S(2)}, u32[]{:S(2)}) collective-permute-start(bf16[32,96,128]{2,1,0:T(8,128)(2,1)} %copy-done), channel_id=1, source_target_pairs={{0,1},{1,0},{2,3},{3,2},{4,5},{5,4},{6,7},{7,6},{8,9},{9,8},{10,11... | collective-permute-start | bytes 2359304 | tf_op jit(solution)/shard_map/ppermute | solution.py:34
  60.4 6.5 %copy-start.5 = (bf16[128,1536]{1,0:T(8,128)(2,1)}, bf16[128,1536]{1,0:T(8,128)(2,1)S(1)}, u32[]{:S(2)}) copy-start(bf16[128,1536]{1,0:T(8,128)(2,1)S(1)} %collective-permute-done.c1_ref) | copy-start | bytes 1179652
  60.5 6.5 %copy-start.6 = (bf16[128,1536]{1,0:T(8,128)(2,1)}, bf16[128,1536]{1,0:T(8,128)(2,1)S(1)}, u32[]{:S(2)}) copy-start(bf16[128,1536]{1,0:T(8,128)(2,1)S(1)} %collective-permute-done.1.c2_ref) | copy-start | bytes 1179652
  60.5 6.4 %copy-start.7 = (bf16[128,1536]{1,0:T(8,128)(2,1)}, bf16[128,1536]{1,0:T(8,128)(2,1)S(1)}, u32[]{:S(2)}) copy-start(bf16[128,1536]{1,0:T(8,128)(2,1)S(1)} %collective-permute-done.2.c3_ref) | copy-start | bytes 1179652
  66.9 0.7 copy-start.3
  70.5 20.8 %all-to-all-start.2 = ((f32[32,2,1536]{2,1,0:T(2,128)}), f32[32,2,1536]{2,1,0:T(2,128)S(1)}, u32[]{:S(2)}, u32[]{:S(2)}) async-start(f32[32,2,1536]{2,1,0:T(2,128)} %partial_sums.1), calls=%async_computation.2 | async-start | bytes 786432 | tf_op jit(solution)/shard_map/all_to_all | solution.py:25
  91.3 0.7 copy-start.2
  93.9 12.6 %all-to-all-start.3 = ((bf16[8,2,1664]{2,1,0:T(2,128)(2,1)}), bf16[8,2,1664]{2,1,0:T(2,128)(2,1)S(1)}, u32[]{:S(2)}, u32[]{:S(2)}) async-start(bf16[8,2,1664]{2,1,0:T(2,128)(2,1)} %get-tuple-element.21), calls=%async_computation.3 | async-start | bytes 106496 | tf_op jit(solution)/shard_map/all_to_all | solution.py:25
  98.7 20.5 %copy-start.12 = (f32[8,512]{1,0:T(8,128)S(1)}, f32[8,512]{1,0:T(8,128)}, u32[]{:S(2)}) copy-start(f32[8,512]{1,0:T(8,128)} %fq_ref.1) | copy-start | bytes 49156
  101.7 17.6 %copy-start.13 = (f32[8,512]{1,0:T(8,128)S(1)}, f32[8,512]{1,0:T(8,128)}, u32[]{:S(2)}) copy-start(f32[8,512]{1,0:T(8,128)} %sq_ref.1) | copy-start | bytes 49156
  101.7 18.2 %copy-start.9 = (f32[8,1024]{1,0:T(8,128)S(1)}, f32[8,1024]{1,0:T(8,128)}, u32[]{:S(2)}) copy-start(f32[8,1024]{1,0:T(8,128)} %fo_ref.1) | copy-start | bytes 98308
  101.7 18.2 %copy-start.10 = (f32[8,1024]{1,0:T(8,128)S(1)}, f32[8,1024]{1,0:T(8,128)}, u32[]{:S(2)}) copy-start(f32[8,1024]{1,0:T(8,128)} %so_ref.1) | copy-start | bytes 98308
  106.5 10.4 %collective-permute-start.5 = (f32[2,1536]{1,0:T(2,128)}, f32[2,1536]{1,0:T(2,128)S(1)}, u32[]{:S(2)}, u32[]{:S(2)}) collective-permute-start(f32[2,1536]{1,0:T(2,128)} %get-tuple-element.27), channel_id=1, source_target_pairs={{0,2},{2,4},{4,6},{6,0},{1,3},{3,5},{5,7},{7,1},{8,10},{10,12},{12... | collective-permute-start | bytes 36872 | tf_op jit(solution)/shard_map/ppermute | solution.py:34
  106.6 10.4 %collective-permute-start.6 = (f32[2,1536]{1,0:T(2,128)}, f32[2,1536]{1,0:T(2,128)S(1)}, u32[]{:S(2)}, u32[]{:S(2)}) collective-permute-start(f32[2,1536]{1,0:T(2,128)} %get-tuple-element.27), channel_id=1, source_target_pairs={{0,4},{2,6},{4,0},{6,2},{1,5},{3,7},{5,1},{7,3},{8,12},{10,14},{12... | collective-permute-start | bytes 36872 | tf_op jit(solution)/shard_map/ppermute | solution.py:34
  108.4 8.6 %collective-permute-start.7 = (f32[2,1536]{1,0:T(2,128)}, f32[2,1536]{1,0:T(2,128)S(1)}, u32[]{:S(2)}, u32[]{:S(2)}) collective-permute-start(f32[2,1536]{1,0:T(2,128)} %get-tuple-element.27), channel_id=1, source_target_pairs={{0,6},{2,0},{4,2},{6,4},{1,7},{3,1},{5,3},{7,5},{8,14},{10,8},{12,... | collective-permute-start | bytes 36872 | tf_op jit(solution)/shard_map/ppermute | solution.py:34
  111.7 16.0 %all-to-all-start.4 = ((bf16[16,16,1664]{2,1,0:T(8,128)(2,1)}), bf16[16,16,1664]{2,1,0:T(8,128)(2,1)S(1)}, u32[]{:S(2)}, u32[]{:S(2)}) async-start(bf16[16,16,1664]{2,1,0:T(8,128)(2,1)} %broadcast_in_dim.21), calls=%async_computation.4 | async-start | bytes 1703936 | tf_op jit(solution)/shard_map/all_to_all | solution.py:25
  127.8 7.2 %copy-start.1 = (bf16[16,16,1664]{2,1,0:T(8,128)(2,1)}, bf16[16,16,1664]{2,1,0:T(8,128)(2,1)S(1)}, u32[]{:S(2)}) copy-start(bf16[16,16,1664]{2,1,0:T(8,128)(2,1)S(1)} %all-to-all-done.4) | copy-start | bytes 2555908
  128.6 6.4 %collective-permute-start.3 = (f32[1,1]{1,0:T(1,128)}, f32[1,1]{1,0:T(1,128)}, u32[]{:S(2)}, u32[]{:S(2)}) collective-permute-start(f32[1,1]{1,0:T(1,128)} %bitcast.4.mine_ref), channel_id=1, source_target_pairs={{0,1},{1,0},{2,3},{3,2},{4,5},{5,4},{6,7},{7,6},{8,9},{9,8},{10,11... | collective-permute-start | bytes 20 | tf_op jit(solution)/shard_map/ppermute | solution.py:34
Sparse Core Ops, SparseCore 0:
  10.6 112.2 all-gather.1

commit v3 on v2

--- a/solution.py
+++ b/solution.py
@@ -5,6 +5,7 @@
 from jax.experimental.pallas import tpu as pltpu
 from jax.sharding import Mesh, PartitionSpec as P
 
+
 D = 2048
 DA = 1024
 RANK = 256
@@ -46,6 +47,12 @@
 
 
 VMEM = pl.BlockSpec(memory_space=pltpu.VMEM)
+
+
+def near(array):
+    return pltpu.with_memory_space_constraint(array, pltpu.VMEM)
+
+
 SMEM = pl.BlockSpec(memory_space=pltpu.SMEM)
 
 
@@ -82,24 +89,26 @@
         project_kernel,
         in_specs=[VMEM, VMEM, VMEM],
         out_specs=VMEM,
-        out_shape=jax.ShapeDtypeStruct((NREP, NTP, 2, FS, 128), f32),
+        out_shape=pltpu.VMEM((NREP, NTP, 2, FS, 128), f32),
         name="project",
-    )(factors, inputs, attended)
-
-
-def partial_kernel(rep_ref, red_ref, c0_ref, c1_ref, c2_ref, c3_ref, out_ref):
+    )(near(factors), near(inputs), near(attended))
+
+
+def partial_kernel(rep_ref, red_ref, query_ref, output_ref, c1_ref, c2_ref, c3_ref, out_ref):
     rep = rep_ref[0]
     totals = [None, None]
-    for k, cot_ref in enumerate((c0_ref, c1_ref, c2_ref, c3_ref)):
+    own = (query_ref[...], output_ref[...])
+    sent = [(c[:, :512], c[:, 512:]) for c in (c1_ref, c2_ref, c3_ref)]
+    for k, cots in enumerate([own] + sent):
         red = red_ref[lax.rem(rep + (NREP - k), NREP)]
-        for n, (low, high) in enumerate(((0, 512), (512, 1536))):
+        for n in range(2):
             left = red[:, n].reshape(64, 128)
             first = left.astype(bf16)
             rest = left - first.astype(f32)
             second = rest.astype(bf16)
             third = (rest - second.astype(f32)).astype(bf16)
             terms = jnp.concatenate([first, second, third], axis=0)
-            part = jnp.dot(terms, cot_ref[:, low:high], preferred_element_type=f32)
+            part = jnp.dot(terms, cots[n], preferred_element_type=f32)
             totals[n] = part if totals[n] is None else totals[n] + part
     for n, (low, high) in enumerate(((0, 512), (512, 1536))):
         part = totals[n]
@@ -111,11 +120,11 @@
 def partial_sums(rep, red, cots):
     return pl.pallas_call(
         partial_kernel,
-        in_specs=[SMEM] + [VMEM] * 5,
+        in_specs=[SMEM] + [VMEM] * 6,
         out_specs=VMEM,
-        out_shape=jax.ShapeDtypeStruct((FS, NTP, 1536), f32),
+        out_shape=pltpu.VMEM((FS, NTP, 1536), f32),
         name="partial_sums",
-    )(rep, red, *cots)
+    )(rep, near(red), *[near(c) for c in cots])
 
 
 def moments(low_sum, first, second):
@@ -164,11 +173,11 @@
         in_specs=[SMEM] + [VMEM] * 5,
         out_specs=[VMEM, VMEM],
         out_shape=[
-            jax.ShapeDtypeStruct((2, 1536), f32),
-            jax.ShapeDtypeStruct((NZ, 2, 1664), bf16),
+            pltpu.VMEM((2, 1536), f32),
+            pltpu.VMEM((NZ, 2, 1664), bf16),
         ],
         name="normed_payload",
-    )(rep, part, first_query, second_query, first_output, second_output)
+    )(rep, *[near(a) for a in (part, first_query, second_query, first_output, second_output)])
 
 
 def finish_kernel(
@@ -205,7 +214,8 @@
 
 
 def finish(mine, other, half, rows, weight_query, weight_output, weights, factors):
-    step = 4
+    step = 8
+
     def whole(shape):
         return pl.BlockSpec(shape, lambda i: (0,) * len(shape))
 
@@ -266,7 +276,7 @@
     weights = lax.all_gather(weights, ("z", "x"), axis=0, tiled=True)
 
     cots = jnp.concatenate([query_cot, output_cot], axis=1)
-    cots = [cots, shifted(cots, "rep", 1), shifted(cots, "rep", 2), shifted(cots, "rep", 3)]
+    cots = [shifted(cots, "rep", 1), shifted(cots, "rep", 2), shifted(cots, "rep", 3)]
 
     both = jnp.concatenate([proj_query, proj_output], axis=0)
     mine = jnp.dot(both, one_hot(rank_of(core), 128, RANK), preferred_element_type=f32)
@@ -274,7 +284,7 @@
 
     red = project(factors, inputs, attended).reshape(8, 2, FS, 128)
     red = exchange(red, ("rep", "tp")).reshape(NREP, NTP, 2, FS, 128)
-    part = exchange(partial_sums(here, red, cots), ("x", "z"))
+    part = exchange(partial_sums(here, red, [query_cot, output_cot] + cots), ("x", "z"))
     low, half = normed_payload(
         here, part, first_query, second_query, first_output, second_output
     )

time: 153 us -> 146 us (0.954)
  Pallas kernels: 19.4 us -> 14.6 us
  other arithmetic: 4.68 us -> 2.18 us
  local copies, waits for them, and re-layouts: 7.2 us -> 5.2 us
  waiting for transfers between devices: 53.1 us -> 55.1 us
    pallas_call x1, Pallas kernels: 10.4 us -> 8.37 us  [finish(): pl.pallas_call(finish_kernel, grid=(FS // step,), in_specs=[SMEM, SMEM, w...]
    all_to_all x5, waiting for transfers between devices: 52.1 us -> 54.2 us  [exchange(): return lax.all_to_all(pieces, axes, split_axis=0, concat_axis=0, tiled=True)]
  transfers between devices with their start and end apart: 14 -> 14, of which waited for: 6 -> 6; matrix products, arithmetic and copies ran while one was open for 10% -> 8% of each run, Pallas kernels for 5% -> 3%
where the time goes in v3:
time: 146 us; the launch traced here: 145 us
  waiting for transfers between devices  55.1 us (38%)
  starting transfers between devices  47.9 us (33%)
  Pallas kernels  14.6 us (10%)
  between operations  14.3 us (10%)
  matrix products  6.08 us (4%)
  local copies, waits for them, and re-layouts  5.2 us (4%)
  other arithmetic  2.18 us (1%)
    all_to_all x5, waiting for transfers between devices, exchange(): return lax.all_to_all(pieces, axes, split_axis=0, concat_axis=0, tiled=True)  54.2 us
    all_to_all x5, starting transfers between devices, exchange(): return lax.all_to_all(pieces, axes, split_axis=0, concat_axis=0, tiled=True)  34.7 us
    ppermute x8, starting transfers between devices, shifted(): return lax.ppermute(array, axis, [(i, (i + by) % n) for i in range(n)])  13.2 us
    pallas_call x1, Pallas kernels, finish(): pl.pallas_call(finish_kernel, grid=(FS // step,), in_specs=[SMEM, SMEM, w...  8.37 us
  transfers between devices with their start and end apart: 14, of which 6 were waited for; matrix products, arithmetic and copies ran while one was open for 8% of the time, Pallas kernels for 3%

profile of v3, /device:TPU:1, one launch (start us, length us, event | category | flops | bytes accessed | tf_op | source)
XLA Modules:
  0.0 145.3 jit_solution(8682747078976575276)
XLA Ops:
  7.3 1.8 %join.1 = f32[128,512]{1,0:T(8,128)} custom-call(f32[64,512]{1,0:T(8,128)} %wq_ref.1, f32[32,1024]{1,0:T(8,128)} %wo_ref.1), custom_call_target="tpu_custom_call" | custom-call | tf_op jit(solution)/shard_map/join/pallas_call | solution.py:66
  9.1 0.9 convolution_convert_fusion
  10.0 1.0 broadcast_in_dim.20
  11.0 11.9 %all-to-all-start = ((bf16[32,96,128]{2,1,0:T(8,128)(2,1)}), bf16[32,96,128]{2,1,0:T(8,128)(2,1)S(1)}, u32[]{:S(2)}, u32[]{:S(2)}) async-start(bf16[32,96,128]{2,1,0:T(8,128)(2,1)} %broadcast_in_dim.20), calls=%async_computation | async-start | bytes 1572864 | tf_op jit(solution)/shard_map/all_to_all | solution.py:26
  22.9 1.4 collective-permute-start
  24.3 2.6 %collective-permute-start.1 = (bf16[128,1536]{1,0:T(8,128)(2,1)S(1)}, bf16[128,1536]{1,0:T(8,128)(2,1)S(1)}, u32[]{:S(2)}, u32[]{:S(2)}) collective-permute-start(bf16[128,1536]{1,0:T(8,128)(2,1)S(1)} %constant_dynamic-update-slice_fusion), channel_id=1, source_target_pairs={{0,4},{2,6},{4,0},{6,2},{1,5},{3,7},{5,1},{7,3},{8,12},{10,14},{12... | collective-permute-start | bytes 1179656 | tf_op jit(solution)/shard_map/ppermute | solution.py:35
  26.9 1.1 collective-permute-start.2
  28.0 20.6 %all-to-all-done.factor_ref = bf16[32,96,128]{2,1,0:T(8,128)(2,1)S(1)} async-done(((bf16[32,96,128]{2,1,0:T(8,128)(2,1)}), bf16[32,96,128]{2,1,0:T(8,128)(2,1)S(1)}, u32[]{:S(2)}, u32[]{:S(2)}) %all-to-all-start) | async-done | bytes 786464 | tf_op jit(solution)/shard_map/all_to_all | solution.py:26
  48.6 1.1 project.1
  49.7 8.5 %all-to-all-start.1 = ((f32[8,2,32,128]{3,2,1,0:T(8,128)}), f32[8,2,32,128]{3,2,1,0:T(8,128)S(1)}, u32[]{:S(2)}, u32[]{:S(2)}) async-start(f32[8,2,32,128]{3,2,1,0:T(8,128)} %bitcast.1), calls=%async_computation.1 | async-start | bytes 524288 | tf_op jit(solution)/shard_map/all_to_all | solution.py:26
  58.3 0.7 copy-done.3
  59.0 5.7 %all-to-all-done.1 = f32[8,2,32,128]{3,2,1,0:T(8,128)S(1)} async-done(((f32[8,2,32,128]{3,2,1,0:T(8,128)}), f32[8,2,32,128]{3,2,1,0:T(8,128)S(1)}, u32[]{:S(2)}, u32[]{:S(2)}) %all-to-all-start.1) | async-done | bytes 262176 | tf_op jit(solution)/shard_map/all_to_all | solution.py:26
  64.7 1.0 copy-done.4
  65.7 2.5 %partial_sums.1 = f32[32,2,1536]{2,1,0:T(2,128)} custom-call(s32[1]{0:T(128)} %bitcast.rep_ref, f32[4,2,2,32,128]{4,3,2,1,0:T(8,128)S(1)} %bitcast.20, bf16[128,512]{1,0:T(8,128)(2,1)S(1)} %copy-done.2, bf16[128,1024]{1,0:T(8,128)(2,1)S(1)} %copy-done, bf16[128,1536]{1,0:T(8,128)(2,1)S(1)} %copy-done.4, bf16[128,1536]{1,0:T(8,128)(2,1)S(1)} %collective-permute-done.1.c2_ref, ...), custom_call_target="tpu_custom_call" | custom-call | tf_op jit(solution)/shard_map/partial_sums/pallas_call | solution.py:121
  68.3 4.1 %all-to-all-start.2 = ((f32[32,2,1536]{2,1,0:T(2,128)}), f32[32,2,1536]{2,1,0:T(2,128)S(1)}, u32[]{:S(2)}, u32[]{:S(2)}) async-start(f32[32,2,1536]{2,1,0:T(2,128)} %partial_sums.1), calls=%async_computation.2 | async-start | bytes 786432 | tf_op jit(solution)/shard_map/all_to_all | solution.py:26
  72.6 2.3 %fusion.1 = f32[3072,256]{1,0:T(8,128)} fusion(bf16[3072,128]{1,0:T(8,128)(2,1)S(1)} %bitcast.19, s32[128]{0:T(128)S(1)} %get-tuple-element.35), kind=kOutput, calls=%fused_computation.8 | convolution fusion | flops 201359360 | bytes 3932672 | tf_op jit(solution)/shard_map/dot_general | solution.py:303
  74.8 14.2 %all-to-all-done.2.part_ref = f32[32,2,1536]{2,1,0:T(2,128)S(1)} async-done(((f32[32,2,1536]{2,1,0:T(2,128)}), f32[32,2,1536]{2,1,0:T(2,128)S(1)}, u32[]{:S(2)}, u32[]{:S(2)}) %all-to-all-start.2) | async-done | bytes 393248 | tf_op jit(solution)/shard_map/all_to_all | solution.py:26
  89.1 0.8 normed_payload.1
  89.9 4.6 %all-to-all-start.3 = ((bf16[8,2,1664]{2,1,0:T(2,128)(2,1)}), bf16[8,2,1664]{2,1,0:T(2,128)(2,1)S(1)}, u32[]{:S(2)}, u32[]{:S(2)}) async-start(bf16[8,2,1664]{2,1,0:T(2,128)(2,1)} %get-tuple-element.21), calls=%async_computation.3 | async-start | bytes 106496 | tf_op jit(solution)/shard_map/all_to_all | solution.py:26
  94.5 2.9 %fusion = bf16[3072,256]{1,0:T(8,128)(2,1)S(1)} fusion(f32[3072,256]{1,0:T(8,128)} %fusion.1, bf16[3072,128]{1,0:T(8,128)(2,1)} %bitcast.6, s32[128]{0:T(128)S(1)} %get-tuple-element.34), kind=kOutput, calls=%fused_computation.2 | convolution fusion | flops 202932224 | bytes 5505536 | tf_op jit(solution)/shard_map/dot_general | solution.py:304
  97.4 4.9 %all-to-all-done.3 = bf16[8,2,1664]{2,1,0:T(2,128)(2,1)S(1)} async-done(((bf16[8,2,1664]{2,1,0:T(2,128)(2,1)}), bf16[8,2,1664]{2,1,0:T(2,128)(2,1)S(1)}, u32[]{:S(2)}, u32[]{:S(2)}) %all-to-all-start.3) | async-done | bytes 53280 | tf_op jit(solution)/shard_map/all_to_all | solution.py:26
  102.5 1.5 %collective-permute-start.6 = (f32[2,1536]{1,0:T(2,128)S(1)}, f32[2,1536]{1,0:T(2,128)S(1)}, u32[]{:S(2)}, u32[]{:S(2)}) collective-permute-start(f32[2,1536]{1,0:T(2,128)S(1)} %get-tuple-element.27), channel_id=1, source_target_pairs={{0,4},{2,6},{4,0},{6,2},{1,5},{3,7},{5,1},{7,3},{8,12},{10,14},{12... | collective-permute-start | bytes 36872 | tf_op jit(solution)/shard_map/ppermute | solution.py:35
  104.0 1.0 collective-permute-start.7
  105.0 0.6 dynamic-slice_bitcast_fusion.rows_ref
  105.7 1.0 broadcast_in_dim.21
  106.6 5.6 %all-to-all-start.4 = ((bf16[16,16,1664]{2,1,0:T(8,128)(2,1)}), bf16[16,16,1664]{2,1,0:T(8,128)(2,1)S(1)}, u32[]{:S(2)}, u32[]{:S(2)}) async-start(bf16[16,16,1664]{2,1,0:T(8,128)(2,1)} %broadcast_in_dim.21), calls=%async_computation.4 | async-start | bytes 1703936 | tf_op jit(solution)/shard_map/all_to_all | solution.py:26
  113.6 0.6 fusion.8
  114.2 8.8 %all-to-all-done.4 = bf16[16,16,1664]{2,1,0:T(8,128)(2,1)S(1)} async-done(((bf16[16,16,1664]{2,1,0:T(8,128)(2,1)}), bf16[16,16,1664]{2,1,0:T(8,128)(2,1)S(1)}, u32[]{:S(2)}, u32[]{:S(2)}) %all-to-all-start.4) | async-done | bytes 852000 | tf_op jit(solution)/shard_map/all_to_all | solution.py:26
  123.0 0.8 convert_reduce_fusion
  123.8 5.5 %collective-permute-start.3 = (f32[1,1]{1,0:T(1,128)}, f32[1,1]{1,0:T(1,128)}, u32[]{:S(2)}, u32[]{:S(2)}) collective-permute-start(f32[1,1]{1,0:T(1,128)} %bitcast.4.mine_ref), channel_id=1, source_target_pairs={{0,1},{1,0},{2,3},{3,2},{4,5},{5,4},{6,7},{7,6},{8,9},{9,8},{10,11... | collective-permute-start | bytes 20 | tf_op jit(solution)/shard_map/ppermute | solution.py:35
  129.2 0.9 collective-permute-done.3.other_ref
  130.1 8.4 %finish.1 = (bf16[2048,512]{1,0:T(8,128)(2,1)}, bf16[1024,1024]{1,0:T(8,128)(2,1)}, f32[64,512]{1,0:T(8,128)}, f32[32,1024]{1,0:T(8,128)}, f32[64,512]{1,0:T(8,128)}, /*index=5*/f32[32,1024]{1,0:T(8,128)}) custom-call(f32[1,1]{1,0:T(1,128)} %bitcast.4.mine_ref, f32[1,1]{1,0:T(1,128)} %collective-permute-done.3.other_ref, bf16[256,1664]{1,0:T(8,128)(2,1)} %bitcast.26, ...), custom_call_target="tpu_custom_call" | custom-call | tf_op jit(solution)/shard_map/finish/pallas_call | solution.py:222
  (49 shorter events, 1.9 us)
Async XLA Ops:
  7.2 15.7 %copy-start.2 = (bf16[128,512]{1,0:T(8,128)(2,1)S(1)}, bf16[128,512]{1,0:T(8,128)(2,1)}, u32[]{:S(2)}) copy-start(bf16[128,512]{1,0:T(8,128)(2,1)} %query_ref.2) | copy-start | bytes 393220
  7.2 15.7 %copy-start = (bf16[128,1024]{1,0:T(8,128)(2,1)S(1)}, bf16[128,1024]{1,0:T(8,128)(2,1)}, u32[]{:S(2)}) copy-start(bf16[128,1024]{1,0:T(8,128)(2,1)} %output_ref.2) | copy-start | bytes 786436
  7.2 41.4 %copy-start.1 = (bf16[128,2048]{1,0:T(8,128)(2,1)S(1)}, bf16[128,2048]{1,0:T(8,128)(2,1)}, u32[]{:S(2)}) copy-start(bf16[128,2048]{1,0:T(8,128)(2,1)} %inputs_ref.1) | copy-start | bytes 1572868
  7.2 41.4 %copy-start.5 = (bf16[128,1024]{1,0:T(8,128)(2,1)S(1)}, bf16[128,1024]{1,0:T(8,128)(2,1)}, u32[]{:S(2)}) copy-start(bf16[128,1024]{1,0:T(8,128)(2,1)} %attended_ref.1) | copy-start | bytes 786436
  7.2 122.9 %all-gather.2.cloned.1.call-start = ((), (), s32[]{:S(2)}) async-start(), calls=%async_computation.5 | async-start | bytes 8650752 | tf_op jit(solution)/shard_map/all_gather | solution.py:276
  11.0 37.6 %all-to-all-start = ((bf16[32,96,128]{2,1,0:T(8,128)(2,1)}), bf16[32,96,128]{2,1,0:T(8,128)(2,1)S(1)}, u32[]{:S(2)}, u32[]{:S(2)}) async-start(bf16[32,96,128]{2,1,0:T(8,128)(2,1)} %broadcast_in_dim.20), calls=%async_computation | async-start | bytes 1572864 | tf_op jit(solution)/shard_map/all_to_all | solution.py:26
  22.9 35.3 %collective-permute-start = (bf16[128,1536]{1,0:T(8,128)(2,1)S(1)}, bf16[128,1536]{1,0:T(8,128)(2,1)S(1)}, u32[]{:S(2)}, u32[]{:S(2)}) collective-permute-start(bf16[128,1536]{1,0:T(8,128)(2,1)S(1)} %constant_dynamic-update-slice_fusion), channel_id=1, source_target_pairs={{0,2},{2,4},{4,6},{6,0},{1,3},{3,5},{5,7},{7,1},{8,10},{10,12},{12... | collective-permute-start | bytes 1179656 | tf_op jit(solution)/shard_map/ppermute | solution.py:35
  24.3 34.7 %collective-permute-start.1 = (bf16[128,1536]{1,0:T(8,128)(2,1)S(1)}, bf16[128,1536]{1,0:T(8,128)(2,1)S(1)}, u32[]{:S(2)}, u32[]{:S(2)}) collective-permute-start(bf16[128,1536]{1,0:T(8,128)(2,1)S(1)} %constant_dynamic-update-slice_fusion), channel_id=1, source_target_pairs={{0,4},{2,6},{4,0},{6,2},{1,5},{3,7},{5,1},{7,3},{8,12},{10,14},{12... | collective-permute-start | bytes 1179656 | tf_op jit(solution)/shard_map/ppermute | solution.py:35
  26.9 32.1 %collective-permute-start.2 = (bf16[128,1536]{1,0:T(8,128)(2,1)S(1)}, bf16[128,1536]{1,0:T(8,128)(2,1)}, u32[]{:S(2)}, u32[]{:S(2)}) collective-permute-start(bf16[128,1536]{1,0:T(8,128)(2,1)S(1)} %constant_dynamic-update-slice_fusion), channel_id=1, source_target_pairs={{0,6},{2,0},{4,2},{6,4},{1,7},{3,1},{5,3},{7,5},{8,14},{10,8},{12,... | collective-permute-start | bytes 1179656 | tf_op jit(solution)/shard_map/ppermute | solution.py:35
  49.7 15.0 %all-to-all-start.1 = ((f32[8,2,32,128]{3,2,1,0:T(8,128)}), f32[8,2,32,128]{3,2,1,0:T(8,128)S(1)}, u32[]{:S(2)}, u32[]{:S(2)}) async-start(f32[8,2,32,128]{3,2,1,0:T(8,128)} %bitcast.1), calls=%async_computation.1 | async-start | bytes 524288 | tf_op jit(solution)/shard_map/all_to_all | solution.py:26
  58.2 36.3 %collective-permute-start.4 = (bf16[32,96,128]{2,1,0:T(8,128)(2,1)S(1)}, bf16[32,96,128]{2,1,0:T(8,128)(2,1)}, u32[]{:S(2)}, u32[]{:S(2)}) collective-permute-start(bf16[32,96,128]{2,1,0:T(8,128)(2,1)S(1)} %all-to-all-done.factor_ref), channel_id=1, source_target_pairs={{0,1},{1,0},{2,3},{3,2},{4,5},{5,4},{6,7},{7,6},{8,9},{9,8},{10,11... | collective-permute-start | bytes 2359304 | tf_op jit(solution)/shard_map/ppermute | solution.py:35
  58.3 0.7 copy-start.3
  64.7 1.0 copy-start.4
  65.7 23.4 %copy-start.6 = (f32[8,1024]{1,0:T(8,128)S(1)}, f32[8,1024]{1,0:T(8,128)}, u32[]{:S(2)}) copy-start(f32[8,1024]{1,0:T(8,128)} %fo_ref.1) | copy-start | bytes 98308
  65.7 23.4 %copy-start.7 = (f32[8,1024]{1,0:T(8,128)S(1)}, f32[8,1024]{1,0:T(8,128)}, u32[]{:S(2)}) copy-start(f32[8,1024]{1,0:T(8,128)} %so_ref.1) | copy-start | bytes 98308
  65.7 23.4 %copy-start.8 = (f32[8,512]{1,0:T(8,128)S(1)}, f32[8,512]{1,0:T(8,128)}, u32[]{:S(2)}) copy-start(f32[8,512]{1,0:T(8,128)} %fq_ref.1) | copy-start | bytes 49156
  65.7 23.4 %copy-start.9 = (f32[8,512]{1,0:T(8,128)S(1)}, f32[8,512]{1,0:T(8,128)}, u32[]{:S(2)}) copy-start(f32[8,512]{1,0:T(8,128)} %sq_ref.1) | copy-start | bytes 49156
  68.3 20.8 %all-to-all-start.2 = ((f32[32,2,1536]{2,1,0:T(2,128)}), f32[32,2,1536]{2,1,0:T(2,128)S(1)}, u32[]{:S(2)}, u32[]{:S(2)}) async-start(f32[32,2,1536]{2,1,0:T(2,128)} %partial_sums.1), calls=%async_computation.2 | async-start | bytes 786432 | tf_op jit(solution)/shard_map/all_to_all | solution.py:26
  89.9 12.4 %all-to-all-start.3 = ((bf16[8,2,1664]{2,1,0:T(2,128)(2,1)}), bf16[8,2,1664]{2,1,0:T(2,128)(2,1)S(1)}, u32[]{:S(2)}, u32[]{:S(2)}) async-start(bf16[8,2,1664]{2,1,0:T(2,128)(2,1)} %get-tuple-element.21), calls=%async_computation.3 | async-start | bytes 106496 | tf_op jit(solution)/shard_map/all_to_all | solution.py:26
  97.4 32.7 %copy-start.10 = (bf16[3072,256]{1,0:T(8,128)(2,1)}, bf16[3072,256]{1,0:T(8,128)(2,1)S(1)}, u32[]{:S(2)}) copy-start(bf16[3072,256]{1,0:T(8,128)(2,1)S(1)} %fusion) | copy-start | bytes 4718596
  102.3 9.9 %collective-permute-start.5 = (f32[2,1536]{1,0:T(2,128)S(1)}, f32[2,1536]{1,0:T(2,128)S(1)}, u32[]{:S(2)}, u32[]{:S(2)}) collective-permute-start(f32[2,1536]{1,0:T(2,128)S(1)} %get-tuple-element.27), channel_id=1, source_target_pairs={{0,2},{2,4},{4,6},{6,0},{1,3},{3,5},{5,7},{7,1},{8,10},{10,12},{12... | collective-permute-start | bytes 36872 | tf_op jit(solution)/shard_map/ppermute | solution.py:35
  102.5 9.7 %collective-permute-start.6 = (f32[2,1536]{1,0:T(2,128)S(1)}, f32[2,1536]{1,0:T(2,128)S(1)}, u32[]{:S(2)}, u32[]{:S(2)}) collective-permute-start(f32[2,1536]{1,0:T(2,128)S(1)} %get-tuple-element.27), channel_id=1, source_target_pairs={{0,4},{2,6},{4,0},{6,2},{1,5},{3,7},{5,1},{7,3},{8,12},{10,14},{12... | collective-permute-start | bytes 36872 | tf_op jit(solution)/shard_map/ppermute | solution.py:35
  104.0 8.2 %collective-permute-start.7 = (f32[2,1536]{1,0:T(2,128)S(1)}, f32[2,1536]{1,0:T(2,128)S(1)}, u32[]{:S(2)}, u32[]{:S(2)}) collective-permute-start(f32[2,1536]{1,0:T(2,128)S(1)} %get-tuple-element.27), channel_id=1, source_target_pairs={{0,6},{2,0},{4,2},{6,4},{1,7},{3,1},{5,3},{7,5},{8,14},{10,8},{12,... | collective-permute-start | bytes 36872 | tf_op jit(solution)/shard_map/ppermute | solution.py:35
  106.6 16.4 %all-to-all-start.4 = ((bf16[16,16,1664]{2,1,0:T(8,128)(2,1)}), bf16[16,16,1664]{2,1,0:T(8,128)(2,1)S(1)}, u32[]{:S(2)}, u32[]{:S(2)}) async-start(bf16[16,16,1664]{2,1,0:T(8,128)(2,1)} %broadcast_in_dim.21), calls=%async_computation.4 | async-start | bytes 1703936 | tf_op jit(solution)/shard_map/all_to_all | solution.py:26
  123.0 7.1 %copy-start.11 = (bf16[16,16,1664]{2,1,0:T(8,128)(2,1)}, bf16[16,16,1664]{2,1,0:T(8,128)(2,1)S(1)}, u32[]{:S(2)}) copy-start(bf16[16,16,1664]{2,1,0:T(8,128)(2,1)S(1)} %all-to-all-done.4) | copy-start | bytes 2555908
  123.8 6.3 %collective-permute-start.3 = (f32[1,1]{1,0:T(1,128)}, f32[1,1]{1,0:T(1,128)}, u32[]{:S(2)}, u32[]{:S(2)}) collective-permute-start(f32[1,1]{1,0:T(1,128)} %bitcast.4.mine_ref), channel_id=1, source_target_pairs={{0,1},{1,0},{2,3},{3,2},{4,5},{5,4},{6,7},{7,6},{8,9},{9,8},{10,11... | collective-permute-start | bytes 20 | tf_op jit(solution)/shard_map/ppermute | solution.py:35
Sparse Core Ops, SparseCore 0:
  10.6 111.9 all-gather.1

commit v4 on v3

--- a/solution.py
+++ b/solution.py
@@ -35,17 +35,6 @@
     return lax.ppermute(array, axis, [(i, (i + by) % n) for i in range(n)])
 
 
-def one_hot(rows_of, columns, rows):
-    r = lax.broadcasted_iota(jnp.int32, (rows, columns), 0)
-    return (r == rows_of).astype(bf16)
-
-
-def rank_of(core):
-    k = lax.broadcasted_iota(jnp.int32, (1, RANK // NTP), 1)
-    x, j, z = k // 32, (k // 8) % 4, k % 8
-    return 8 * (4 * z + x) + 2 * j + core
-
-
 VMEM = pl.BlockSpec(memory_space=pltpu.VMEM)
 
 
@@ -72,7 +61,38 @@
     )(query, output)
 
 
-def project_kernel(factor_ref, inputs_ref, attended_ref, out_ref):
+def select_kernel(place_ref, query_ref, output_ref, out_ref):
+    rep, core = place_ref[0], place_ref[1]
+    both = jnp.concatenate([query_ref[...], output_ref[...]], axis=0)
+    i = lax.broadcasted_iota(jnp.int32, (24, 96), 0)
+    r = lax.broadcasted_iota(jnp.int32, (24, 96), 1)
+    rows = (r == jnp.where(i < 16, 16 * rep + i, 48 + 8 * rep + i)).astype(bf16)
+    k = lax.broadcasted_iota(jnp.int32, (RANK, 128), 1)
+    r = lax.broadcasted_iota(jnp.int32, (RANK, 128), 0)
+    ranks = (r == 32 * (k % 8) + 8 * (k // 32) + 2 * ((k // 8) % 4) + core).astype(bf16)
+    chosen = jnp.dot(rows, both, preferred_element_type=f32).astype(bf16)
+    chosen = jnp.dot(chosen, ranks, preferred_element_type=f32).astype(bf16)
+    for n in range(NZ):
+        out_ref[n] = chosen
+
+
+def select(place, query, output):
+    return pl.pallas_call(
+        select_kernel,
+        in_specs=[SMEM, VMEM, VMEM],
+        out_specs=VMEM,
+        out_shape=pltpu.VMEM((NZ, 24, 128), bf16),
+        name="select",
+    )(place, query, output)
+
+
+def project_kernel(piece_ref, inputs_ref, attended_ref, red_ref, factor_ref):
+    for z in range(NZ):
+        for x in range(NX):
+            for j in range(NREP):
+                n, at = NX * z + x, 24 * z
+                factor_ref[n, 16 * j : 16 * j + 16] = piece_ref[NREP * x + j, at : at + 16]
+                factor_ref[n, 64 + 8 * j : 72 + 8 * j] = piece_ref[NREP * x + j, at + 16 : at + 24]
     factors_q = factor_ref[:, :64, :].reshape(D, 128)
     factors_o = factor_ref[:, 64:, :].reshape(DA, 128)
     for n, (left, right) in enumerate(((inputs_ref, factors_q), (attended_ref, factors_o))):
@@ -80,18 +100,21 @@
         red = red.reshape(NX, NREP, NZ, 128)
         for j in range(NREP):
             mine = red[:, j].reshape(FS, 128)
-            out_ref[j, 0, n] = mine
-            out_ref[j, 1, n] = mine
-
-
-def project(factors, inputs, attended):
+            red_ref[j, 0, n] = mine
+            red_ref[j, 1, n] = mine
+
+
+def project(pieces, inputs, attended):
     return pl.pallas_call(
         project_kernel,
         in_specs=[VMEM, VMEM, VMEM],
-        out_specs=VMEM,
-        out_shape=pltpu.VMEM((NREP, NTP, 2, FS, 128), f32),
+        out_specs=[VMEM, VMEM],
+        out_shape=[
+            pltpu.VMEM((NREP, NTP, 2, FS, 128), f32),
+            pltpu.VMEM((FS, 96, 128), bf16),
+        ],
         name="project",
-    )(near(factors), near(inputs), near(attended))
+    )(near(pieces), near(inputs), near(attended))
 
 
 def partial_kernel(rep_ref, red_ref, query_ref, output_ref, c1_ref, c2_ref, c3_ref, out_ref):
@@ -278,11 +301,12 @@
     cots = jnp.concatenate([query_cot, output_cot], axis=1)
     cots = [shifted(cots, "rep", 1), shifted(cots, "rep", 2), shifted(cots, "rep", 3)]
 
-    both = jnp.concatenate([proj_query, proj_output], axis=0)
-    mine = jnp.dot(both, one_hot(rank_of(core), 128, RANK), preferred_element_type=f32)
-    factors = from_everyone(mine.astype(bf16).reshape(96, 128), ("z", "x"), FS)
-
-    red = project(factors, inputs, attended).reshape(8, 2, FS, 128)
+    piece = select(jnp.stack([rep, core]), proj_query, proj_output)
+    piece = exchange(piece, "z")
+    piece = from_everyone(piece.reshape(NZ * 24, 128), ("x", "rep"), 16)
+
+    red, factors = project(piece, inputs, attended)
+    red = red.reshape(8, 2, FS, 128)
     red = exchange(red, ("rep", "tp")).reshape(NREP, NTP, 2, FS, 128)
     part = exchange(partial_sums(here, red, [query_cot, output_cot] + cots), ("x", "z"))
     low, half = normed_payload(

time: 146 us -> 148 us (1.014)
  blocking collectives: 0 us -> 15.9 us
  waiting for transfers between devices: 55.1 us -> 44.2 us
  starting transfers between devices: 47.9 us -> 43.5 us
    all_to_all x5, waiting for transfers between devices: 54.2 us -> 36.3 us  [exchange(): return lax.all_to_all(pieces, axes, split_axis=0, concat_axis=0, tiled=True)]
    all_to_all x0 -> x1, blocking collectives: none -> 15.9 us  [exchange(): return lax.all_to_all(pieces, axes, split_axis=0, concat_axis=0, tiled=True)]
    ppermute x8, waiting for transfers between devices: 0.9 us -> 7.9 us  [shifted(): return lax.ppermute(array, axis, [(i, (i + by) % n) for i in range(n)])]
    all_to_all x5, starting transfers between devices: 34.7 us -> 29.5 us  [exchange(): return lax.all_to_all(pieces, axes, split_axis=0, concat_axis=0, tiled=True)]
  transfers between devices with their start and end apart: 14 -> 14, of which waited for: 6 -> 7; matrix products, arithmetic and copies ran while one was open for 8% -> 9% of each run, Pallas kernels for 3% -> 4%
where the time goes in v4:
time: 148 us; the launch traced here: 147 us
  waiting for transfers between devices  44.2 us (30%)
  starting transfers between devices  43.5 us (29%)
  Pallas kernels  15.9 us (11%)
  blocking collectives  15.9 us (11%)
  between operations  14.3 us (10%)
  local copies, waits for them, and re-layouts  5.75 us (4%)
  matrix products  5.1 us (3%)
  other arithmetic  2.8 us (2%)
    all_to_all x5, waiting for transfers between devices, exchange(): return lax.all_to_all(pieces, axes, split_axis=0, concat_axis=0, tiled=True)  36.3 us
    all_to_all x5, starting transfers between devices, exchange(): return lax.all_to_all(pieces, axes, split_axis=0, concat_axis=0, tiled=True)  29.5 us
    all_to_all x1, blocking collectives, exchange(): return lax.all_to_all(pieces, axes, split_axis=0, concat_axis=0, tiled=True)  15.9 us
    ppermute x8, starting transfers between devices, shifted(): return lax.ppermute(array, axis, [(i, (i + by) % n) for i in range(n)])  13.9 us
    pallas_call x1, Pallas kernels, finish(): pl.pallas_call(finish_kernel, grid=(FS // step,), in_specs=[SMEM, SMEM, w...  8.42 us
    ppermute x8, waiting for transfers between devices, shifted(): return lax.ppermute(array, axis, [(i, (i + by) % n) for i in range(n)])  7.9 us
  transfers between devices with their start and end apart: 14, of which 7 were waited for; matrix products, arithmetic and copies ran while one was open for 9% of the time, Pallas kernels for 4%

profile of v4, /device:TPU:1, one launch (start us, length us, event | category | flops | bytes accessed | tf_op | source)
XLA Modules:
  0.0 147.4 jit_solution(2579453316271555012)
XLA Ops:
  7.3 1.8 %join.1 = f32[128,512]{1,0:T(8,128)} custom-call(f32[64,512]{1,0:T(8,128)} %wq_ref.1, f32[32,1024]{1,0:T(8,128)} %wo_ref.1), custom_call_target="tpu_custom_call" | custom-call | tf_op jit(solution)/shard_map/join/pallas_call | solution.py:55
  9.7 1.0 select.17
  10.7 15.9 %all_to_all.30 = bf16[8,24,128]{2,1,0:T(8,128)(2,1)S(1)} all-to-all(bf16[8,24,128]{2,1,0:T(8,128)(2,1)S(1)} %select.17), channel_id=1, replica_groups=mesh['z'=8,'x'=4,'rep'=4,'tp'=2] {'z'}, dimensions={0} | all-to-all | bytes 98304 | tf_op jit(solution)/shard_map/all_to_all | solution.py:26
  26.6 1.0 broadcast_in_dim.20
  27.6 6.8 %all-to-all-start.1 = ((bf16[16,192,128]{2,1,0:T(8,128)(2,1)}), bf16[16,192,128]{2,1,0:T(8,128)(2,1)S(1)}, u32[]{:S(2)}, u32[]{:S(2)}) async-start(bf16[16,192,128]{2,1,0:T(8,128)(2,1)} %broadcast_in_dim.20), calls=%async_computation.1 | async-start | bytes 1572864 | tf_op jit(solution)/shard_map/all_to_all | solution.py:26
  35.0 0.7 constant_dynamic-update-slice_fusion
  35.8 1.4 collective-permute-start
  37.1 2.4 %collective-permute-start.1 = (bf16[128,1536]{1,0:T(8,128)(2,1)}, bf16[128,1536]{1,0:T(8,128)(2,1)}, u32[]{:S(2)}, u32[]{:S(2)}) collective-permute-start(bf16[128,1536]{1,0:T(8,128)(2,1)} %constant_dynamic-update-slice_fusion), channel_id=1, source_target_pairs={{0,4},{2,6},{4,0},{6,2},{1,5},{3,7},{5,1},{7,3},{8,12},{10,14},{12... | collective-permute-start | bytes 1179656 | tf_op jit(solution)/shard_map/ppermute | solution.py:35
  39.5 1.2 collective-permute-start.2
  40.7 6.6 %all-to-all-done.1.piece_ref = bf16[16,192,128]{2,1,0:T(8,128)(2,1)S(1)} async-done(((bf16[16,192,128]{2,1,0:T(8,128)(2,1)}), bf16[16,192,128]{2,1,0:T(8,128)(2,1)S(1)}, u32[]{:S(2)}, u32[]{:S(2)}) %all-to-all-start.1) | async-done | bytes 786464 | tf_op jit(solution)/shard_map/all_to_all | solution.py:26
  47.3 1.2 project.1
  48.5 0.9 copy-done.2
  49.3 7.3 %all-to-all-start.2 = ((f32[8,2,32,128]{3,2,1,0:T(8,128)}), f32[8,2,32,128]{3,2,1,0:T(8,128)S(1)}, u32[]{:S(2)}, u32[]{:S(2)}) async-start(f32[8,2,32,128]{3,2,1,0:T(8,128)} %bitcast.3), calls=%async_computation.2 | async-start | bytes 524288 | tf_op jit(solution)/shard_map/all_to_all | solution.py:26
  56.8 6.9 %collective-permute-done.1.c2_ref = bf16[128,1536]{1,0:T(8,128)(2,1)} collective-permute-done((bf16[128,1536]{1,0:T(8,128)(2,1)}, bf16[128,1536]{1,0:T(8,128)(2,1)}, u32[]{:S(2)}, u32[]{:S(2)}) %collective-permute-start.1) | collective-permute-done | bytes 393248 | tf_op jit(solution)/shard_map/ppermute | solution.py:35
  63.7 3.4 %all-to-all-done.2 = f32[8,2,32,128]{3,2,1,0:T(8,128)S(1)} async-done(((f32[8,2,32,128]{3,2,1,0:T(8,128)}), f32[8,2,32,128]{3,2,1,0:T(8,128)S(1)}, u32[]{:S(2)}, u32[]{:S(2)}) %all-to-all-start.2) | async-done | bytes 262176 | tf_op jit(solution)/shard_map/all_to_all | solution.py:26
  67.1 2.7 %partial_sums.1 = f32[32,2,1536]{2,1,0:T(2,128)} custom-call(s32[1]{0:T(128)} %bitcast.rep_ref, f32[4,2,2,32,128]{4,3,2,1,0:T(8,128)S(1)} %bitcast.21, bf16[128,512]{1,0:T(8,128)(2,1)S(1)} %copy-done.5, bf16[128,1024]{1,0:T(8,128)(2,1)S(1)} %copy-done.1, bf16[128,1536]{1,0:T(8,128)(2,1)S(1)} %collective-permute-done.c1_ref, ...), custom_call_target="tpu_custom_call" | custom-call | tf_op jit(solution)/shard_map/partial_sums/pallas_call | solution.py:144
  69.8 4.3 %all-to-all-start.3 = ((f32[32,2,1536]{2,1,0:T(2,128)}), f32[32,2,1536]{2,1,0:T(2,128)S(1)}, u32[]{:S(2)}, u32[]{:S(2)}) async-start(f32[32,2,1536]{2,1,0:T(2,128)} %partial_sums.1), calls=%async_computation.3 | async-start | bytes 786432 | tf_op jit(solution)/shard_map/all_to_all | solution.py:26
  74.4 2.3 %fusion.1 = f32[3072,256]{1,0:T(8,128)} fusion(bf16[3072,128]{1,0:T(8,128)(2,1)S(1)} %bitcast.22, s32[128]{0:T(128)S(1)} %get-tuple-element.39), kind=kOutput, calls=%fused_computation.6 | convolution fusion | flops 201359360 | bytes 3932672 | tf_op jit(solution)/shard_map/dot_general | solution.py:327
  76.7 12.6 %all-to-all-done.3.part_ref = f32[32,2,1536]{2,1,0:T(2,128)S(1)} async-done(((f32[32,2,1536]{2,1,0:T(2,128)}), f32[32,2,1536]{2,1,0:T(2,128)S(1)}, u32[]{:S(2)}, u32[]{:S(2)}) %all-to-all-start.3) | async-done | bytes 393248 | tf_op jit(solution)/shard_map/all_to_all | solution.py:26
  89.3 0.8 normed_payload.1
  90.1 5.8 %all-to-all-start.4 = ((bf16[8,2,1664]{2,1,0:T(2,128)(2,1)}), bf16[8,2,1664]{2,1,0:T(2,128)(2,1)S(1)}, u32[]{:S(2)}, u32[]{:S(2)}) async-start(bf16[8,2,1664]{2,1,0:T(2,128)(2,1)} %get-tuple-element.24), calls=%async_computation.4 | async-start | bytes 106496 | tf_op jit(solution)/shard_map/all_to_all | solution.py:26
  95.9 2.8 %fusion = bf16[3072,256]{1,0:T(8,128)(2,1)S(1)} fusion(f32[3072,256]{1,0:T(8,128)} %fusion.1, bf16[3072,128]{1,0:T(8,128)(2,1)} %bitcast.8, s32[128]{0:T(128)S(1)} %get-tuple-element.38), kind=kOutput, calls=%fused_computation.2 | convolution fusion | flops 202932224 | bytes 5505536 | tf_op jit(solution)/shard_map/dot_general | solution.py:328
  98.7 4.9 %all-to-all-done.4 = bf16[8,2,1664]{2,1,0:T(2,128)(2,1)S(1)} async-done(((bf16[8,2,1664]{2,1,0:T(2,128)(2,1)}), bf16[8,2,1664]{2,1,0:T(2,128)(2,1)S(1)}, u32[]{:S(2)}, u32[]{:S(2)}) %all-to-all-start.4) | async-done | bytes 53280 | tf_op jit(solution)/shard_map/all_to_all | solution.py:26
  103.7 2.0 %collective-permute-start.7 = (f32[2,1536]{1,0:T(2,128)S(1)}, f32[2,1536]{1,0:T(2,128)S(1)}, u32[]{:S(2)}, u32[]{:S(2)}) collective-permute-start(f32[2,1536]{1,0:T(2,128)S(1)} %get-tuple-element.31), channel_id=1, source_target_pairs={{0,6},{2,0},{4,2},{6,4},{1,7},{3,1},{5,3},{7,5},{8,14},{10,8},{12,... | collective-permute-start | bytes 36872 | tf_op jit(solution)/shard_map/ppermute | solution.py:35
  105.7 1.3 collective-permute-start.6
  107.6 1.0 broadcast_in_dim.21
  108.5 5.4 %all-to-all-start.5 = ((bf16[16,16,1664]{2,1,0:T(8,128)(2,1)}), bf16[16,16,1664]{2,1,0:T(8,128)(2,1)S(1)}, u32[]{:S(2)}, u32[]{:S(2)}) async-start(bf16[16,16,1664]{2,1,0:T(8,128)(2,1)} %broadcast_in_dim.21), calls=%async_computation.5 | async-start | bytes 1703936 | tf_op jit(solution)/shard_map/all_to_all | solution.py:26
  116.0 8.8 %all-to-all-done.5 = bf16[16,16,1664]{2,1,0:T(8,128)(2,1)S(1)} async-done(((bf16[16,16,1664]{2,1,0:T(8,128)(2,1)}), bf16[16,16,1664]{2,1,0:T(8,128)(2,1)S(1)}, u32[]{:S(2)}, u32[]{:S(2)}) %all-to-all-start.5) | async-done | bytes 852000 | tf_op jit(solution)/shard_map/all_to_all | solution.py:26
  124.7 0.8 convert_reduce_fusion
  125.5 5.5 %collective-permute-start.3 = (f32[1,1]{1,0:T(1,128)}, f32[1,1]{1,0:T(1,128)}, u32[]{:S(2)}, u32[]{:S(2)}) collective-permute-start(f32[1,1]{1,0:T(1,128)} %bitcast.6.mine_ref), channel_id=1, source_target_pairs={{0,1},{1,0},{2,3},{3,2},{4,5},{5,4},{6,7},{7,6},{8,9},{9,8},{10,11... | collective-permute-start | bytes 20 | tf_op jit(solution)/shard_map/ppermute | solution.py:35
  131.1 1.0 collective-permute-done.3.other_ref
  132.1 8.4 %finish.1 = (bf16[2048,512]{1,0:T(8,128)(2,1)}, bf16[1024,1024]{1,0:T(8,128)(2,1)}, f32[64,512]{1,0:T(8,128)}, f32[32,1024]{1,0:T(8,128)}, f32[64,512]{1,0:T(8,128)}, /*index=5*/f32[32,1024]{1,0:T(8,128)}) custom-call(f32[1,1]{1,0:T(1,128)} %bitcast.6.mine_ref, f32[1,1]{1,0:T(1,128)} %collective-permute-done.3.other_ref, bf16[256,1664]{1,0:T(8,128)(2,1)} %bitcast.28, ...), custom_call_target="tpu_custom_call" | custom-call | tf_op jit(solution)/shard_map/finish/pallas_call | solution.py:245
  (52 shorter events, 4.4 us)
Async XLA Ops:
  7.2 27.2 %copy-start.5 = (bf16[128,512]{1,0:T(8,128)(2,1)S(1)}, bf16[128,512]{1,0:T(8,128)(2,1)}, u32[]{:S(2)}) copy-start(bf16[128,512]{1,0:T(8,128)(2,1)} %query_ref.4) | copy-start | bytes 393220
  7.2 27.9 %copy-start = (bf16[128,1024]{1,0:T(8,128)(2,1)S(1)}, bf16[128,1024]{1,0:T(8,128)(2,1)}, u32[]{:S(2)}) copy-start(bf16[128,1024]{1,0:T(8,128)(2,1)} %output_ref.4) | copy-start | bytes 786436
  7.2 59.9 %copy-start.1 = (bf16[128,1024]{1,0:T(8,128)(2,1)S(1)}, bf16[128,1024]{1,0:T(8,128)(2,1)}, u32[]{:S(2)}) copy-start(bf16[128,1024]{1,0:T(8,128)(2,1)} %output_ref.4) | copy-start | bytes 786436
  7.2 40.1 %copy-start.4 = (bf16[128,2048]{1,0:T(8,128)(2,1)S(1)}, bf16[128,2048]{1,0:T(8,128)(2,1)}, u32[]{:S(2)}) copy-start(bf16[128,2048]{1,0:T(8,128)(2,1)} %inputs_ref.1) | copy-start | bytes 1572868
  7.2 40.1 %copy-start.6 = (bf16[128,1024]{1,0:T(8,128)(2,1)S(1)}, bf16[128,1024]{1,0:T(8,128)(2,1)}, u32[]{:S(2)}) copy-start(bf16[128,1024]{1,0:T(8,128)(2,1)} %attended_ref.1) | copy-start | bytes 786436
  7.2 124.9 %all-gather.2.cloned.1.call-start = ((), (), s32[]{:S(2)}) async-start(), calls=%async_computation.6 | async-start | bytes 8650752 | tf_op jit(solution)/shard_map/all_gather | solution.py:299
  27.6 19.7 %all-to-all-start.1 = ((bf16[16,192,128]{2,1,0:T(8,128)(2,1)}), bf16[16,192,128]{2,1,0:T(8,128)(2,1)S(1)}, u32[]{:S(2)}, u32[]{:S(2)}) async-start(bf16[16,192,128]{2,1,0:T(8,128)(2,1)} %broadcast_in_dim.20), calls=%async_computation.1 | async-start | bytes 1572864 | tf_op jit(solution)/shard_map/all_to_all | solution.py:26
  35.8 21.0 %collective-permute-start = (bf16[128,1536]{1,0:T(8,128)(2,1)}, bf16[128,1536]{1,0:T(8,128)(2,1)S(1)}, u32[]{:S(2)}, u32[]{:S(2)}) collective-permute-start(bf16[128,1536]{1,0:T(8,128)(2,1)} %constant_dynamic-update-slice_fusion), channel_id=1, source_target_pairs={{0,2},{2,4},{4,6},{6,0},{1,3},{3,5},{5,7},{7,1},{8,10},{10,12},{12... | collective-permute-start | bytes 1179656 | tf_op jit(solution)/shard_map/ppermute | solution.py:35
  37.1 26.6 %collective-permute-start.1 = (bf16[128,1536]{1,0:T(8,128)(2,1)}, bf16[128,1536]{1,0:T(8,128)(2,1)}, u32[]{:S(2)}, u32[]{:S(2)}) collective-permute-start(bf16[128,1536]{1,0:T(8,128)(2,1)} %constant_dynamic-update-slice_fusion), channel_id=1, source_target_pairs={{0,4},{2,6},{4,0},{6,2},{1,5},{3,7},{5,1},{7,3},{8,12},{10,14},{12... | collective-permute-start | bytes 1179656 | tf_op jit(solution)/shard_map/ppermute | solution.py:35
  39.5 24.2 %collective-permute-start.2 = (bf16[128,1536]{1,0:T(8,128)(2,1)}, bf16[128,1536]{1,0:T(8,128)(2,1)}, u32[]{:S(2)}, u32[]{:S(2)}) collective-permute-start(bf16[128,1536]{1,0:T(8,128)(2,1)} %constant_dynamic-update-slice_fusion), channel_id=1, source_target_pairs={{0,6},{2,0},{4,2},{6,4},{1,7},{3,1},{5,3},{7,5},{8,14},{10,8},{12,... | collective-permute-start | bytes 1179656 | tf_op jit(solution)/shard_map/ppermute | solution.py:35
  48.5 0.9 copy-start.2
  49.3 25.1 %copy-start.3 = (bf16[32,96,128]{2,1,0:T(8,128)(2,1)S(1)}, bf16[32,96,128]{2,1,0:T(8,128)(2,1)}, u32[]{:S(2)}) copy-start(bf16[32,96,128]{2,1,0:T(8,128)(2,1)} %copy-done.2) | copy-start | bytes 2359300
  49.3 17.8 %all-to-all-start.2 = ((f32[8,2,32,128]{3,2,1,0:T(8,128)}), f32[8,2,32,128]{3,2,1,0:T(8,128)S(1)}, u32[]{:S(2)}, u32[]{:S(2)}) async-start(f32[8,2,32,128]{3,2,1,0:T(8,128)} %bitcast.3), calls=%async_computation.2 | async-start | bytes 524288 | tf_op jit(solution)/shard_map/all_to_all | solution.py:26
  56.6 39.3 %collective-permute-start.4 = (bf16[32,96,128]{2,1,0:T(8,128)(2,1)}, bf16[32,96,128]{2,1,0:T(8,128)(2,1)}, u32[]{:S(2)}, u32[]{:S(2)}) collective-permute-start(bf16[32,96,128]{2,1,0:T(8,128)(2,1)} %copy-done.2), channel_id=1, source_target_pairs={{0,1},{1,0},{2,3},{3,2},{4,5},{5,4},{6,7},{7,6},{8,9},{9,8},{10,11... | collective-permute-start | bytes 2359304 | tf_op jit(solution)/shard_map/ppermute | solution.py:35
  67.1 22.2 %copy-start.7 = (f32[8,1024]{1,0:T(8,128)S(1)}, f32[8,1024]{1,0:T(8,128)}, u32[]{:S(2)}) copy-start(f32[8,1024]{1,0:T(8,128)} %fo_ref.1) | copy-start | bytes 98308
  67.1 22.2 %copy-start.8 = (f32[8,1024]{1,0:T(8,128)S(1)}, f32[8,1024]{1,0:T(8,128)}, u32[]{:S(2)}) copy-start(f32[8,1024]{1,0:T(8,128)} %so_ref.1) | copy-start | bytes 98308
  67.1 22.2 %copy-start.9 = (f32[8,512]{1,0:T(8,128)S(1)}, f32[8,512]{1,0:T(8,128)}, u32[]{:S(2)}) copy-start(f32[8,512]{1,0:T(8,128)} %fq_ref.1) | copy-start | bytes 49156
  67.1 22.1 %copy-start.10 = (f32[8,512]{1,0:T(8,128)S(1)}, f32[8,512]{1,0:T(8,128)}, u32[]{:S(2)}) copy-start(f32[8,512]{1,0:T(8,128)} %sq_ref.1) | copy-start | bytes 49156
  69.8 19.4 %all-to-all-start.3 = ((f32[32,2,1536]{2,1,0:T(2,128)}), f32[32,2,1536]{2,1,0:T(2,128)S(1)}, u32[]{:S(2)}, u32[]{:S(2)}) async-start(f32[32,2,1536]{2,1,0:T(2,128)} %partial_sums.1), calls=%async_computation.3 | async-start | bytes 786432 | tf_op jit(solution)/shard_map/all_to_all | solution.py:26
  90.1 13.6 %all-to-all-start.4 = ((bf16[8,2,1664]{2,1,0:T(2,128)(2,1)}), bf16[8,2,1664]{2,1,0:T(2,128)(2,1)S(1)}, u32[]{:S(2)}, u32[]{:S(2)}) async-start(bf16[8,2,1664]{2,1,0:T(2,128)(2,1)} %get-tuple-element.24), calls=%async_computation.4 | async-start | bytes 106496 | tf_op jit(solution)/shard_map/all_to_all | solution.py:26
  98.7 33.4 %copy-start.11 = (bf16[3072,256]{1,0:T(8,128)(2,1)}, bf16[3072,256]{1,0:T(8,128)(2,1)S(1)}, u32[]{:S(2)}) copy-start(bf16[3072,256]{1,0:T(8,128)(2,1)S(1)} %fusion) | copy-start | bytes 4718596
  103.7 10.2 %collective-permute-start.7 = (f32[2,1536]{1,0:T(2,128)S(1)}, f32[2,1536]{1,0:T(2,128)S(1)}, u32[]{:S(2)}, u32[]{:S(2)}) collective-permute-start(f32[2,1536]{1,0:T(2,128)S(1)} %get-tuple-element.31), channel_id=1, source_target_pairs={{0,6},{2,0},{4,2},{6,4},{1,7},{3,1},{5,3},{7,5},{8,14},{10,8},{12,... | collective-permute-start | bytes 36872 | tf_op jit(solution)/shard_map/ppermute | solution.py:35
  105.7 8.3 %collective-permute-start.6 = (f32[2,1536]{1,0:T(2,128)S(1)}, f32[2,1536]{1,0:T(2,128)S(1)}, u32[]{:S(2)}, u32[]{:S(2)}) collective-permute-start(f32[2,1536]{1,0:T(2,128)S(1)} %get-tuple-element.31), channel_id=1, source_target_pairs={{0,4},{2,6},{4,0},{6,2},{1,5},{3,7},{5,1},{7,3},{8,12},{10,14},{12... | collective-permute-start | bytes 36872 | tf_op jit(solution)/shard_map/ppermute | solution.py:35
  106.9 7.0 %collective-permute-start.5 = (f32[2,1536]{1,0:T(2,128)S(1)}, f32[2,1536]{1,0:T(2,128)S(1)}, u32[]{:S(2)}, u32[]{:S(2)}) collective-permute-start(f32[2,1536]{1,0:T(2,128)S(1)} %get-tuple-element.31), channel_id=1, source_target_pairs={{0,2},{2,4},{4,6},{6,0},{1,3},{3,5},{5,7},{7,1},{8,10},{10,12},{12... | collective-permute-start | bytes 36872 | tf_op jit(solution)/shard_map/ppermute | solution.py:35
  108.5 16.2 %all-to-all-start.5 = ((bf16[16,16,1664]{2,1,0:T(8,128)(2,1)}), bf16[16,16,1664]{2,1,0:T(8,128)(2,1)S(1)}, u32[]{:S(2)}, u32[]{:S(2)}) async-start(bf16[16,16,1664]{2,1,0:T(8,128)(2,1)} %broadcast_in_dim.21), calls=%async_computation.5 | async-start | bytes 1703936 | tf_op jit(solution)/shard_map/all_to_all | solution.py:26
  124.7 7.4 %copy-start.12 = (bf16[16,16,1664]{2,1,0:T(8,128)(2,1)}, bf16[16,16,1664]{2,1,0:T(8,128)(2,1)S(1)}, u32[]{:S(2)}) copy-start(bf16[16,16,1664]{2,1,0:T(8,128)(2,1)S(1)} %all-to-all-done.5) | copy-start | bytes 2555908
  125.5 6.6 %collective-permute-start.3 = (f32[1,1]{1,0:T(1,128)}, f32[1,1]{1,0:T(1,128)}, u32[]{:S(2)}, u32[]{:S(2)}) collective-permute-start(f32[1,1]{1,0:T(1,128)} %bitcast.6.mine_ref), channel_id=1, source_target_pairs={{0,1},{1,0},{2,3},{3,2},{4,5},{5,4},{6,7},{7,6},{8,9},{9,8},{10,11... | collective-permute-start | bytes 20 | tf_op jit(solution)/shard_map/ppermute | solution.py:35
Sparse Core Ops, SparseCore 0:
  10.6 107.9 all-gather.1

commit v5 on v3

--- a/solution.py
+++ b/solution.py
@@ -56,10 +56,27 @@
 SMEM = pl.BlockSpec(memory_space=pltpu.SMEM)
 
 
+def coded(w):
+    s = jnp.abs(w) * 2.0**18
+    s = s * s
+    s = s * s
+    s = s * s
+    return jnp.where(w < 0, -s, s).astype(bf16)
+
+
+def decoded(code):
+    v = code.astype(f32)
+    s = jnp.abs(v)
+    s = jnp.maximum(s, 2.0**-126)
+    s = lax.rsqrt(lax.rsqrt(s * lax.rsqrt(s)))
+    s = jnp.where(v == 0, 0.0, s * 2.0**-18)
+    return jnp.where(v < 0, -s, s)
+
+
 def join_kernel(query_ref, output_ref, both_ref):
-    both_ref[:64] = query_ref[...]
-    both_ref[64:96] = output_ref[:, :512]
-    both_ref[96:] = output_ref[:, 512:]
+    both_ref[:64] = coded(query_ref[...])
+    both_ref[64:96] = coded(output_ref[:, :512])
+    both_ref[96:] = coded(output_ref[:, 512:])
 
 
 def join(query, output):
@@ -67,9 +84,25 @@
         join_kernel,
         in_specs=[VMEM, VMEM],
         out_specs=VMEM,
-        out_shape=jax.ShapeDtypeStruct((128, 512), f32),
+        out_shape=jax.ShapeDtypeStruct((128, 512), bf16),
         name="join",
     )(query, output)
+
+
+def decode_kernel(code_ref, out_ref):
+    out_ref[...] = decoded(code_ref[...])
+
+
+def decode(codes):
+    step = 8
+    return pl.pallas_call(
+        decode_kernel,
+        grid=(FS // step,),
+        in_specs=[pl.BlockSpec((step, 128, 512), lambda i: (i, 0, 0))],
+        out_specs=pl.BlockSpec((step, 128, 512), lambda i: (i, 0, 0)),
+        out_shape=jax.ShapeDtypeStruct((FS, 128, 512), f32),
+        name="decode",
+    )(pltpu.with_memory_space_constraint(codes, pltpu.HBM))
 
 
 def project_kernel(factor_ref, inputs_ref, attended_ref, out_ref):
@@ -124,7 +157,7 @@
         out_specs=VMEM,
         out_shape=pltpu.VMEM((FS, NTP, 1536), f32),
         name="partial_sums",
-    )(rep, near(red), *[near(c) for c in cots])
+    )(rep, near(red), *cots)
 
 
 def moments(low_sum, first, second):
@@ -180,76 +213,89 @@
     )(rep, *[near(a) for a in (part, first_query, second_query, first_output, second_output)])
 
 
+CHUNKS = 4
+
+
 def finish_kernel(
-    mine_ref, other_ref, half_ref, rows_ref, wq_ref, wo_ref, w_ref, p_ref,
+    mine_ref, other_ref, half_ref, rows_ref, wq_ref, wo_ref, p_ref, w_ref,
     copy_q_ref, copy_o_ref, step_q_ref, step_o_ref, new_q_ref, new_o_ref,
+    w_buf, q_buf, o_buf, sq_buf, so_buf, nq_buf, no_buf, in_sem, out_sem,
 ):
+    n = FS // CHUNKS
+    arrivals = []
+    for c in range(CHUNKS):
+        part = pl.ds(c * n, n)
+        arrivals.append(pltpu.make_async_copy(w_ref.at[part], w_buf.at[part], in_sem.at[c]))
+        arrivals[-1].start()
+    departures = []
+
+    def send(source, target):
+        departures.append(
+            pltpu.make_async_copy(source, target, out_sem.at[len(departures)])
+        )
+        departures[-1].start()
+
     total = jnp.full((1, 128), mine_ref[0, 0] + other_ref[0, 0], f32)
     scale = lax.rsqrt(total / (RANK * (DA + D)) + mean_eps)[:, :1]
 
-    @pl.when(pl.program_id(0) == 0)
-    def _():
-        rows = rows_ref[...]
-        uq = jnp.dot(rows[:64], half_ref[:, :512], preferred_element_type=f32)
-        uo = jnp.dot(rows[64:], half_ref[:, 512:1536], preferred_element_type=f32)
-        step_q = scale * uq
-        step_o = scale * uo
-        step_q_ref[...] = step_q
-        step_o_ref[...] = step_o
-        new_q_ref[...] = wq_ref[...] - learn_rate * step_q
-        new_o_ref[...] = wo_ref[...] - learn_rate * step_o
-
-    p = p_ref[...]
-    n = p.shape[0]
-    pq = p[:, :64, :].reshape(n * 64, RANK)
-    po = p[:, 64:, :].reshape(n * 32, RANK)
-    uq = jnp.dot(pq, half_ref[:, :512], preferred_element_type=f32)
-    uo = jnp.dot(po, half_ref[:, 512:1536], preferred_element_type=f32)
-    wq = w_ref[:, :64, :].reshape(n * 64, 512)
-    copy_q_ref[...] = (wq - learn_rate * (scale * uq)).astype(bf16)
-    w0 = w_ref[:, 64:96, :].reshape(n * 32, 512)
-    w1 = w_ref[:, 96:, :].reshape(n * 32, 512)
-    copy_o_ref[:, :512] = (w0 - learn_rate * (scale * uo[:, :512])).astype(bf16)
-    copy_o_ref[:, 512:] = (w1 - learn_rate * (scale * uo[:, 512:])).astype(bf16)
+    rows = rows_ref[...]
+    step_q = scale * jnp.dot(rows[:64], half_ref[:, :512], preferred_element_type=f32)
+    step_o = scale * jnp.dot(rows[64:], half_ref[:, 512:1536], preferred_element_type=f32)
+    sq_buf[...] = step_q
+    so_buf[...] = step_o
+    nq_buf[...] = wq_ref[...] - learn_rate * step_q
+    no_buf[...] = wo_ref[...] - learn_rate * step_o
+    send(sq_buf, step_q_ref)
+    send(so_buf, step_o_ref)
+    send(nq_buf, new_q_ref)
+    send(no_buf, new_o_ref)
+
+    for c in range(CHUNKS):
+        part = pl.ds(c * n, n)
+        pq = p_ref[part, :64, :].reshape(n * 64, RANK)
+        po = p_ref[part, 64:, :].reshape(n * 32, RANK)
+        uq = jnp.dot(pq, half_ref[:, :512], preferred_element_type=f32)
+        uo = jnp.dot(po, half_ref[:, 512:1536], preferred_element_type=f32)
+        arrivals[c].wait()
+        q_rows, o_rows = pl.ds(c * n * 64, n * 64), pl.ds(c * n * 32, n * 32)
+        wq = w_buf[part, :64, :].reshape(n * 64, 512)
+        q_buf[q_rows, :] = (wq - learn_rate * (scale * uq)).astype(bf16)
+        w0 = w_buf[part, 64:96, :].reshape(n * 32, 512)
+        w1 = w_buf[part, 96:, :].reshape(n * 32, 512)
+        o_buf[o_rows, :512] = (w0 - learn_rate * (scale * uo[:, :512])).astype(bf16)
+        o_buf[o_rows, 512:] = (w1 - learn_rate * (scale * uo[:, 512:])).astype(bf16)
+        send(q_buf.at[q_rows], copy_q_ref.at[q_rows])
+        send(o_buf.at[o_rows], copy_o_ref.at[o_rows])
+    for departure in departures:
+        departure.wait()
 
 
 def finish(mine, other, half, rows, weight_query, weight_output, weights, factors):
-    step = 8
-
-    def whole(shape):
-        return pl.BlockSpec(shape, lambda i: (0,) * len(shape))
-
+    hbm = pl.BlockSpec(memory_space=pl.ANY)
+    leaving = [
+        jax.ShapeDtypeStruct((D, 512), bf16),
+        jax.ShapeDtypeStruct((DA, 1024), bf16),
+        jax.ShapeDtypeStruct((64, 512), f32),
+        jax.ShapeDtypeStruct((32, 1024), f32),
+        jax.ShapeDtypeStruct((64, 512), f32),
+        jax.ShapeDtypeStruct((32, 1024), f32),
+    ]
     return pl.pallas_call(
         finish_kernel,
-        grid=(FS // step,),
-        in_specs=[
-            SMEM,
-            SMEM,
-            whole((RANK, 1664)),
-            whole((96, RANK)),
-            whole((64, 512)),
-            whole((32, 1024)),
-            pl.BlockSpec((step, 128, 512), lambda i: (i, 0, 0)),
-            pl.BlockSpec((step, 96, RANK), lambda i: (i, 0, 0)),
-        ],
-        out_specs=[
-            pl.BlockSpec((step * 64, 512), lambda i: (i, 0)),
-            pl.BlockSpec((step * 32, 1024), lambda i: (i, 0)),
-            whole((64, 512)),
-            whole((32, 1024)),
-            whole((64, 512)),
-            whole((32, 1024)),
-        ],
-        out_shape=[
-            jax.ShapeDtypeStruct((D, 512), bf16),
-            jax.ShapeDtypeStruct((DA, 1024), bf16),
-            jax.ShapeDtypeStruct((64, 512), f32),
-            jax.ShapeDtypeStruct((32, 1024), f32),
-            jax.ShapeDtypeStruct((64, 512), f32),
-            jax.ShapeDtypeStruct((32, 1024), f32),
-        ],
+        in_specs=[SMEM, SMEM] + [VMEM] * 5 + [hbm],
+        out_specs=[hbm] * 6,
+        out_shape=leaving,
+        scratch_shapes=[pltpu.VMEM((FS, 128, 512), f32)]
+        + [pltpu.VMEM(a.shape, a.dtype) for a in leaving]
+        + [pltpu.SemaphoreType.DMA((CHUNKS,)), pltpu.SemaphoreType.DMA((4 + 2 * CHUNKS,))],
+        compiler_params=pltpu.CompilerParams(vmem_limit_bytes=32 * 2**20),
         name="finish",
-    )(mine, other, half, rows, weight_query, weight_output, weights, factors)
+    )(
+        mine,
+        other,
+        *[near(a) for a in (half, rows, weight_query, weight_output, factors)],
+        pltpu.with_memory_space_constraint(weights, pltpu.HBM),
+    )
 
 
 def local(
@@ -274,6 +320,7 @@
 
     weights = join(weight_query, weight_output)
     weights = lax.all_gather(weights, ("z", "x"), axis=0, tiled=True)
+    weights = decode(weights.reshape(FS, 128, 512))
 
     cots = jnp.concatenate([query_cot, output_cot], axis=1)
     cots = [shifted(cots, "rep", 1), shifted(cots, "rep", 2), shifted(cots, "rep", 3)]
@@ -284,12 +331,12 @@
 
     red = project(factors, inputs, attended).reshape(8, 2, FS, 128)
     red = exchange(red, ("rep", "tp")).reshape(NREP, NTP, 2, FS, 128)
-    part = exchange(partial_sums(here, red, [query_cot, output_cot] + cots), ("x", "z"))
+    part = partial_sums(here, red, [query_cot, output_cot] + cots)
+    part = exchange(part, ("x", "z"))
     low, half = normed_payload(
         here, part, first_query, second_query, first_output, second_output
     )
     half = exchange(half, "z")
-    low, half = lax.optimization_barrier((low, half))
     low_rows = [low, shifted(low, "rep", 1), shifted(low, "rep", 2), shifted(low, "rep", 3)]
     half = from_everyone(half.reshape(16, 1664), ("x", "rep"), 16).reshape(RANK, 1664)
     total = jnp.sum(half[:, 1536:].astype(f32)).reshape(1, 1)
@@ -307,7 +354,7 @@
 
     copy_q, copy_o, step_q, step_o, new_q, new_o = finish(
         total, other, half, rows, weight_query, weight_output,
-        weights.reshape(FS, 128, 512), whole,
+        weights, whole,
     )
 
     rolled = jnp.stack(low_rows)

time: 146 us -> 147 us (level)
  Pallas kernels: 14.6 us -> 20.9 us
  matrix products: 6.08 us -> 2.17 us
  waiting for transfers between devices: 55.1 us -> 52.2 us
  starting transfers between devices: 47.9 us -> 49.7 us
    pallas_call x1 -> x2, Pallas kernels: 8.37 us -> 14.3 us  [the longest x1 7.57 us: decode(): pl.pallas_call(decode_kernel, grid=(FS // step,), in_specs=[pl.BlockSpec(...]
    ppermute x8, starting transfers between devices: 13.2 us -> 17.9 us  [shifted(): return lax.ppermute(array, axis, [(i, (i + by) % n) for i in range(n)])]
    all_to_all x5, starting transfers between devices: 34.7 us -> 31.7 us  [exchange(): return lax.all_to_all(pieces, axes, split_axis=0, concat_axis=0, tiled=True)]
    dot_general x1, matrix products: 2.89 us -> 0.62 us  [local(): jnp.dot(others.reshape(FS * 96, 128), spread_other, preferred_element_typ...]
    all_to_all x5, waiting for transfers between devices: 54.2 us -> 52.2 us  [exchange(): return lax.all_to_all(pieces, axes, split_axis=0, concat_axis=0, tiled=True)]
    dot_general x1, matrix products: 2.26 us -> 0.62 us  [local(): jnp.dot(factors.reshape(FS * 96, 128), spread, preferred_element_type=f32)]
  transfers between devices with their start and end apart: 14 -> 14, of which waited for: 6 -> 5; matrix products, arithmetic and copies ran while one was open for 8% -> 6% of each run, Pallas kernels for 3% -> 8%
where the time goes in v5:
time: 147 us; the launch traced here: 146 us
  waiting for transfers between devices  52.2 us (36%)
  starting transfers between devices  49.7 us (34%)
  Pallas kernels  20.9 us (14%)
  between operations  14.3 us (10%)
  local copies, waits for them, and re-layouts  5.12 us (3%)
  matrix products  2.17 us (1%)
  other arithmetic  2.05 us (1%)
    all_to_all x5, waiting for transfers between devices, exchange(): return lax.all_to_all(pieces, axes, split_axis=0, concat_axis=0, tiled=True)  52.2 us
    all_to_all x5, starting transfers between devices, exchange(): return lax.all_to_all(pieces, axes, split_axis=0, concat_axis=0, tiled=True)  31.7 us
    ppermute x8, starting transfers between devices, shifted(): return lax.ppermute(array, axis, [(i, (i + by) % n) for i in range(n)])  17.9 us
    pallas_call x1, Pallas kernels, decode(): pl.pallas_call(decode_kernel, grid=(FS // step,), in_specs=[pl.BlockSpec(...  7.57 us
    pallas_call x1, Pallas kernels, finish(): pl.pallas_call(finish_kernel, in_specs=[SMEM, SMEM] + [VMEM] * 5 + [hbm],...  6.75 us
  transfers between devices with their start and end apart: 14, of which 5 were waited for; matrix products, arithmetic and copies ran while one was open for 6% of the time, Pallas kernels for 8%

profile of v5, /device:TPU:1, one launch (start us, length us, event | category | flops | bytes accessed | tf_op | source)
XLA Modules:
  0.0 146.5 jit_solution(2722481253785719828)
XLA Ops:
  7.3 1.8 %join.1 = bf16[128,512]{1,0:T(8,128)(2,1)} custom-call(f32[64,512]{1,0:T(8,128)} %wq_ref.1, f32[32,1024]{1,0:T(8,128)} %wo_ref.1), custom_call_target="tpu_custom_call" | custom-call | tf_op jit(solution)/shard_map/join/pallas_call | solution.py:83
  9.1 0.9 convolution_convert_fusion
  10.0 1.0 broadcast_in_dim.20
  11.0 11.9 %all-to-all-start = ((bf16[32,96,128]{2,1,0:T(8,128)(2,1)}), bf16[32,96,128]{2,1,0:T(8,128)(2,1)S(1)}, u32[]{:S(2)}, u32[]{:S(2)}) async-start(bf16[32,96,128]{2,1,0:T(8,128)(2,1)} %broadcast_in_dim.20), calls=%async_computation | async-start | bytes 1572864 | tf_op jit(solution)/shard_map/all_to_all | solution.py:26
  22.8 1.6 %constant_dynamic-update-slice_fusion.1 = bf16[128,1536]{1,0:T(8,128)(2,1)} fusion(bf16[128,512]{1,0:T(8,128)(2,1)} %query_ref.2), kind=kLoop, calls=%fused_computation.26 | loop fusion | bytes 262144
  24.4 0.7 constant_dynamic-update-slice_fusion
  25.1 1.3 collective-permute-start
  26.4 2.6 %collective-permute-start.1 = (bf16[128,1536]{1,0:T(8,128)(2,1)}, bf16[128,1536]{1,0:T(8,128)(2,1)}, u32[]{:S(2)}, u32[]{:S(2)}) collective-permute-start(bf16[128,1536]{1,0:T(8,128)(2,1)} %constant_dynamic-update-slice_fusion), channel_id=1, source_target_pairs={{0,4},{2,6},{4,0},{6,2},{1,5},{3,7},{5,1},{7,3},{8,12},{10,14},{12... | collective-permute-start | bytes 1179656 | tf_op jit(solution)/shard_map/ppermute | solution.py:35
  29.1 1.1 collective-permute-start.2
  30.1 16.3 %all-to-all-done.factor_ref = bf16[32,96,128]{2,1,0:T(8,128)(2,1)S(1)} async-done(((bf16[32,96,128]{2,1,0:T(8,128)(2,1)}), bf16[32,96,128]{2,1,0:T(8,128)(2,1)S(1)}, u32[]{:S(2)}, u32[]{:S(2)}) %all-to-all-start) | async-done | bytes 786464 | tf_op jit(solution)/shard_map/all_to_all | solution.py:26
  46.4 3.2 %collective-permute-start.4 = (bf16[32,96,128]{2,1,0:T(8,128)(2,1)S(1)}, bf16[32,96,128]{2,1,0:T(8,128)(2,1)S(1)}, u32[]{:S(2)}, u32[]{:S(2)}) collective-permute-start(bf16[32,96,128]{2,1,0:T(8,128)(2,1)S(1)} %all-to-all-done.factor_ref), channel_id=1, source_target_pairs={{0,1},{1,0},{2,3},{3,2},{4,5},{5,4},{6,7},{7,6},{8,9},{9,8},{10,11... | collective-permute-start | bytes 2359304 | tf_op jit(solution)/shard_map/ppermute | solution.py:35
  49.6 1.1 project.1
  50.8 4.6 %all-to-all-start.1 = ((f32[8,2,32,128]{3,2,1,0:T(8,128)}), f32[8,2,32,128]{3,2,1,0:T(8,128)S(1)}, u32[]{:S(2)}, u32[]{:S(2)}) async-start(f32[8,2,32,128]{3,2,1,0:T(8,128)} %bitcast.1), calls=%async_computation.1 | async-start | bytes 524288 | tf_op jit(solution)/shard_map/all_to_all | solution.py:26
  55.6 6.2 %all-to-all-done.1 = f32[8,2,32,128]{3,2,1,0:T(8,128)S(1)} async-done(((f32[8,2,32,128]{3,2,1,0:T(8,128)}), f32[8,2,32,128]{3,2,1,0:T(8,128)S(1)}, u32[]{:S(2)}, u32[]{:S(2)}) %all-to-all-start.1) | async-done | bytes 262176 | tf_op jit(solution)/shard_map/all_to_all | solution.py:26
  61.8 2.9 %partial_sums.1 = f32[32,2,1536]{2,1,0:T(2,128)} custom-call(s32[1]{0:T(128)} %bitcast.rep_ref, f32[4,2,2,32,128]{4,3,2,1,0:T(8,128)S(1)} %bitcast.24, bf16[128,512]{1,0:T(8,128)(2,1)} %query_ref.2, bf16[128,1024]{1,0:T(8,128)(2,1)} %output_ref.2, bf16[128,1536]{1,0:T(8,128)(2,1)} %copy-done.9, bf16[128,1536]{1,0:T(8,128)(2,1)} %collective-permute-done.1.c2_ref, ...), custom_call_target="tpu_custom_call" | custom-call | tf_op jit(solution)/shard_map/partial_sums/pallas_call | solution.py:154
  64.7 5.0 %all-to-all-start.2 = ((f32[32,2,1536]{2,1,0:T(2,128)}), f32[32,2,1536]{2,1,0:T(2,128)S(1)}, u32[]{:S(2)}, u32[]{:S(2)}) async-start(f32[32,2,1536]{2,1,0:T(2,128)} %partial_sums.1), calls=%async_computation.2 | async-start | bytes 786432 | tf_op jit(solution)/shard_map/all_to_all | solution.py:26
  69.8 0.6 fusion.1
  70.5 0.6 fusion
  71.1 13.7 %all-to-all-done.2.part_ref = f32[32,2,1536]{2,1,0:T(2,128)S(1)} async-done(((f32[32,2,1536]{2,1,0:T(2,128)}), f32[32,2,1536]{2,1,0:T(2,128)S(1)}, u32[]{:S(2)}, u32[]{:S(2)}) %all-to-all-start.2) | async-done | bytes 393248 | tf_op jit(solution)/shard_map/all_to_all | solution.py:26
  84.9 0.8 normed_payload.1
  86.1 3.2 %collective-permute-start.6 = (f32[2,1536]{1,0:T(2,128)S(1)}, f32[2,1536]{1,0:T(2,128)S(1)}, u32[]{:S(2)}, u32[]{:S(2)}) collective-permute-start(f32[2,1536]{1,0:T(2,128)S(1)} %get-tuple-element.23), channel_id=1, source_target_pairs={{0,4},{2,6},{4,0},{6,2},{1,5},{3,7},{5,1},{7,3},{8,12},{10,14},{12... | collective-permute-start | bytes 36872 | tf_op jit(solution)/shard_map/ppermute | solution.py:35
  89.8 5.3 %all-to-all-start.3 = ((bf16[8,2,1664]{2,1,0:T(2,128)(2,1)}), bf16[8,2,1664]{2,1,0:T(2,128)(2,1)S(1)}, u32[]{:S(2)}, u32[]{:S(2)}) async-start(bf16[8,2,1664]{2,1,0:T(2,128)(2,1)} %get-tuple-element.18), calls=%async_computation.3 | async-start | bytes 106496 | tf_op jit(solution)/shard_map/all_to_all | solution.py:26
  95.8 6.5 %all-to-all-done.3 = bf16[8,2,1664]{2,1,0:T(2,128)(2,1)S(1)} async-done(((bf16[8,2,1664]{2,1,0:T(2,128)(2,1)}), bf16[8,2,1664]{2,1,0:T(2,128)(2,1)S(1)}, u32[]{:S(2)}, u32[]{:S(2)}) %all-to-all-start.3) | async-done | bytes 53280 | tf_op jit(solution)/shard_map/all_to_all | solution.py:26
  102.3 1.0 broadcast_in_dim.21
  103.3 4.9 %all-to-all-start.4 = ((bf16[16,16,1664]{2,1,0:T(8,128)(2,1)}), bf16[16,16,1664]{2,1,0:T(8,128)(2,1)S(1)}, u32[]{:S(2)}, u32[]{:S(2)}) async-start(bf16[16,16,1664]{2,1,0:T(8,128)(2,1)} %broadcast_in_dim.21), calls=%async_computation.4 | async-start | bytes 1703936 | tf_op jit(solution)/shard_map/all_to_all | solution.py:26
  108.2 0.6 fusion.9
  108.9 0.6 fusion.8
  109.5 9.5 %all-to-all-done.4 = bf16[16,16,1664]{2,1,0:T(8,128)(2,1)S(1)} async-done(((bf16[16,16,1664]{2,1,0:T(8,128)(2,1)}), bf16[16,16,1664]{2,1,0:T(8,128)(2,1)S(1)}, u32[]{:S(2)}, u32[]{:S(2)}) %all-to-all-start.4) | async-done | bytes 852000 | tf_op jit(solution)/shard_map/all_to_all | solution.py:26
  119.0 0.6 convert_reduce_fusion
  119.6 5.7 %collective-permute-start.3 = (f32[1,1]{1,0:T(1,128)}, f32[1,1]{1,0:T(1,128)}, u32[]{:S(2)}, u32[]{:S(2)}) collective-permute-start(f32[1,1]{1,0:T(1,128)} %bitcast.4.mine_ref), channel_id=1, source_target_pairs={{0,1},{1,0},{2,3},{3,2},{4,5},{5,4},{6,7},{7,6},{8,9},{9,8},{10,11... | collective-permute-start | bytes 20 | tf_op jit(solution)/shard_map/ppermute | solution.py:35
  125.3 7.6 %decode.1.w_ref = f32[32,128,512]{2,1,0:T(8,128)} custom-call(bf16[32,128,512]{2,1,0:T(8,128)(2,1)} %bitcast.26), custom_call_target="tpu_custom_call" | custom-call | tf_op jit(solution)/shard_map/decode/pallas_call | solution.py:98
  132.8 6.8 %finish.1 = (bf16[2048,512]{1,0:T(8,128)(2,1)}, bf16[1024,1024]{1,0:T(8,128)(2,1)}, f32[64,512]{1,0:T(8,128)}, f32[32,1024]{1,0:T(8,128)}, f32[64,512]{1,0:T(8,128)}, /*index=5*/f32[32,1024]{1,0:T(8,128)}) custom-call(f32[1,1]{1,0:T(1,128)} %bitcast.4.mine_ref, f32[1,1]{1,0:T(1,128)} %collective-permute-done.3.other_ref, bf16[256,1664]{1,0:T(8,128)(2,1)S(1)} %bitcast.23, ...), custom_call_target="tpu_custom_call" | custom-call | tf_op jit(solution)/shard_map/finish/pallas_call | solution.py:283
  (46 shorter events, 2.0 us)
Async XLA Ops:
  7.2 17.2 %copy-start.8 = (bf16[128,1024]{1,0:T(8,128)(2,1)S(1)}, bf16[128,1024]{1,0:T(8,128)(2,1)}, u32[]{:S(2)}) copy-start(bf16[128,1024]{1,0:T(8,128)(2,1)} %output_ref.2) | copy-start | bytes 786436
  7.2 42.4 %copy-start.2 = (bf16[128,2048]{1,0:T(8,128)(2,1)S(1)}, bf16[128,2048]{1,0:T(8,128)(2,1)}, u32[]{:S(2)}) copy-start(bf16[128,2048]{1,0:T(8,128)(2,1)} %inputs_ref.1) | copy-start | bytes 1572868
  7.2 42.4 %copy-start.3 = (bf16[128,1024]{1,0:T(8,128)(2,1)S(1)}, bf16[128,1024]{1,0:T(8,128)(2,1)}, u32[]{:S(2)}) copy-start(bf16[128,1024]{1,0:T(8,128)(2,1)} %attended_ref.1) | copy-start | bytes 786436
  7.2 118.1 %all-gather.2.cloned.1.call-start = ((), (), s32[]{:S(2)}) async-start(), calls=%async_computation.5 | async-start | bytes 4325376 | tf_op jit(solution)/shard_map/all_gather | solution.py:322
  11.0 35.4 %all-to-all-start = ((bf16[32,96,128]{2,1,0:T(8,128)(2,1)}), bf16[32,96,128]{2,1,0:T(8,128)(2,1)S(1)}, u32[]{:S(2)}, u32[]{:S(2)}) async-start(bf16[32,96,128]{2,1,0:T(8,128)(2,1)} %broadcast_in_dim.20), calls=%async_computation | async-start | bytes 1572864 | tf_op jit(solution)/shard_map/all_to_all | solution.py:26
  25.1 30.4 %collective-permute-start = (bf16[128,1536]{1,0:T(8,128)(2,1)}, bf16[128,1536]{1,0:T(8,128)(2,1)S(1)}, u32[]{:S(2)}, u32[]{:S(2)}) collective-permute-start(bf16[128,1536]{1,0:T(8,128)(2,1)} %constant_dynamic-update-slice_fusion), channel_id=1, source_target_pairs={{0,2},{2,4},{4,6},{6,0},{1,3},{3,5},{5,7},{7,1},{8,10},{10,12},{12... | collective-permute-start | bytes 1179656 | tf_op jit(solution)/shard_map/ppermute | solution.py:35
  26.4 29.2 %collective-permute-start.1 = (bf16[128,1536]{1,0:T(8,128)(2,1)}, bf16[128,1536]{1,0:T(8,128)(2,1)}, u32[]{:S(2)}, u32[]{:S(2)}) collective-permute-start(bf16[128,1536]{1,0:T(8,128)(2,1)} %constant_dynamic-update-slice_fusion), channel_id=1, source_target_pairs={{0,4},{2,6},{4,0},{6,2},{1,5},{3,7},{5,1},{7,3},{8,12},{10,14},{12... | collective-permute-start | bytes 1179656 | tf_op jit(solution)/shard_map/ppermute | solution.py:35
  29.1 26.6 %collective-permute-start.2 = (bf16[128,1536]{1,0:T(8,128)(2,1)}, bf16[128,1536]{1,0:T(8,128)(2,1)}, u32[]{:S(2)}, u32[]{:S(2)}) collective-permute-start(bf16[128,1536]{1,0:T(8,128)(2,1)} %constant_dynamic-update-slice_fusion), channel_id=1, source_target_pairs={{0,6},{2,0},{4,2},{6,4},{1,7},{3,1},{5,3},{7,5},{8,14},{10,8},{12,... | collective-permute-start | bytes 1179656 | tf_op jit(solution)/shard_map/ppermute | solution.py:35
  46.4 24.1 %collective-permute-start.4 = (bf16[32,96,128]{2,1,0:T(8,128)(2,1)S(1)}, bf16[32,96,128]{2,1,0:T(8,128)(2,1)S(1)}, u32[]{:S(2)}, u32[]{:S(2)}) collective-permute-start(bf16[32,96,128]{2,1,0:T(8,128)(2,1)S(1)} %all-to-all-done.factor_ref), channel_id=1, source_target_pairs={{0,1},{1,0},{2,3},{3,2},{4,5},{5,4},{6,7},{7,6},{8,9},{9,8},{10,11... | collective-permute-start | bytes 2359304 | tf_op jit(solution)/shard_map/ppermute | solution.py:35
  50.8 11.1 %all-to-all-start.1 = ((f32[8,2,32,128]{3,2,1,0:T(8,128)}), f32[8,2,32,128]{3,2,1,0:T(8,128)S(1)}, u32[]{:S(2)}, u32[]{:S(2)}) async-start(f32[8,2,32,128]{3,2,1,0:T(8,128)} %bitcast.1), calls=%async_computation.1 | async-start | bytes 524288 | tf_op jit(solution)/shard_map/all_to_all | solution.py:26
  55.6 6.3 %copy-start.9 = (bf16[128,1536]{1,0:T(8,128)(2,1)}, bf16[128,1536]{1,0:T(8,128)(2,1)S(1)}, u32[]{:S(2)}) copy-start(bf16[128,1536]{1,0:T(8,128)(2,1)S(1)} %collective-permute-done.c1_ref) | copy-start | bytes 1179652
  64.7 20.1 %all-to-all-start.2 = ((f32[32,2,1536]{2,1,0:T(2,128)}), f32[32,2,1536]{2,1,0:T(2,128)S(1)}, u32[]{:S(2)}, u32[]{:S(2)}) async-start(f32[32,2,1536]{2,1,0:T(2,128)} %partial_sums.1), calls=%async_computation.2 | async-start | bytes 786432 | tf_op jit(solution)/shard_map/all_to_all | solution.py:26
  70.4 14.4 %copy-start.4 = (f32[8,1024]{1,0:T(8,128)S(1)}, f32[8,1024]{1,0:T(8,128)}, u32[]{:S(2)}) copy-start(f32[8,1024]{1,0:T(8,128)} %fo_ref.1) | copy-start | bytes 98308
  70.4 14.4 %copy-start.5 = (f32[8,1024]{1,0:T(8,128)S(1)}, f32[8,1024]{1,0:T(8,128)}, u32[]{:S(2)}) copy-start(f32[8,1024]{1,0:T(8,128)} %so_ref.1) | copy-start | bytes 98308
  70.4 14.4 %copy-start.6 = (f32[8,512]{1,0:T(8,128)S(1)}, f32[8,512]{1,0:T(8,128)}, u32[]{:S(2)}) copy-start(f32[8,512]{1,0:T(8,128)} %fq_ref.1) | copy-start | bytes 49156
  70.5 14.4 %copy-start.7 = (f32[8,512]{1,0:T(8,128)S(1)}, f32[8,512]{1,0:T(8,128)}, u32[]{:S(2)}) copy-start(f32[8,512]{1,0:T(8,128)} %sq_ref.1) | copy-start | bytes 49156
  85.7 9.4 %collective-permute-start.5 = (f32[2,1536]{1,0:T(2,128)S(1)}, f32[2,1536]{1,0:T(2,128)S(1)}, u32[]{:S(2)}, u32[]{:S(2)}) collective-permute-start(f32[2,1536]{1,0:T(2,128)S(1)} %get-tuple-element.23), channel_id=1, source_target_pairs={{0,2},{2,4},{4,6},{6,0},{1,3},{3,5},{5,7},{7,1},{8,10},{10,12},{12... | collective-permute-start | bytes 36872 | tf_op jit(solution)/shard_map/ppermute | solution.py:35
  86.1 9.0 %collective-permute-start.6 = (f32[2,1536]{1,0:T(2,128)S(1)}, f32[2,1536]{1,0:T(2,128)S(1)}, u32[]{:S(2)}, u32[]{:S(2)}) collective-permute-start(f32[2,1536]{1,0:T(2,128)S(1)} %get-tuple-element.23), channel_id=1, source_target_pairs={{0,4},{2,6},{4,0},{6,2},{1,5},{3,7},{5,1},{7,3},{8,12},{10,14},{12... | collective-permute-start | bytes 36872 | tf_op jit(solution)/shard_map/ppermute | solution.py:35
  89.2 5.9 %collective-permute-start.7 = (f32[2,1536]{1,0:T(2,128)S(1)}, f32[2,1536]{1,0:T(2,128)S(1)}, u32[]{:S(2)}, u32[]{:S(2)}) collective-permute-start(f32[2,1536]{1,0:T(2,128)S(1)} %get-tuple-element.23), channel_id=1, source_target_pairs={{0,6},{2,0},{4,2},{6,4},{1,7},{3,1},{5,3},{7,5},{8,14},{10,8},{12,... | collective-permute-start | bytes 36872 | tf_op jit(solution)/shard_map/ppermute | solution.py:35
  89.8 12.6 %all-to-all-start.3 = ((bf16[8,2,1664]{2,1,0:T(2,128)(2,1)}), bf16[8,2,1664]{2,1,0:T(2,128)(2,1)S(1)}, u32[]{:S(2)}, u32[]{:S(2)}) async-start(bf16[8,2,1664]{2,1,0:T(2,128)(2,1)} %get-tuple-element.18), calls=%async_computation.3 | async-start | bytes 106496 | tf_op jit(solution)/shard_map/all_to_all | solution.py:26
  103.3 15.7 %all-to-all-start.4 = ((bf16[16,16,1664]{2,1,0:T(8,128)(2,1)}), bf16[16,16,1664]{2,1,0:T(8,128)(2,1)S(1)}, u32[]{:S(2)}, u32[]{:S(2)}) async-start(bf16[16,16,1664]{2,1,0:T(8,128)(2,1)} %broadcast_in_dim.21), calls=%async_computation.4 | async-start | bytes 1703936 | tf_op jit(solution)/shard_map/all_to_all | solution.py:26
  119.6 13.2 %collective-permute-start.3 = (f32[1,1]{1,0:T(1,128)}, f32[1,1]{1,0:T(1,128)}, u32[]{:S(2)}, u32[]{:S(2)}) collective-permute-start(f32[1,1]{1,0:T(1,128)} %bitcast.4.mine_ref), channel_id=1, source_target_pairs={{0,1},{1,0},{2,3},{3,2},{4,5},{5,4},{6,7},{7,6},{8,9},{9,8},{10,11... | collective-permute-start | bytes 20 | tf_op jit(solution)/shard_map/ppermute | solution.py:35
  125.3 7.6 %copy-start = (f32[64,512]{1,0:T(8,128)S(1)}, f32[64,512]{1,0:T(8,128)}, u32[]{:S(2)}) copy-start(f32[64,512]{1,0:T(8,128)} %wq_ref.1) | copy-start | bytes 393220
  125.3 7.6 %copy-start.1 = (f32[32,1024]{1,0:T(8,128)S(1)}, f32[32,1024]{1,0:T(8,128)}, u32[]{:S(2)}) copy-start(f32[32,1024]{1,0:T(8,128)} %wo_ref.1) | copy-start | bytes 393220
Sparse Core Ops, SparseCore 0:
  11.2 89.8 all-gather.1

commit v6 on v5

--- a/solution.py
+++ b/solution.py
@@ -33,17 +33,6 @@
 def shifted(array, axis, by):
     n = lax.axis_size(axis)
     return lax.ppermute(array, axis, [(i, (i + by) % n) for i in range(n)])
-
-
-def one_hot(rows_of, columns, rows):
-    r = lax.broadcasted_iota(jnp.int32, (rows, columns), 0)
-    return (r == rows_of).astype(bf16)
-
-
-def rank_of(core):
-    k = lax.broadcasted_iota(jnp.int32, (1, RANK // NTP), 1)
-    x, j, z = k // 32, (k // 8) % 4, k % 8
-    return 8 * (4 * z + x) + 2 * j + core
 
 
 VMEM = pl.BlockSpec(memory_space=pltpu.VMEM)
@@ -73,20 +62,31 @@
     return jnp.where(v < 0, -s, s)
 
 
-def join_kernel(query_ref, output_ref, both_ref):
-    both_ref[:64] = coded(query_ref[...])
-    both_ref[64:96] = coded(output_ref[:, :512])
-    both_ref[96:] = coded(output_ref[:, 512:])
-
-
-def join(query, output):
-    return pl.pallas_call(
-        join_kernel,
-        in_specs=[VMEM, VMEM],
-        out_specs=VMEM,
-        out_shape=jax.ShapeDtypeStruct((128, 512), bf16),
-        name="join",
-    )(query, output)
+def prepare_kernel(core_ref, wq_ref, wo_ref, pq_ref, po_ref, code_ref, factor_ref):
+    k = lax.broadcasted_iota(jnp.int32, (RANK, 128), 1)
+    r = lax.broadcasted_iota(jnp.int32, (RANK, 128), 0)
+    core = core_ref[0]
+    ranks = (r == 32 * (k % 8) + 8 * (k // 32) + 2 * ((k // 8) % 4) + core).astype(bf16)
+    both = jnp.concatenate([pq_ref[...], po_ref[...]], axis=0)
+    mine = jnp.dot(both, ranks, preferred_element_type=f32).astype(bf16)
+    for n in range(FS):
+        factor_ref[n] = mine
+    code_ref[:64] = coded(wq_ref[...])
+    code_ref[64:96] = coded(wo_ref[:, :512])
+    code_ref[96:] = coded(wo_ref[:, 512:])
+
+
+def prepare(core, weight_query, weight_output, proj_query, proj_output):
+    return pl.pallas_call(
+        prepare_kernel,
+        in_specs=[SMEM] + [VMEM] * 4,
+        out_specs=[VMEM, VMEM],
+        out_shape=[
+            jax.ShapeDtypeStruct((128, 512), bf16),
+            jax.ShapeDtypeStruct((FS, 96, 128), bf16),
+        ],
+        name="prepare",
+    )(core, weight_query, weight_output, proj_query, proj_output)
 
 
 def decode_kernel(code_ref, out_ref):
@@ -156,6 +156,7 @@
         in_specs=[SMEM] + [VMEM] * 6,
         out_specs=VMEM,
         out_shape=pltpu.VMEM((FS, NTP, 1536), f32),
+        compiler_params=pltpu.CompilerParams(vmem_limit_bytes=16 * 2**20),
         name="partial_sums",
     )(rep, near(red), *cots)
 
@@ -209,6 +210,7 @@
             pltpu.VMEM((2, 1536), f32),
             pltpu.VMEM((NZ, 2, 1664), bf16),
         ],
+        compiler_params=pltpu.CompilerParams(vmem_limit_bytes=16 * 2**20),
         name="normed_payload",
     )(rep, *[near(a) for a in (part, first_query, second_query, first_output, second_output)])
 
@@ -318,16 +320,16 @@
 
     here = rep.reshape(1)
 
-    weights = join(weight_query, weight_output)
+    weights, factors = prepare(
+        core.reshape(1), weight_query, weight_output, proj_query, proj_output
+    )
     weights = lax.all_gather(weights, ("z", "x"), axis=0, tiled=True)
     weights = decode(weights.reshape(FS, 128, 512))
 
     cots = jnp.concatenate([query_cot, output_cot], axis=1)
     cots = [shifted(cots, "rep", 1), shifted(cots, "rep", 2), shifted(cots, "rep", 3)]
 
-    both = jnp.concatenate([proj_query, proj_output], axis=0)
-    mine = jnp.dot(both, one_hot(rank_of(core), 128, RANK), preferred_element_type=f32)
-    factors = from_everyone(mine.astype(bf16).reshape(96, 128), ("z", "x"), FS)
+    factors = exchange(factors, ("z", "x"))
 
     red = project(factors, inputs, attended).reshape(8, 2, FS, 128)
     red = exchange(red, ("rep", "tp")).reshape(NREP, NTP, 2, FS, 128)

time: 147 us -> 145 us (0.986)
  transfers between devices with their start and end apart: 14 -> 14, of which waited for: 5 -> 5; matrix products, arithmetic and copies ran while one was open for 6% -> 7% of each run, Pallas kernels for 8% -> 8%
where the time goes in v6:
time: 145 us; the launch traced here: 144 us
  waiting for transfers between devices  51.1 us (35%)
  starting transfers between devices  48.3 us (33%)
  Pallas kernels  20.1 us (14%)
  between operations  14.3 us (10%)
  local copies, waits for them, and re-layouts  6.03 us (4%)
  matrix products  2.39 us (2%)
  other arithmetic  2.08 us (1%)
    all_to_all x5, waiting for transfers between devices, exchange(): return lax.all_to_all(pieces, axes, split_axis=0, concat_axis=0, tiled=True)  51.1 us
    all_to_all x5, starting transfers between devices, exchange(): return lax.all_to_all(pieces, axes, split_axis=0, concat_axis=0, tiled=True)  31.6 us
    ppermute x8, starting transfers between devices, shifted(): return lax.ppermute(array, axis, [(i, (i + by) % n) for i in range(n)])  16.7 us
    pallas_call x1, Pallas kernels, decode(): pl.pallas_call(decode_kernel, grid=(FS // step,), in_specs=[pl.BlockSpec(...  7.57 us
    pallas_call x1, Pallas kernels, finish(): pl.pallas_call(finish_kernel, in_specs=[SMEM, SMEM] + [VMEM] * 5 + [hbm],...  6.83 us
  transfers between devices with their start and end apart: 14, of which 5 were waited for; matrix products, arithmetic and copies ran while one was open for 7% of the time, Pallas kernels for 8%

profile of v6, /device:TPU:1, one launch (start us, length us, event | category | flops | bytes accessed | tf_op | source)
XLA Modules:
  0.0 144.3 jit_solution(18042840361288885657)
XLA Ops:
  7.3 2.2 %prepare.1 = (bf16[128,512]{1,0:T(8,128)(2,1)}, bf16[32,96,128]{2,1,0:T(8,128)(2,1)}) custom-call(s32[1]{0:T(128)} %bitcast.1.core_ref, f32[64,512]{1,0:T(8,128)} %wq_ref.3, f32[32,1024]{1,0:T(8,128)} %wo_ref.3, bf16[64,256]{1,0:T(8,128)(2,1)} %pq_ref.1, bf16[32,256]{1,0:T(8,128)(2,1)} %po_ref.1), custom_call_target="tpu_custom_call" | custom-call | tf_op jit(solution)/shard_map/prepare/pallas_call | solution.py:80
  9.5 11.9 %all-to-all-start = ((bf16[32,96,128]{2,1,0:T(8,128)(2,1)}), bf16[32,96,128]{2,1,0:T(8,128)(2,1)S(1)}, u32[]{:S(2)}, u32[]{:S(2)}) async-start(bf16[32,96,128]{2,1,0:T(8,128)(2,1)} %get-tuple-element.20), calls=%async_computation | async-start | bytes 1572864 | tf_op jit(solution)/shard_map/all_to_all | solution.py:26
  21.4 1.6 %constant_dynamic-update-slice_fusion.1 = bf16[128,1536]{1,0:T(8,128)(2,1)} fusion(bf16[128,512]{1,0:T(8,128)(2,1)} %query_ref.1), kind=kLoop, calls=%fused_computation.20 | loop fusion | bytes 262144
  23.0 1.7 %constant_dynamic-update-slice_fusion = bf16[128,1536]{1,0:T(8,128)(2,1)} fusion(bf16[128,1536]{1,0:T(8,128)(2,1)} %constant_dynamic-update-slice_fusion.1, bf16[128,1024]{1,0:T(8,128)(2,1)} %output_ref.1), kind=kLoop, calls=%fused_computation.19 | loop fusion | bytes 524288 | tf_op jit(solution)/shard_map/concatenate | solution.py:329
  24.6 1.3 collective-permute-start
  25.9 2.6 %collective-permute-start.1 = (bf16[128,1536]{1,0:T(8,128)(2,1)}, bf16[128,1536]{1,0:T(8,128)(2,1)S(1)}, u32[]{:S(2)}, u32[]{:S(2)}) collective-permute-start(bf16[128,1536]{1,0:T(8,128)(2,1)} %constant_dynamic-update-slice_fusion), channel_id=1, source_target_pairs={{0,4},{2,6},{4,0},{6,2},{1,5},{3,7},{5,1},{7,3},{8,12},{10,14},{12... | collective-permute-start | bytes 1179656 | tf_op jit(solution)/shard_map/ppermute | solution.py:35
  28.6 1.1 collective-permute-start.2
  29.6 14.8 %all-to-all-done.factor_ref = bf16[32,96,128]{2,1,0:T(8,128)(2,1)S(1)} async-done(((bf16[32,96,128]{2,1,0:T(8,128)(2,1)}), bf16[32,96,128]{2,1,0:T(8,128)(2,1)S(1)}, u32[]{:S(2)}, u32[]{:S(2)}) %all-to-all-start) | async-done | bytes 786464 | tf_op jit(solution)/shard_map/all_to_all | solution.py:26
  44.4 3.3 %collective-permute-start.4 = (bf16[32,96,128]{2,1,0:T(8,128)(2,1)S(1)}, bf16[32,96,128]{2,1,0:T(8,128)(2,1)}, u32[]{:S(2)}, u32[]{:S(2)}) collective-permute-start(bf16[32,96,128]{2,1,0:T(8,128)(2,1)S(1)} %all-to-all-done.factor_ref), channel_id=1, source_target_pairs={{0,1},{1,0},{2,3},{3,2},{4,5},{5,4},{6,7},{7,6},{8,9},{9,8},{10,11... | collective-permute-start | bytes 2359304 | tf_op jit(solution)/shard_map/ppermute | solution.py:35
  47.8 0.9 copy-done.5
  48.7 1.1 project.1
  49.9 4.4 %all-to-all-start.1 = ((f32[8,2,32,128]{3,2,1,0:T(8,128)}), f32[8,2,32,128]{3,2,1,0:T(8,128)S(1)}, u32[]{:S(2)}, u32[]{:S(2)}) async-start(f32[8,2,32,128]{3,2,1,0:T(8,128)} %bitcast.2), calls=%async_computation.1 | async-start | bytes 524288 | tf_op jit(solution)/shard_map/all_to_all | solution.py:26
  54.5 6.2 %all-to-all-done.1 = f32[8,2,32,128]{3,2,1,0:T(8,128)S(1)} async-done(((f32[8,2,32,128]{3,2,1,0:T(8,128)}), f32[8,2,32,128]{3,2,1,0:T(8,128)S(1)}, u32[]{:S(2)}, u32[]{:S(2)}) %all-to-all-start.1) | async-done | bytes 262176 | tf_op jit(solution)/shard_map/all_to_all | solution.py:26
  60.8 1.5 %partial_sums.1 = f32[32,2,1536]{2,1,0:T(2,128)} custom-call(s32[1]{0:T(128)} %bitcast.rep_ref, f32[4,2,2,32,128]{4,3,2,1,0:T(8,128)S(1)} %bitcast.25, bf16[128,512]{1,0:T(8,128)(2,1)S(1)} %copy-done.4, bf16[128,1024]{1,0:T(8,128)(2,1)S(1)} %copy-done, bf16[128,1536]{1,0:T(8,128)(2,1)S(1)} %collective-permute-done.c1_ref, ...), custom_call_target="tpu_custom_call" | custom-call | tf_op jit(solution)/shard_map/partial_sums/pallas_call | solution.py:154
  62.3 5.1 %all-to-all-start.2 = ((f32[32,2,1536]{2,1,0:T(2,128)}), f32[32,2,1536]{2,1,0:T(2,128)S(1)}, u32[]{:S(2)}, u32[]{:S(2)}) async-start(f32[32,2,1536]{2,1,0:T(2,128)} %partial_sums.1), calls=%async_computation.2 | async-start | bytes 786432 | tf_op jit(solution)/shard_map/all_to_all | solution.py:26
  67.4 0.6 fusion.1
  68.1 1.8 %fusion = bf16[3072,256]{1,0:T(8,128)(2,1)S(1)} fusion(f32[3072,256]{1,0:T(8,128)S(1)} %fusion.1, bf16[3072,128]{1,0:T(8,128)(2,1)} %bitcast.7, s32[128]{0:T(128)S(1)} %get-tuple-element.34), kind=kOutput, calls=%fused_computation.2 | convolution fusion | flops 202932224 | bytes 5505536 | tf_op jit(solution)/shard_map/dot_general | solution.py:353
  69.9 13.8 %all-to-all-done.2.part_ref = f32[32,2,1536]{2,1,0:T(2,128)S(1)} async-done(((f32[32,2,1536]{2,1,0:T(2,128)}), f32[32,2,1536]{2,1,0:T(2,128)S(1)}, u32[]{:S(2)}, u32[]{:S(2)}) %all-to-all-start.2) | async-done | bytes 393248 | tf_op jit(solution)/shard_map/all_to_all | solution.py:26
  83.7 0.8 normed_payload.1
  85.3 2.0 %collective-permute-start.7 = (f32[2,1536]{1,0:T(2,128)S(1)}, f32[2,1536]{1,0:T(2,128)S(1)}, u32[]{:S(2)}, u32[]{:S(2)}) collective-permute-start(f32[2,1536]{1,0:T(2,128)S(1)} %get-tuple-element.27), channel_id=1, source_target_pairs={{0,6},{2,0},{4,2},{6,4},{1,7},{3,1},{5,3},{7,5},{8,14},{10,8},{12,... | collective-permute-start | bytes 36872 | tf_op jit(solution)/shard_map/ppermute | solution.py:35
  87.2 4.9 %all-to-all-start.3 = ((bf16[8,2,1664]{2,1,0:T(2,128)(2,1)}), bf16[8,2,1664]{2,1,0:T(2,128)(2,1)S(1)}, u32[]{:S(2)}, u32[]{:S(2)}) async-start(bf16[8,2,1664]{2,1,0:T(2,128)(2,1)} %get-tuple-element.21), calls=%async_computation.3 | async-start | bytes 106496 | tf_op jit(solution)/shard_map/all_to_all | solution.py:26
  92.2 0.6 gather_fusion
  92.9 6.7 %all-to-all-done.3 = bf16[8,2,1664]{2,1,0:T(2,128)(2,1)S(1)} async-done(((bf16[8,2,1664]{2,1,0:T(2,128)(2,1)}), bf16[8,2,1664]{2,1,0:T(2,128)(2,1)S(1)}, u32[]{:S(2)}, u32[]{:S(2)}) %all-to-all-start.3) | async-done | bytes 53280 | tf_op jit(solution)/shard_map/all_to_all | solution.py:26
  99.6 1.0 broadcast_in_dim.17
  100.6 5.2 %all-to-all-start.4 = ((bf16[16,16,1664]{2,1,0:T(8,128)(2,1)}), bf16[16,16,1664]{2,1,0:T(8,128)(2,1)S(1)}, u32[]{:S(2)}, u32[]{:S(2)}) async-start(bf16[16,16,1664]{2,1,0:T(8,128)(2,1)} %broadcast_in_dim.17), calls=%async_computation.4 | async-start | bytes 1703936 | tf_op jit(solution)/shard_map/all_to_all | solution.py:26
  105.9 0.6 fusion.5
  106.5 0.6 fusion.4
  107.1 9.5 %all-to-all-done.4 = bf16[16,16,1664]{2,1,0:T(8,128)(2,1)S(1)} async-done(((bf16[16,16,1664]{2,1,0:T(8,128)(2,1)}), bf16[16,16,1664]{2,1,0:T(8,128)(2,1)S(1)}, u32[]{:S(2)}, u32[]{:S(2)}) %all-to-all-start.4) | async-done | bytes 852000 | tf_op jit(solution)/shard_map/all_to_all | solution.py:26
  116.6 0.7 convert_reduce_fusion
  117.3 5.7 %collective-permute-start.3 = (f32[1,1]{1,0:T(1,128)}, f32[1,1]{1,0:T(1,128)}, u32[]{:S(2)}, u32[]{:S(2)}) collective-permute-start(f32[1,1]{1,0:T(1,128)} %bitcast.5.mine_ref), channel_id=1, source_target_pairs={{0,1},{1,0},{2,3},{3,2},{4,5},{5,4},{6,7},{7,6},{8,9},{9,8},{10,11... | collective-permute-start | bytes 20 | tf_op jit(solution)/shard_map/ppermute | solution.py:35
  123.0 7.6 %decode.1.w_ref = f32[32,128,512]{2,1,0:T(8,128)} custom-call(bf16[32,128,512]{2,1,0:T(8,128)(2,1)} %bitcast.27), custom_call_target="tpu_custom_call" | custom-call | tf_op jit(solution)/shard_map/decode/pallas_call | solution.py:98
  130.6 6.8 %finish.1 = (bf16[2048,512]{1,0:T(8,128)(2,1)}, bf16[1024,1024]{1,0:T(8,128)(2,1)}, f32[64,512]{1,0:T(8,128)}, f32[32,1024]{1,0:T(8,128)}, f32[64,512]{1,0:T(8,128)}, /*index=5*/f32[32,1024]{1,0:T(8,128)}) custom-call(f32[1,1]{1,0:T(1,128)} %bitcast.5.mine_ref, f32[1,1]{1,0:T(1,128)} %collective-permute-done.3.other_ref, bf16[256,1664]{1,0:T(8,128)(2,1)S(1)} %bitcast.24, ...), custom_call_target="tpu_custom_call" | custom-call | tf_op jit(solution)/shard_map/finish/pallas_call | solution.py:285
  (43 shorter events, 1.2 us)
Async XLA Ops:
  7.2 53.6 %copy-start.4 = (bf16[128,512]{1,0:T(8,128)(2,1)S(1)}, bf16[128,512]{1,0:T(8,128)(2,1)}, u32[]{:S(2)}) copy-start(bf16[128,512]{1,0:T(8,128)(2,1)} %query_ref.1) | copy-start | bytes 393220
  7.2 53.6 %copy-start = (bf16[128,1024]{1,0:T(8,128)(2,1)S(1)}, bf16[128,1024]{1,0:T(8,128)(2,1)}, u32[]{:S(2)}) copy-start(bf16[128,1024]{1,0:T(8,128)(2,1)} %output_ref.1) | copy-start | bytes 786436
  7.2 40.6 %copy-start.3 = (bf16[128,2048]{1,0:T(8,128)(2,1)S(1)}, bf16[128,2048]{1,0:T(8,128)(2,1)}, u32[]{:S(2)}) copy-start(bf16[128,2048]{1,0:T(8,128)(2,1)} %inputs_ref.1) | copy-start | bytes 1572868
  7.2 115.8 %all-gather.2.cloned.1.call-start = ((), (), s32[]{:S(2)}) async-start(), calls=%async_computation.5 | async-start | bytes 4325376 | tf_op jit(solution)/shard_map/all_gather | solution.py:326
  9.5 34.9 %all-to-all-start = ((bf16[32,96,128]{2,1,0:T(8,128)(2,1)}), bf16[32,96,128]{2,1,0:T(8,128)(2,1)S(1)}, u32[]{:S(2)}, u32[]{:S(2)}) async-start(bf16[32,96,128]{2,1,0:T(8,128)(2,1)} %get-tuple-element.20), calls=%async_computation | async-start | bytes 1572864 | tf_op jit(solution)/shard_map/all_to_all | solution.py:26
  24.6 29.9 %collective-permute-start = (bf16[128,1536]{1,0:T(8,128)(2,1)}, bf16[128,1536]{1,0:T(8,128)(2,1)S(1)}, u32[]{:S(2)}, u32[]{:S(2)}) collective-permute-start(bf16[128,1536]{1,0:T(8,128)(2,1)} %constant_dynamic-update-slice_fusion), channel_id=1, source_target_pairs={{0,2},{2,4},{4,6},{6,0},{1,3},{3,5},{5,7},{7,1},{8,10},{10,12},{12... | collective-permute-start | bytes 1179656 | tf_op jit(solution)/shard_map/ppermute | solution.py:35
  25.9 28.6 %collective-permute-start.1 = (bf16[128,1536]{1,0:T(8,128)(2,1)}, bf16[128,1536]{1,0:T(8,128)(2,1)S(1)}, u32[]{:S(2)}, u32[]{:S(2)}) collective-permute-start(bf16[128,1536]{1,0:T(8,128)(2,1)} %constant_dynamic-update-slice_fusion), channel_id=1, source_target_pairs={{0,4},{2,6},{4,0},{6,2},{1,5},{3,7},{5,1},{7,3},{8,12},{10,14},{12... | collective-permute-start | bytes 1179656 | tf_op jit(solution)/shard_map/ppermute | solution.py:35
  28.6 26.0 %collective-permute-start.2 = (bf16[128,1536]{1,0:T(8,128)(2,1)}, bf16[128,1536]{1,0:T(8,128)(2,1)S(1)}, u32[]{:S(2)}, u32[]{:S(2)}) collective-permute-start(bf16[128,1536]{1,0:T(8,128)(2,1)} %constant_dynamic-update-slice_fusion), channel_id=1, source_target_pairs={{0,6},{2,0},{4,2},{6,4},{1,7},{3,1},{5,3},{7,5},{8,14},{10,8},{12,... | collective-permute-start | bytes 1179656 | tf_op jit(solution)/shard_map/ppermute | solution.py:35
  44.4 23.6 %collective-permute-start.4 = (bf16[32,96,128]{2,1,0:T(8,128)(2,1)S(1)}, bf16[32,96,128]{2,1,0:T(8,128)(2,1)}, u32[]{:S(2)}, u32[]{:S(2)}) collective-permute-start(bf16[32,96,128]{2,1,0:T(8,128)(2,1)S(1)} %all-to-all-done.factor_ref), channel_id=1, source_target_pairs={{0,1},{1,0},{2,3},{3,2},{4,5},{5,4},{6,7},{7,6},{8,9},{9,8},{10,11... | collective-permute-start | bytes 2359304 | tf_op jit(solution)/shard_map/ppermute | solution.py:35
  47.8 1.0 copy-start.5
  49.9 10.9 %all-to-all-start.1 = ((f32[8,2,32,128]{3,2,1,0:T(8,128)}), f32[8,2,32,128]{3,2,1,0:T(8,128)S(1)}, u32[]{:S(2)}, u32[]{:S(2)}) async-start(f32[8,2,32,128]{3,2,1,0:T(8,128)} %bitcast.2), calls=%async_computation.1 | async-start | bytes 524288 | tf_op jit(solution)/shard_map/all_to_all | solution.py:26
  62.3 21.4 %all-to-all-start.2 = ((f32[32,2,1536]{2,1,0:T(2,128)}), f32[32,2,1536]{2,1,0:T(2,128)S(1)}, u32[]{:S(2)}, u32[]{:S(2)}) async-start(f32[32,2,1536]{2,1,0:T(2,128)} %partial_sums.1), calls=%async_computation.2 | async-start | bytes 786432 | tf_op jit(solution)/shard_map/all_to_all | solution.py:26
  68.0 15.7 %copy-start.6 = (f32[8,1024]{1,0:T(8,128)S(1)}, f32[8,1024]{1,0:T(8,128)}, u32[]{:S(2)}) copy-start(f32[8,1024]{1,0:T(8,128)} %fo_ref.1) | copy-start | bytes 98308
  68.1 15.7 %copy-start.7 = (f32[8,1024]{1,0:T(8,128)S(1)}, f32[8,1024]{1,0:T(8,128)}, u32[]{:S(2)}) copy-start(f32[8,1024]{1,0:T(8,128)} %so_ref.1) | copy-start | bytes 98308
  68.1 15.6 %copy-start.8 = (f32[8,512]{1,0:T(8,128)S(1)}, f32[8,512]{1,0:T(8,128)}, u32[]{:S(2)}) copy-start(f32[8,512]{1,0:T(8,128)} %fq_ref.1) | copy-start | bytes 49156
  68.1 15.6 %copy-start.9 = (f32[8,512]{1,0:T(8,128)S(1)}, f32[8,512]{1,0:T(8,128)}, u32[]{:S(2)}) copy-start(f32[8,512]{1,0:T(8,128)} %sq_ref.1) | copy-start | bytes 49156
  84.5 7.7 %collective-permute-start.5 = (f32[2,1536]{1,0:T(2,128)S(1)}, f32[2,1536]{1,0:T(2,128)S(1)}, u32[]{:S(2)}, u32[]{:S(2)}) collective-permute-start(f32[2,1536]{1,0:T(2,128)S(1)} %get-tuple-element.27), channel_id=1, source_target_pairs={{0,2},{2,4},{4,6},{6,0},{1,3},{3,5},{5,7},{7,1},{8,10},{10,12},{12... | collective-permute-start | bytes 36872 | tf_op jit(solution)/shard_map/ppermute | solution.py:35
  84.8 7.4 %collective-permute-start.6 = (f32[2,1536]{1,0:T(2,128)S(1)}, f32[2,1536]{1,0:T(2,128)S(1)}, u32[]{:S(2)}, u32[]{:S(2)}) collective-permute-start(f32[2,1536]{1,0:T(2,128)S(1)} %get-tuple-element.27), channel_id=1, source_target_pairs={{0,4},{2,6},{4,0},{6,2},{1,5},{3,7},{5,1},{7,3},{8,12},{10,14},{12... | collective-permute-start | bytes 36872 | tf_op jit(solution)/shard_map/ppermute | solution.py:35
  85.3 6.9 %collective-permute-start.7 = (f32[2,1536]{1,0:T(2,128)S(1)}, f32[2,1536]{1,0:T(2,128)S(1)}, u32[]{:S(2)}, u32[]{:S(2)}) collective-permute-start(f32[2,1536]{1,0:T(2,128)S(1)} %get-tuple-element.27), channel_id=1, source_target_pairs={{0,6},{2,0},{4,2},{6,4},{1,7},{3,1},{5,3},{7,5},{8,14},{10,8},{12,... | collective-permute-start | bytes 36872 | tf_op jit(solution)/shard_map/ppermute | solution.py:35
  87.2 12.4 %all-to-all-start.3 = ((bf16[8,2,1664]{2,1,0:T(2,128)(2,1)}), bf16[8,2,1664]{2,1,0:T(2,128)(2,1)S(1)}, u32[]{:S(2)}, u32[]{:S(2)}) async-start(bf16[8,2,1664]{2,1,0:T(2,128)(2,1)} %get-tuple-element.21), calls=%async_computation.3 | async-start | bytes 106496 | tf_op jit(solution)/shard_map/all_to_all | solution.py:26
  100.6 16.0 %all-to-all-start.4 = ((bf16[16,16,1664]{2,1,0:T(8,128)(2,1)}), bf16[16,16,1664]{2,1,0:T(8,128)(2,1)S(1)}, u32[]{:S(2)}, u32[]{:S(2)}) async-start(bf16[16,16,1664]{2,1,0:T(8,128)(2,1)} %broadcast_in_dim.17), calls=%async_computation.4 | async-start | bytes 1703936 | tf_op jit(solution)/shard_map/all_to_all | solution.py:26
  117.3 13.3 %collective-permute-start.3 = (f32[1,1]{1,0:T(1,128)}, f32[1,1]{1,0:T(1,128)}, u32[]{:S(2)}, u32[]{:S(2)}) collective-permute-start(f32[1,1]{1,0:T(1,128)} %bitcast.5.mine_ref), channel_id=1, source_target_pairs={{0,1},{1,0},{2,3},{3,2},{4,5},{5,4},{6,7},{7,6},{8,9},{9,8},{10,11... | collective-permute-start | bytes 20 | tf_op jit(solution)/shard_map/ppermute | solution.py:35
  123.0 7.6 %copy-start.1 = (f32[64,512]{1,0:T(8,128)S(1)}, f32[64,512]{1,0:T(8,128)}, u32[]{:S(2)}) copy-start(f32[64,512]{1,0:T(8,128)} %wq_ref.3) | copy-start | bytes 393220
  123.0 7.6 %copy-start.2 = (f32[32,1024]{1,0:T(8,128)S(1)}, f32[32,1024]{1,0:T(8,128)}, u32[]{:S(2)}) copy-start(f32[32,1024]{1,0:T(8,128)} %wo_ref.3) | copy-start | bytes 393220
Sparse Core Ops, SparseCore 0:
  11.2 89.0 all-gather.1
